TPU v7x, 512 devices: a whole 4x4x16 slice. The times are simulated.
512 devices in a mesh: kv: 128 (over z, x, core), tp: 4 (over y).
Axes of the slice: x: 4, y: 4, z: 16, core: 2. Of those that a mesh axis runs over, the one named last changes fastest.
Arguments:
- queries: bfloat16 [16384, 4096], P('kv', 'tp'), may hold values from -6 to 6
- keys: bfloat16 [16384, 512], P('kv', 'tp'), may hold values from -6 to 6
- values: bfloat16 [16384, 512], P('kv', 'tp'), may hold values from -6 to 6
- logsum: float32 [16384, 32], P('kv', 'tp'), may hold values from 2 to 6
- out_grad: bfloat16 [16384, 4096], P('kv', 'tp'), may hold values from -6 to 6
- normed_input: bfloat16 [16384, 4096], P('kv', 'tp'), may hold values from -6 to 6
- chosen: int32 [256, 16], P('kv'), may hold values from 0 to 511, as said below
Outputs:
- query_grad: float32 [16384, 4096], P('kv', 'tp')
- key_grad: float32 [16384, 512], P('kv', 'tp')
- value_grad: float32 [16384, 512], P('kv', 'tp')
- value_weight_grad: float32 [4096, 512], P('kv', 'tp')
Inputs may be any that keep to these rules, and one draw needn't show every extreme that they name: `chosen`: each row r names 16 distinct key blocks, among them block 0 and the blocks r * 2 to r * 2 + 64 / 32 - 1 that hold the query block's own positions. The rows of one device (aligned runs of 2 rows) name at most one block of any other device's 128 / 32 blocks. Blocks after the query block may be named; their keys are masked.
All inputs are finite; a program needn't handle non-finite values.
Results may differ from a plain program's by a relative error of at most 0.008.
Values may be sent and summed in bfloat16 or wider, within the bound.
No kernel may reach another device: no remote copies, remote signals or barrier semaphores. Data moves between devices by JAX's collectives and lax.ppermute only.
A program may use at most 64 MiB of HBM per device.

v0:
```python
import jax
import jax.numpy as jnp
from jax import lax
from jax.sharding import Mesh
from jax.sharding import PartitionSpec as P

HD = 128
QB = 64
KB = 32
NSEL = 16
KV = ("kv_0", "kv_1", "kv_2")


def side_by_side(arrays, axis, split_dim, concat_dim, along):
    both = jnp.concatenate(arrays, axis=along)
    whole, at, gathered = (
        lax.all_to_all(both, axis, split_axis=split_dim, concat_axis=concat_dim, tiled=True),
        0,
        [],
    )
    for a in arrays:
        gathered.append(lax.slice_in_dim(whole, at, at + a.shape[along], axis=along))
        at += a.shape[along]
    return tuple(gathered)


def from_everyone(shard, axis):
    copies = jnp.broadcast_to(shard, (lax.axis_size(axis), *shard.shape))
    return lax.all_to_all(copies, axis, split_axis=0, concat_axis=0, tiled=True)


def laid_out(parts, dim):
    parts = jnp.moveaxis(parts, 0, dim)
    dims = parts.shape
    return parts.reshape(*dims[:dim], dims[dim] * dims[dim + 1], *dims[dim + 2 :])


def gathered_copies(shard, axis, dim):
    parts = from_everyone(shard, axis)
    return laid_out(parts, dim)


def cut_along(shard, dim, devices):
    dims = shard.shape
    parts = shard.reshape(*dims[:dim], devices, dims[dim] // devices, *dims[dim + 1 :])
    return jnp.moveaxis(parts, dim, 0)


def sum_at_owner(shard, axis, dim):
    devices = lax.axis_size(axis)
    parts = lax.all_to_all(cut_along(shard, dim, devices), axis, 0, 0, tiled=True)
    return jnp.sum(parts.astype(jnp.float32), axis=0)


def sum_in_two_steps(shard, axes, dim):
    far, near = axes
    own = sum_at_owner(cut_along(shard, dim, lax.axis_size(far)), near, dim + 1)
    return jnp.sum(
        lax.all_to_all(own.astype(jnp.bfloat16), far, 0, 0, tiled=True).astype(jnp.float32), axis=0
    )


def local(queries, keys, values, logsum, out_grad, normed_input, chosen):
    devices = lax.axis_size(KV)
    here = lax.axis_index(KV)
    tok = keys.shape[0]
    kv_cols = keys.shape[1]
    kv_heads = kv_cols // HD
    group = queries.shape[1] // kv_cols
    kblocks = tok // KB
    qblocks = tok // QB
    span = NSEL * KB
    scale = HD ** (-0.5)
    owner = chosen // kblocks
    within = chosen % kblocks
    remote = owner != here
    peers = jnp.arange(devices, dtype=jnp.int32)
    named = (owner[:, :, None] == peers[None, None, :]) & remote[:, :, None]
    wanted = jnp.max(jnp.where(named, within[:, :, None] + 1, 0), axis=(0, 1))
    asked = (
        lax.all_to_all(
            wanted.reshape(devices, 1), KV, split_axis=0, concat_axis=0, tiled=True
        ).reshape(devices)
        - 1
    )
    key_blocks = keys.reshape(kblocks, KB, kv_cols)
    value_blocks = values.reshape(kblocks, KB, kv_cols)
    taken = jnp.maximum(asked, 0)
    live = (asked >= 0)[:, None, None]
    send_keys = jnp.where(live, key_blocks[taken], jnp.zeros((), keys.dtype))
    send_values = jnp.where(live, value_blocks[taken], jnp.zeros((), values.dtype))
    got_keys, got_values = side_by_side((send_keys, send_values), KV, 0, 0, 1)
    pool_keys = jnp.concatenate([key_blocks, got_keys], axis=0)
    pool_values = jnp.concatenate([value_blocks, got_values], axis=0)
    slot = jnp.where(remote, kblocks + owner, within)
    sel_keys = pool_keys[slot].reshape(qblocks, span, kv_heads, HD)
    sel_values = pool_values[slot].reshape(qblocks, span, kv_heads, HD)
    query_rows = queries.reshape(qblocks, QB, kv_heads, group, HD)
    dout = out_grad.reshape(qblocks, QB, kv_heads, group, HD)
    lse = logsum.reshape(qblocks, QB, kv_heads, group)
    scores = (
        jnp.einsum("bqngd,bjnd->bqngj", query_rows, sel_keys, preferred_element_type=jnp.float32)
        * scale
    )
    qpos = here * tok + jnp.arange(tok, dtype=jnp.int32).reshape(qblocks, QB)
    kpos = (chosen[:, :, None] * KB + jnp.arange(KB, dtype=jnp.int32)[None, None, :]).reshape(
        qblocks, span
    )
    valid = (kpos[:, None, :] <= qpos[:, :, None])[:, :, None, None, :]
    prob = jnp.where(valid, jnp.exp(scores - lse[..., None]), 0.0)
    dprob = jnp.einsum("bqngd,bjnd->bqngj", dout, sel_values, preferred_element_type=jnp.float32)
    delta = jnp.sum(prob * dprob, axis=-1, keepdims=True)
    dscore = (prob * (dprob - delta)).astype(jnp.bfloat16)
    prob_low = prob.astype(jnp.bfloat16)
    query_grad = (
        jnp.einsum("bqngj,bjnd->bqngd", dscore, sel_keys, preferred_element_type=jnp.float32)
        * scale
    )
    query_grad = query_grad.reshape(tok, queries.shape[1])
    key_part = (
        jnp.einsum("bqngj,bqngd->bjnd", dscore, query_rows, preferred_element_type=jnp.float32)
        * scale
    )
    value_part = jnp.einsum("bqngj,bqngd->bjnd", prob_low, dout, preferred_element_type=jnp.float32)
    entries = qblocks * NSEL
    pool_size = kblocks + devices
    onehot = (slot.reshape(entries, 1) == jnp.arange(pool_size, dtype=jnp.int32)[None, :]).astype(
        jnp.float32
    )
    key_sum = jnp.dot(
        onehot.T,
        key_part.reshape(entries, KB * kv_cols),
        precision=lax.Precision.HIGHEST,
        preferred_element_type=jnp.float32,
    )
    value_sum = jnp.dot(
        onehot.T,
        value_part.reshape(entries, KB * kv_cols),
        precision=lax.Precision.HIGHEST,
        preferred_element_type=jnp.float32,
    )
    back_keys = key_sum[kblocks:].reshape(devices, KB, kv_cols)
    back_values = value_sum[kblocks:].reshape(devices, KB, kv_cols)
    ret_keys, ret_values = tuple(
        (
            part.astype(jnp.float32)
            for part in side_by_side(
                (back_keys.astype(jnp.bfloat16), back_values.astype(jnp.bfloat16)), KV, 0, 0, 1
            )
        )
    )
    home = (asked[:, None] == jnp.arange(kblocks, dtype=jnp.int32)[None, :]).astype(jnp.float32)
    key_grad = key_sum[:kblocks] + jnp.dot(
        home.T,
        ret_keys.reshape(devices, KB * kv_cols),
        precision=lax.Precision.HIGHEST,
        preferred_element_type=jnp.float32,
    )
    value_grad = value_sum[:kblocks] + jnp.dot(
        home.T,
        ret_values.reshape(devices, KB * kv_cols),
        precision=lax.Precision.HIGHEST,
        preferred_element_type=jnp.float32,
    )
    key_grad = key_grad.reshape(tok, kv_cols)
    value_grad = value_grad.reshape(tok, kv_cols)
    value_low = value_grad.astype(jnp.bfloat16)
    full_input = gathered_copies(normed_input, "tp", 1)
    weight_grad = sum_in_two_steps(
        jnp.einsum("td,tc->dc", full_input, value_low, preferred_element_type=jnp.float32).astype(
            jnp.bfloat16
        ),
        (("kv_0", "kv_1"), "kv_2"),
        0,
    )
    return (query_grad, key_grad, value_grad, weight_grad)


def solution(mesh):
    split = Mesh(mesh.devices.reshape(16, 4, 2, mesh.shape["tp"]), ("kv_0", "kv_1", "kv_2", "tp"))
    placed = (
        P(KV, "tp"),
        P(KV, "tp"),
        P(KV, "tp"),
        P(KV, "tp"),
        P(KV, "tp"),
        P(KV, "tp"),
        P(KV, None),
    )
    return jax.shard_map(
        local,
        mesh=split,
        in_specs=placed,
        out_specs=(P(KV, "tp"), P(KV, "tp"), P(KV, "tp"), P(KV, "tp")),
        check_vma=False,
    )
```

profile of v0, /device:TPU:2, one launch (start us, length us, event | category | flops | bytes accessed | tf_op | source)
XLA Modules:
  0.0 340.8 jit_solution(15525004218114130249)
XLA Ops:
  1.6 33.2 %all_to_all.34 = s32[128,1,1]{2,1,0:T(1,128)S(1)} all-to-all(s32[128,1,1]{2,1,0:T(1,128)S(1)} %copy.44), channel_id=1, replica_groups=mesh['kv_0'=16,'kv_1'=4,'kv_2'=2,'tp'=4] {'kv_0','kv_1','kv_2'}, dimensions={0} | all-to-all | bytes 1024 | tf_op jit(solution)/shard_map/all_to_all | solution.py:81
  34.8 4.6 %fusion.29 = (s32[128]{0:T(128)S(1)}, s32[128]{0:T(128)S(1)}) fusion(s32[128,1,1]{2,1,0:T(1,128)S(1)} %all_to_all.34), kind=kLoop, calls=%fused_computation.64 | loop fusion | flops 256 | bytes 1536 | tf_op jit(solution)/shard_map/sub | solution.py:81
  39.4 1.5 gather_fusion
  41.7 2.4 compare_reduce_fusion
  44.3 1.6 pad_maximum_fusion
  45.9 6.8 %all-to-all-start.1 = ((bf16[128,64,128]{2,1,0:T(8,128)(2,1)}), bf16[128,64,128]{2,1,0:T(8,128)(2,1)S(1)}, u32[]{:S(2)}, u32[]{:S(2)}) async-start(bf16[128,64,128]{2,1,0:T(8,128)(2,1)} %pad_maximum_fusion), calls=%async_computation.1 | async-start | bytes 4194304 | tf_op jit(solution)/shard_map/all_to_all | solution.py:17
  53.5 95.7 %all-to-all-done.1 = bf16[128,64,128]{2,1,0:T(8,128)(2,1)S(1)} async-done(((bf16[128,64,128]{2,1,0:T(8,128)(2,1)}), bf16[128,64,128]{2,1,0:T(8,128)(2,1)S(1)}, u32[]{:S(2)}, u32[]{:S(2)}) %all-to-all-start.1) | async-done | bytes 2097184 | tf_op jit(solution)/shard_map/all_to_all | solution.py:17
  153.2 1.1 fusion.24
  156.4 1.1 fusion.25
  158.9 1.7 pad_maximum_fusion.1
  160.5 10.5 %all-to-all-start.2 = ((bf16[128,64,128]{2,1,0:T(8,128)(2,1)}), bf16[128,64,128]{2,1,0:T(8,128)(2,1)S(1)}, u32[]{:S(2)}, u32[]{:S(2)}) async-start(bf16[128,64,128]{2,1,0:T(8,128)(2,1)} %pad_maximum_fusion.1), calls=%async_computation.2 | async-start | bytes 4194304 | tf_op jit(solution)/shard_map/all_to_all | solution.py:17
  171.1 1.8 copy.51
  172.8 94.6 %all-to-all-done.2 = bf16[128,64,128]{2,1,0:T(8,128)(2,1)S(1)} async-done(((bf16[128,64,128]{2,1,0:T(8,128)(2,1)}), bf16[128,64,128]{2,1,0:T(8,128)(2,1)S(1)}, u32[]{:S(2)}, u32[]{:S(2)}) %all-to-all-start.2) | async-done | bytes 2097184 | tf_op jit(solution)/shard_map/all_to_all | solution.py:17
  267.4 2.1 broadcast_in_dim.72
  269.5 4.5 %all-to-all-start.3 = ((bf16[4,128,1024]{1,2,0:T(8,128)(2,1)}), bf16[4,128,1024]{1,2,0:T(8,128)(2,1)}, u32[]{:S(2)}, u32[]{:S(2)}) async-start(bf16[4,128,1024]{1,2,0:T(8,128)(2,1)} %broadcast_in_dim.72), calls=%async_computation.3 | async-start | bytes 2097152 | tf_op jit(solution)/shard_map/all_to_all | solution.py:29
  274.0 1.3 fusion.30
  275.3 1.3 fusion.32
  276.7 13.5 %all-to-all-done.3 = bf16[4,128,1024]{1,2,0:T(8,128)(2,1)} async-done(((bf16[4,128,1024]{1,2,0:T(8,128)(2,1)}), bf16[4,128,1024]{1,2,0:T(8,128)(2,1)}, u32[]{:S(2)}, u32[]{:S(2)}) %all-to-all-start.3) | async-done | bytes 1048608 | tf_op jit(solution)/shard_map/all_to_all | solution.py:29
  290.2 1.7 fusion
  292.6 4.6 %all_to_all.35 = bf16[2,64,32,128]{3,2,1,0:T(8,128)(2,1)S(1)} all-to-all(bf16[2,64,32,128]{3,2,1,0:T(8,128)(2,1)S(1)} %copy.53), channel_id=1, replica_groups=mesh['kv_0'=16,'kv_1'=4,'kv_2'=2,'tp'=4] {'kv_2'}, dimensions={0} | all-to-all | bytes 2097152 | tf_op jit(solution)/shard_map/all_to_all | solution.py:51
  297.2 1.1 reduce_sum.31
  298.3 8.8 %all-to-all-start.5 = ((bf16[64,32,128]{2,1,0:T(8,128)(2,1)}), bf16[64,32,128]{2,1,0:T(8,128)(2,1)S(1)}, u32[]{:S(2)}, u32[]{:S(2)}) async-start(bf16[64,32,128]{2,1,0:T(8,128)(2,1)} %reduce_sum.31), calls=%async_computation.5 | async-start | bytes 1048576 | tf_op jit(solution)/shard_map/all_to_all | solution.py:59
  308.8 1.3 convolution_add_fusion.1
  311.5 28.6 %all-to-all-done.5 = bf16[64,32,128]{2,1,0:T(8,128)(2,1)S(1)} async-done(((bf16[64,32,128]{2,1,0:T(8,128)(2,1)}), bf16[64,32,128]{2,1,0:T(8,128)(2,1)S(1)}, u32[]{:S(2)}, u32[]{:S(2)}) %all-to-all-start.5) | async-done | bytes 524320 | tf_op jit(solution)/shard_map/all_to_all | solution.py:59
  (61 shorter events, 14.3 us)
Async XLA Ops:
  0.6 40.3 %copy-start.1 = (bf16[128,128]{1,0:T(8,128)(2,1)S(1)}, bf16[128,128]{1,0:T(8,128)(2,1)}, u32[]{:S(2)}) copy-start(bf16[128,128]{1,0:T(8,128)(2,1)} %param.9) | copy-start | bytes 98308
  45.9 6.9 %copy-start.5 = (bf16[128,1024]{1,0:T(8,128)(2,1)S(1)}, bf16[128,1024]{1,0:T(8,128)(2,1)}, u32[]{:S(2)}) copy-start(bf16[128,1024]{1,0:T(8,128)(2,1)} %param.11) | copy-start | bytes 786436
  45.9 7.0 %copy-start.7 = (f32[128,8]{0,1:T(8,128)S(1)}, f32[128,8]{0,1:T(8,128)}, u32[]{:S(2)}) copy-start(f32[128,8]{0,1:T(8,128)} %param.10) | copy-start | bytes 12292
  45.9 7.1 %copy-start.6 = (bf16[128,1024]{1,0:T(8,128)(2,1)S(1)}, bf16[128,1024]{1,0:T(8,128)(2,1)}, u32[]{:S(2)}) copy-start(bf16[128,1024]{1,0:T(8,128)(2,1)} %param.7) | copy-start | bytes 786436
  45.9 103.3 %all-to-all-start.1 = ((bf16[128,64,128]{2,1,0:T(8,128)(2,1)}), bf16[128,64,128]{2,1,0:T(8,128)(2,1)S(1)}, u32[]{:S(2)}, u32[]{:S(2)}) async-start(bf16[128,64,128]{2,1,0:T(8,128)(2,1)} %pad_maximum_fusion), calls=%async_computation.1 | async-start | bytes 4194304 | tf_op jit(solution)/shard_map/all_to_all | solution.py:17
  53.5 96.1 %copy-start = (bf16[128,128]{1,0:T(8,128)(2,1)S(1)}, bf16[128,128]{1,0:T(8,128)(2,1)}, u32[]{:S(2)}) copy-start(bf16[128,128]{1,0:T(8,128)(2,1)} %param.8) | copy-start | bytes 98308
  154.4 1.4 copy-start.3
  157.5 1.4 copy-start.2
  160.5 106.9 %all-to-all-start.2 = ((bf16[128,64,128]{2,1,0:T(8,128)(2,1)}), bf16[128,64,128]{2,1,0:T(8,128)(2,1)S(1)}, u32[]{:S(2)}, u32[]{:S(2)}) async-start(bf16[128,64,128]{2,1,0:T(8,128)(2,1)} %pad_maximum_fusion.1), calls=%async_computation.2 | async-start | bytes 4194304 | tf_op jit(solution)/shard_map/all_to_all | solution.py:17
  269.5 20.7 %all-to-all-start.3 = ((bf16[4,128,1024]{1,2,0:T(8,128)(2,1)}), bf16[4,128,1024]{1,2,0:T(8,128)(2,1)}, u32[]{:S(2)}, u32[]{:S(2)}) async-start(bf16[4,128,1024]{1,2,0:T(8,128)(2,1)} %broadcast_in_dim.72), calls=%async_computation.3 | async-start | bytes 2097152 | tf_op jit(solution)/shard_map/all_to_all | solution.py:29
  298.3 41.8 %all-to-all-start.5 = ((bf16[64,32,128]{2,1,0:T(8,128)(2,1)}), bf16[64,32,128]{2,1,0:T(8,128)(2,1)S(1)}, u32[]{:S(2)}, u32[]{:S(2)}) async-start(bf16[64,32,128]{2,1,0:T(8,128)(2,1)} %reduce_sum.31), calls=%async_computation.5 | async-start | bytes 1048576 | tf_op jit(solution)/shard_map/all_to_all | solution.py:59
  307.1 1.7 copy-start.4
where the time goes:
time: 342 us; the launch traced here: 341 us
  waiting for transfers between devices  232 us (68%)
  blocking collectives  37.8 us (11%)
  starting transfers between devices  30.6 us (9%)
  local copies, waits for them, and re-layouts  16 us (5%)
  other arithmetic  13.6 us (4%)
  matrix products  9.44 us (3%)
    all_to_all x2, waiting for transfers between devices, side_by_side(): lax.all_to_all(both, axis, split_axis=split_dim, concat_axis=concat_dim,...  190 us
    all_to_all x1, blocking collectives, local(): lax.all_to_all(wanted.reshape(devices, 1), KV, split_axis=0, concat_axis=...  33.2 us
    all_to_all x1, waiting for transfers between devices, sum_in_two_steps(): lax.all_to_all(own.astype(jnp.bfloat16), far, 0, 0, tiled=True)  28.6 us
    all_to_all x2, starting transfers between devices, side_by_side(): lax.all_to_all(both, axis, split_axis=split_dim, concat_axis=concat_dim,...  17.3 us
    all_to_all x1, waiting for transfers between devices, from_everyone(): return lax.all_to_all(copies, axis, split_axis=0, concat_axis=0, tiled=True)  13.5 us
    all_to_all x1, starting transfers between devices, sum_in_two_steps(): lax.all_to_all(own.astype(jnp.bfloat16), far, 0, 0, tiled=True)  8.77 us
  transfers between devices with their start and end apart: 4, of which 4 were waited for; matrix products, arithmetic and copies ran while one was open for 3% of the time, Pallas kernels for 0%

commit v1 on v0

v1 whole, which is shorter than its diff:
```python
import jax
import jax.numpy as jnp
from jax import lax
from jax.sharding import Mesh
from jax.sharding import PartitionSpec as P

HD = 128
QB = 64
KB = 32
NSEL = 16
KV = ("z", "x", "c")
XC = ("x", "c")


def to_peers(parts, axis):
    return lax.all_to_all(parts, axis, split_axis=0, concat_axis=0, tiled=True)


def local(queries, keys, values, logsum, out_grad, normed_input, chosen):
    nz = lax.axis_size("z")
    nq = lax.axis_size(XC)
    tp = lax.axis_size("tp")
    here = lax.axis_index(KV)
    tok = keys.shape[0]
    kblocks = tok // KB
    qblocks = tok // QB
    group = queries.shape[1] // HD
    span = NSEL * KB
    scale = HD ** (-0.5)
    peers = nq * nz
    entries = qblocks * NSEL

    owner = chosen // kblocks
    within = chosen % kblocks
    remote = owner != here
    place = (owner % nq) * nz + owner // nq
    named = (place[:, :, None] == jnp.arange(peers, dtype=jnp.int32)) & remote[:, :, None]
    wanted = jnp.max(jnp.where(named, within[:, :, None] + 1, 0), axis=(0, 1))
    asked = to_peers(wanted.reshape(nq, nz), XC)
    slot = jnp.where(remote, place, peers + within).reshape(entries)
    taken = jnp.arange(nz, dtype=jnp.int32)[None, :] * kblocks + jnp.maximum(asked - 1, 0)

    def fetch(rows):
        column = lax.all_gather(rows, "z", axis=0, tiled=True).reshape(nz * kblocks, KB, HD)
        got = to_peers(column[taken.reshape(-1)].reshape(nq, nz * KB, HD), XC)
        pool = jnp.concatenate([got.reshape(peers, KB, HD), rows.reshape(kblocks, KB, HD)], axis=0)
        return pool[slot].reshape(qblocks, span, HD)

    onehot = (slot[:, None] == jnp.arange(peers + kblocks, dtype=jnp.int32)[None, :]).astype(jnp.float32)
    home = ((asked - 1)[:, :, None] == jnp.arange(kblocks, dtype=jnp.int32)).astype(jnp.bfloat16)

    def give_back(part):
        total = jnp.dot(
            onehot.T,
            part.reshape(entries, KB * HD),
            precision=lax.Precision.HIGHEST,
            preferred_element_type=jnp.float32,
        )
        own = total[peers:].reshape(tok, HD)
        sent = total[:peers].astype(jnp.bfloat16).reshape(nq, nz * KB, HD)
        came = to_peers(sent, XC).reshape(nq, nz, KB * HD)
        dense = jnp.einsum("qzk,qze->zke", home, came, preferred_element_type=jnp.float32)
        dense = dense.astype(jnp.bfloat16).reshape(nz, tok, HD)
        sums = to_peers(dense, "z")
        return own + jnp.sum(sums.astype(jnp.float32), axis=0)

    feats = normed_input.shape[1]
    rows_out = feats * tp // peers
    mine = nz // tp
    split = normed_input.reshape(tok, mine, nq, rows_out).transpose(2, 0, 1, 3)
    split = to_peers(split.reshape(nq, tok, mine * rows_out), XC).reshape(nq * tok, mine * rows_out)
    planes = [split]
    for k in range(1, tp):
        planes.append(lax.ppermute(split, "tp", [(i, (i + k) % tp) for i in range(tp)]))

    sel_keys = fetch(keys)
    query_rows = queries.reshape(qblocks, QB, group, HD)
    dout = out_grad.reshape(qblocks, QB, group, HD)
    lse = logsum.reshape(qblocks, QB, group)
    scores = (
        jnp.einsum("bqgd,bjd->bqgj", query_rows, sel_keys, preferred_element_type=jnp.float32)
        * scale
    )
    qpos = here * tok + jnp.arange(tok, dtype=jnp.int32).reshape(qblocks, QB)
    kpos = (chosen[:, :, None] * KB + jnp.arange(KB, dtype=jnp.int32)[None, None, :]).reshape(
        qblocks, span
    )
    valid = (kpos[:, None, :] <= qpos[:, :, None])[:, :, None, :]
    prob = jnp.where(valid, jnp.exp(scores - lse[..., None]), 0.0)
    prob_low = prob.astype(jnp.bfloat16)
    value_grad = give_back(
        jnp.einsum("bqgj,bqgd->bjd", prob_low, dout, preferred_element_type=jnp.float32)
    )

    value_low = value_grad.astype(jnp.bfloat16)
    all_low = lax.all_gather(value_low, XC, axis=0, tiled=True)
    me = lax.axis_index("tp")
    products = jnp.stack(
        [jnp.einsum("tf,tc->fc", p, all_low, preferred_element_type=jnp.float32) for p in planes]
    )
    order = (me - jnp.arange(tp)) % tp
    products = products[order].astype(jnp.bfloat16)
    weight_parts = to_peers(products.reshape(nz, rows_out, HD), "z")
    weight_grad = jnp.sum(weight_parts.astype(jnp.float32), axis=0)

    sel_values = fetch(values)
    dprob = jnp.einsum("bqgd,bjd->bqgj", dout, sel_values, preferred_element_type=jnp.float32)
    delta = jnp.sum(prob * dprob, axis=-1, keepdims=True)
    dscore = (prob * (dprob - delta)).astype(jnp.bfloat16)
    key_grad = give_back(
        jnp.einsum("bqgj,bqgd->bjd", dscore, query_rows, preferred_element_type=jnp.float32) * scale
    )
    query_grad = (
        jnp.einsum("bqgj,bjd->bqgd", dscore, sel_keys, preferred_element_type=jnp.float32) * scale
    )
    return (query_grad.reshape(tok, group * HD), key_grad, value_grad, weight_grad)


def solution(mesh):
    kv, tp = mesh.shape["kv"], mesh.shape["tp"]
    split = Mesh(mesh.devices.reshape(kv // 8, 4, 2, tp), ("z", "x", "c", "tp"))
    cut = P(KV, "tp")
    return jax.shard_map(
        local,
        mesh=split,
        in_specs=(cut, cut, cut, cut, cut, cut, P(KV, None)),
        out_specs=(cut, cut, cut, cut),
        check_vma=False,
    )
```

time: 342 us -> 262 us (0.77)
  the two profiles are of different devices: /device:TPU:2 before, /device:TPU:8 now
where the time goes in v1:
time: 262 us; the launch traced here: 260 us
  blocking collectives  80.3 us (31%)
  starting transfers between devices  63.8 us (24%)
  waiting for transfers between devices  62.8 us (24%)
  local copies, waits for them, and re-layouts  28.5 us (11%)
  matrix products  16.1 us (6%)
  other arithmetic  7.73 us (3%)
    all_gather x2, blocking collectives, fetch(): lax.all_gather(rows, 'z', axis=0, tiled=True).reshape(nz * kblocks, KB, HD)  67.4 us
    all_to_all x9, waiting for transfers between devices, to_peers(): return lax.all_to_all(parts, axis, split_axis=0, concat_axis=0, tiled=True)  62.8 us
    all_to_all x9, starting transfers between devices, to_peers(): return lax.all_to_all(parts, axis, split_axis=0, concat_axis=0, tiled=True)  53.1 us
    all_gather x1, blocking collectives, local(): all_low = lax.all_gather(value_low, XC, axis=0, tiled=True)  12.8 us
    ppermute x3, starting transfers between devices, local(): lax.ppermute(split, 'tp', [(i, (i + k) % tp) for i in range(tp)])  10.7 us
  transfers between devices with their start and end apart: 12, of which 5 were waited for; matrix products, arithmetic and copies ran while one was open for 17% of the time, Pallas kernels for 0%

profile of v1, /device:TPU:8, one launch (start us, length us, event | category | flops | bytes accessed | tf_op | source)
XLA Modules:
  0.0 260.3 jit_solution(17794559753755833579)
XLA Ops:
  2.1 4.3 %all-to-all-start = ((s32[8,1,16]{2,1,0:T(1,128)}), s32[8,1,16]{2,1,0:T(1,128)S(1)}, u32[]{:S(2)}, u32[]{:S(2)}) async-start(s32[8,1,16]{2,1,0:T(1,128)} %bitcast.1), calls=%async_computation | async-start | bytes 8192 | tf_op jit(solution)/shard_map/all_to_all | solution.py:16
  6.4 38.6 %all_gather.9 = bf16[2048,128]{1,0:T(8,128)(2,1)S(1)} all-gather(bf16[128,128]{1,0:T(8,128)(2,1)} %param.8), channel_id=1, replica_groups=mesh['z'=16,'x'=4,'c'=2,'tp'=4] {'z'}, dimensions={0}, use_global_device_ids=true | all-gather | bytes 557056 | tf_op jit(solution)/shard_map/all_gather | solution.py:44
  47.5 4.9 %all-to-all-start.1 = ((bf16[8,512,128]{2,1,0:T(8,128)(2,1)}), bf16[8,512,128]{2,1,0:T(8,128)(2,1)S(1)}, u32[]{:S(2)}, u32[]{:S(2)}) async-start(bf16[8,512,128]{2,1,0:T(8,128)(2,1)} %bitcast.4), calls=%async_computation.1 | async-start | bytes 2097152 | tf_op jit(solution)/shard_map/all_to_all | solution.py:16
  54.4 28.9 %all_gather.10 = bf16[2048,128]{1,0:T(8,128)(2,1)S(1)} all-gather(bf16[128,128]{1,0:T(8,128)(2,1)S(1)} %copy-done.10), channel_id=1, replica_groups=mesh['z'=16,'x'=4,'c'=2,'tp'=4] {'z'}, dimensions={0}, use_global_device_ids=true | all-gather | bytes 557056 | tf_op jit(solution)/shard_map/all_gather | solution.py:44
  85.0 5.5 %all-to-all-start.2 = ((bf16[8,512,128]{2,1,0:T(8,128)(2,1)}), bf16[8,512,128]{2,1,0:T(8,128)(2,1)S(1)}, u32[]{:S(2)}, u32[]{:S(2)}) async-start(bf16[8,512,128]{2,1,0:T(8,128)(2,1)} %bitcast.13), calls=%async_computation.2 | async-start | bytes 2097152 | tf_op jit(solution)/shard_map/all_to_all | solution.py:16
  93.5 12.8 %all-to-all-done.2 = bf16[8,512,128]{2,1,0:T(8,128)(2,1)S(1)} async-done(((bf16[8,512,128]{2,1,0:T(8,128)(2,1)}), bf16[8,512,128]{2,1,0:T(8,128)(2,1)S(1)}, u32[]{:S(2)}, u32[]{:S(2)}) %all-to-all-start.2) | async-done | bytes 1048608 | tf_op jit(solution)/shard_map/all_to_all | solution.py:16
  106.4 4.1 %all-to-all-start.7 = ((bf16[8,128,128]{1,2,0:T(8,128)(2,1)}), bf16[8,128,128]{1,2,0:T(8,128)(2,1)}, u32[]{:S(2)}, u32[]{:S(2)}) async-start(bf16[8,128,128]{1,2,0:T(8,128)(2,1)} %bitcast.27), calls=%async_computation.7 | async-start | bytes 524288 | tf_op jit(solution)/shard_map/all_to_all | solution.py:16
  118.3 4.7 %all-to-all-start.5 = ((bf16[8,512,128]{2,1,0:T(8,128)(2,1)}), bf16[8,512,128]{2,1,0:T(8,128)(2,1)S(1)}, u32[]{:S(2)}, u32[]{:S(2)}) async-start(bf16[8,512,128]{2,1,0:T(8,128)(2,1)} %reshape.289), calls=%async_computation.5 | async-start | bytes 2097152 | tf_op jit(solution)/shard_map/all_to_all | solution.py:16
  127.3 2.2 fusion.14
  130.8 2.4 reshape.284
  133.2 5.8 %all-to-all-done.5 = bf16[8,512,128]{2,1,0:T(8,128)(2,1)S(1)} async-done(((bf16[8,512,128]{2,1,0:T(8,128)(2,1)}), bf16[8,512,128]{2,1,0:T(8,128)(2,1)S(1)}, u32[]{:S(2)}, u32[]{:S(2)}) %all-to-all-start.5) | async-done | bytes 1048608 | tf_op jit(solution)/shard_map/all_to_all | solution.py:16
  139.0 4.2 %all-to-all-start.3 = ((bf16[8,512,128]{2,1,0:T(8,128)(2,1)}), bf16[8,512,128]{2,1,0:T(8,128)(2,1)}, u32[]{:S(2)}, u32[]{:S(2)}) async-start(bf16[8,512,128]{2,1,0:T(8,128)(2,1)} %reshape.284), calls=%async_computation.3 | async-start | bytes 2097152 | tf_op jit(solution)/shard_map/all_to_all | solution.py:16
  144.6 2.5 convolution_convert_fusion
  148.5 10.7 %all-to-all-done.3 = bf16[8,512,128]{2,1,0:T(8,128)(2,1)} async-done(((bf16[8,512,128]{2,1,0:T(8,128)(2,1)}), bf16[8,512,128]{2,1,0:T(8,128)(2,1)}, u32[]{:S(2)}, u32[]{:S(2)}) %all-to-all-start.3) | async-done | bytes 1048608 | tf_op jit(solution)/shard_map/all_to_all | solution.py:16
  159.2 7.0 %all-to-all-start.6 = ((bf16[16,128,128]{2,1,0:T(8,128)(2,1)}), bf16[16,128,128]{2,1,0:T(8,128)(2,1)}, u32[]{:S(2)}, u32[]{:S(2)}) async-start(bf16[16,128,128]{2,1,0:T(8,128)(2,1)} %reshape.291), calls=%async_computation.6 | async-start | bytes 1048576 | tf_op jit(solution)/shard_map/all_to_all | solution.py:16
  169.8 2.4 reshape.286
  172.2 22.7 %all-to-all-done.6 = bf16[16,128,128]{2,1,0:T(8,128)(2,1)} async-done(((bf16[16,128,128]{2,1,0:T(8,128)(2,1)}), bf16[16,128,128]{2,1,0:T(8,128)(2,1)}, u32[]{:S(2)}, u32[]{:S(2)}) %all-to-all-start.6) | async-done | bytes 524320 | tf_op jit(solution)/shard_map/all_to_all | solution.py:16
  194.9 6.4 %all-to-all-start.4 = ((bf16[16,128,128]{2,1,0:T(8,128)(2,1)}), bf16[16,128,128]{2,1,0:T(8,128)(2,1)S(1)}, u32[]{:S(2)}, u32[]{:S(2)}) async-start(bf16[16,128,128]{2,1,0:T(8,128)(2,1)} %reshape.286), calls=%async_computation.4 | async-start | bytes 1048576 | tf_op jit(solution)/shard_map/all_to_all | solution.py:16
  202.5 2.4 collective-permute-start.2
  204.9 4.5 %collective-permute-start.1 = (bf16[1024,128]{1,0:T(8,128)(2,1)S(1)}, bf16[1024,128]{1,0:T(8,128)(2,1)}, u32[]{:S(2)}, u32[]{:S(2)}) collective-permute-start(bf16[1024,128]{1,0:T(8,128)(2,1)S(1)} %bitcast.110), channel_id=1, source_target_pairs={{0,2},{1,3},{2,0},{3,1},{4,6},{5,7},{6,4},{7,5},{8,10},{9,11},{10,... | collective-permute-start | bytes 786440 | tf_op jit(solution)/shard_map/ppermute | solution.py:74
  209.4 3.8 %collective-permute-start = (bf16[1024,128]{1,0:T(8,128)(2,1)S(1)}, bf16[1024,128]{1,0:T(8,128)(2,1)}, u32[]{:S(2)}, u32[]{:S(2)}) collective-permute-start(bf16[1024,128]{1,0:T(8,128)(2,1)S(1)} %bitcast.111), channel_id=1, source_target_pairs={{0,1},{1,2},{2,3},{3,0},{4,5},{5,6},{6,7},{7,4},{8,9},{9,10},{10,1... | collective-permute-start | bytes 786440 | tf_op jit(solution)/shard_map/ppermute | solution.py:74
  215.0 12.8 %all_gather.11 = bf16[1024,128]{1,0:T(8,128)(2,1)S(1)} all-gather(bf16[128,128]{1,0:T(8,128)(2,1)S(1)} %get-tuple-element.4), channel_id=1, replica_groups=mesh['z'=16,'x'=4,'c'=2,'tp'=4] {'x','c'}, dimensions={0}, use_global_device_ids=true | all-gather | bytes 294912 | tf_op jit(solution)/shard_map/all_gather | solution.py:96
  233.2 12.0 %all-to-all-start.8 = ((bf16[16,32,128]{2,1,0:T(8,128)(2,1)}), bf16[16,32,128]{2,1,0:T(8,128)(2,1)S(1)}, u32[]{:S(2)}, u32[]{:S(2)}) async-start(bf16[16,32,128]{2,1,0:T(8,128)(2,1)} %bitcast.38), calls=%async_computation.8 | async-start | bytes 262144 | tf_op jit(solution)/shard_map/all_to_all | solution.py:16
  248.9 10.7 %all-to-all-done.8 = bf16[16,32,128]{2,1,0:T(8,128)(2,1)S(1)} async-done(((bf16[16,32,128]{2,1,0:T(8,128)(2,1)}), bf16[16,32,128]{2,1,0:T(8,128)(2,1)S(1)}, u32[]{:S(2)}, u32[]{:S(2)}) %all-to-all-start.8) | async-done | bytes 131104 | tf_op jit(solution)/shard_map/all_to_all | solution.py:16
  (107 shorter events, 42.9 us)
Async XLA Ops:
  2.1 43.0 %all-to-all-start = ((s32[8,1,16]{2,1,0:T(1,128)}), s32[8,1,16]{2,1,0:T(1,128)S(1)}, u32[]{:S(2)}, u32[]{:S(2)}) async-start(s32[8,1,16]{2,1,0:T(1,128)} %bitcast.1), calls=%async_computation | async-start | bytes 8192 | tf_op jit(solution)/shard_map/all_to_all | solution.py:16
  45.8 7.3 %copy-start.6 = (bf16[128,1024]{1,0:T(8,128)(2,1)S(1)}, bf16[128,1024]{1,0:T(8,128)(2,1)}, u32[]{:S(2)}) copy-start(bf16[128,1024]{1,0:T(8,128)(2,1)} %param.11) | copy-start | bytes 786436
  45.8 7.3 %copy-start.12 = (f32[128,8]{0,1:T(8,128)S(1)}, f32[128,8]{0,1:T(8,128)}, u32[]{:S(2)}) copy-start(f32[128,8]{0,1:T(8,128)} %param.10) | copy-start | bytes 12292
  45.8 7.4 %copy-start.7 = (bf16[128,1024]{1,0:T(8,128)(2,1)S(1)}, bf16[128,1024]{1,0:T(8,128)(2,1)}, u32[]{:S(2)}) copy-start(bf16[128,1024]{1,0:T(8,128)(2,1)} %param.7) | copy-start | bytes 786436
  47.5 6.0 %copy-start.8 = (bf16[128,1024]{1,0:T(8,128)(2,1)S(1)}, bf16[128,1024]{1,0:T(8,128)(2,1)}, u32[]{:S(2)}) copy-start(bf16[128,1024]{1,0:T(8,128)(2,1)} %param.12) | copy-start | bytes 786436
  47.5 6.9 %copy-start.10 = (bf16[128,128]{1,0:T(8,128)(2,1)S(1)}, bf16[128,128]{1,0:T(8,128)(2,1)}, u32[]{:S(2)}) copy-start(bf16[128,128]{1,0:T(8,128)(2,1)} %param.9) | copy-start | bytes 98308
  47.5 37.4 %all-to-all-start.1 = ((bf16[8,512,128]{2,1,0:T(8,128)(2,1)}), bf16[8,512,128]{2,1,0:T(8,128)(2,1)S(1)}, u32[]{:S(2)}, u32[]{:S(2)}) async-start(bf16[8,512,128]{2,1,0:T(8,128)(2,1)} %bitcast.4), calls=%async_computation.1 | async-start | bytes 2097152 | tf_op jit(solution)/shard_map/all_to_all | solution.py:16
  83.3 7.3 %copy-start.9 = (bf16[128,128]{1,0:T(8,128)(2,1)S(1)}, bf16[128,128]{1,0:T(8,128)(2,1)}, u32[]{:S(2)}) copy-start(bf16[128,128]{1,0:T(8,128)(2,1)} %param.8) | copy-start | bytes 98308
  85.0 21.4 %all-to-all-start.2 = ((bf16[8,512,128]{2,1,0:T(8,128)(2,1)}), bf16[8,512,128]{2,1,0:T(8,128)(2,1)S(1)}, u32[]{:S(2)}, u32[]{:S(2)}) async-start(bf16[8,512,128]{2,1,0:T(8,128)(2,1)} %bitcast.13), calls=%async_computation.2 | async-start | bytes 2097152 | tf_op jit(solution)/shard_map/all_to_all | solution.py:16
  93.5 18.0 %copy-start.4 = (bf16[32,32,128]{2,1,0:T(8,128)(2,1)}, bf16[32,32,128]{2,1,0:T(8,128)(2,1)S(1)}, u32[]{:S(2)}) copy-start(bf16[32,32,128]{2,1,0:T(8,128)(2,1)S(1)} %gather_fusion.1) | copy-start | bytes 786436
  106.4 12.0 %all-to-all-start.7 = ((bf16[8,128,128]{1,2,0:T(8,128)(2,1)}), bf16[8,128,128]{1,2,0:T(8,128)(2,1)}, u32[]{:S(2)}, u32[]{:S(2)}) async-start(bf16[8,128,128]{1,2,0:T(8,128)(2,1)} %bitcast.27), calls=%async_computation.7 | async-start | bytes 524288 | tf_op jit(solution)/shard_map/all_to_all | solution.py:16
  118.3 20.6 %all-to-all-start.5 = ((bf16[8,512,128]{2,1,0:T(8,128)(2,1)}), bf16[8,512,128]{2,1,0:T(8,128)(2,1)S(1)}, u32[]{:S(2)}, u32[]{:S(2)}) async-start(bf16[8,512,128]{2,1,0:T(8,128)(2,1)} %reshape.289), calls=%async_computation.5 | async-start | bytes 2097152 | tf_op jit(solution)/shard_map/all_to_all | solution.py:16
  129.5 115.7 %copy-start.1 = (f32[132,4096]{1,0:T(8,128)}, f32[132,4096]{1,0:T(8,128)S(1)}, u32[]{:S(2)}) copy-start(f32[132,4096]{1,0:T(8,128)S(1)} %fusion.14) | copy-start | bytes 6488068
  130.8 12.4 %copy-start.11 = (s32[8,16]{1,0:T(8,128)S(1)}, s32[8,16]{1,0:T(8,128)}, u32[]{:S(2)}) copy-start(s32[8,16]{1,0:T(8,128)} %get-tuple-element.9) | copy-start | bytes 1540
  139.0 20.2 %all-to-all-start.3 = ((bf16[8,512,128]{2,1,0:T(8,128)(2,1)}), bf16[8,512,128]{2,1,0:T(8,128)(2,1)}, u32[]{:S(2)}, u32[]{:S(2)}) async-start(bf16[8,512,128]{2,1,0:T(8,128)(2,1)} %reshape.284), calls=%async_computation.3 | async-start | bytes 2097152 | tf_op jit(solution)/shard_map/all_to_all | solution.py:16
  159.2 35.8 %all-to-all-start.6 = ((bf16[16,128,128]{2,1,0:T(8,128)(2,1)}), bf16[16,128,128]{2,1,0:T(8,128)(2,1)}, u32[]{:S(2)}, u32[]{:S(2)}) async-start(bf16[16,128,128]{2,1,0:T(8,128)(2,1)} %reshape.291), calls=%async_computation.6 | async-start | bytes 1048576 | tf_op jit(solution)/shard_map/all_to_all | solution.py:16
  167.7 45.5 %slice-start.1 = ((f32[132,4096]{1,0:T(8,128)}), f32[4,4096]{1,0:T(4,128)S(1)}, s32[]{:S(2)}) async-start(f32[132,4096]{1,0:T(8,128)} %copy-done.2), calls=%async_computation.10 | async-start | bytes 131072 | tf_op jit(solution)/shard_map/slice | solution.py:59
  194.9 38.3 %all-to-all-start.4 = ((bf16[16,128,128]{2,1,0:T(8,128)(2,1)}), bf16[16,128,128]{2,1,0:T(8,128)(2,1)S(1)}, u32[]{:S(2)}, u32[]{:S(2)}) async-start(bf16[16,128,128]{2,1,0:T(8,128)(2,1)} %reshape.286), calls=%async_computation.4 | async-start | bytes 1048576 | tf_op jit(solution)/shard_map/all_to_all | solution.py:16
  202.5 25.6 %collective-permute-start.2 = (bf16[1024,128]{1,0:T(8,128)(2,1)S(1)}, bf16[1024,128]{1,0:T(8,128)(2,1)}, u32[]{:S(2)}, u32[]{:S(2)}) collective-permute-start(bf16[1024,128]{1,0:T(8,128)(2,1)S(1)} %bitcast.109), channel_id=1, source_target_pairs={{0,3},{1,0},{2,1},{3,2},{4,7},{5,4},{6,5},{7,6},{8,11},{9,8},{10,9... | collective-permute-start | bytes 786440 | tf_op jit(solution)/shard_map/ppermute | solution.py:74
  204.9 24.5 %collective-permute-start.1 = (bf16[1024,128]{1,0:T(8,128)(2,1)S(1)}, bf16[1024,128]{1,0:T(8,128)(2,1)}, u32[]{:S(2)}, u32[]{:S(2)}) collective-permute-start(bf16[1024,128]{1,0:T(8,128)(2,1)S(1)} %bitcast.110), channel_id=1, source_target_pairs={{0,2},{1,3},{2,0},{3,1},{4,6},{5,7},{6,4},{7,5},{8,10},{9,11},{10,... | collective-permute-start | bytes 786440 | tf_op jit(solution)/shard_map/ppermute | solution.py:74
  209.4 21.2 %collective-permute-start = (bf16[1024,128]{1,0:T(8,128)(2,1)S(1)}, bf16[1024,128]{1,0:T(8,128)(2,1)}, u32[]{:S(2)}, u32[]{:S(2)}) collective-permute-start(bf16[1024,128]{1,0:T(8,128)(2,1)S(1)} %bitcast.111), channel_id=1, source_target_pairs={{0,1},{1,2},{2,3},{3,0},{4,5},{5,6},{6,7},{7,4},{8,9},{9,10},{10,1... | collective-permute-start | bytes 786440 | tf_op jit(solution)/shard_map/ppermute | solution.py:74
  214.4 30.9 %copy-start.5 = (bf16[32,32,128]{2,1,0:T(8,128)(2,1)S(1)}, bf16[32,32,128]{2,1,0:T(8,128)(2,1)}, u32[]{:S(2)}) copy-start(bf16[32,32,128]{2,1,0:T(8,128)(2,1)} %copy-done.4) | copy-start | bytes 786436
  233.2 26.4 %all-to-all-start.8 = ((bf16[16,32,128]{2,1,0:T(8,128)(2,1)}), bf16[16,32,128]{2,1,0:T(8,128)(2,1)S(1)}, u32[]{:S(2)}, u32[]{:S(2)}) async-start(bf16[16,32,128]{2,1,0:T(8,128)(2,1)} %bitcast.38), calls=%async_computation.8 | async-start | bytes 262144 | tf_op jit(solution)/shard_map/all_to_all | solution.py:16
  245.3 2.9 %slice-start = ((f32[132,4096]{1,0:T(8,128)}), f32[4,4096]{1,0:T(4,128)S(1)}, s32[]{:S(2)}) async-start(f32[132,4096]{1,0:T(8,128)} %copy-done.1), calls=%async_computation.9 | async-start | bytes 131072 | tf_op jit(solution)/shard_map/slice | solution.py:59
  (4 other events, 5.7 us)

commit v2 on v1

v2 whole, which is shorter than its diff:
```python
import functools

import jax
import jax.numpy as jnp
from jax import lax
from jax.experimental import pallas as pl
from jax.experimental.pallas import tpu as pltpu
from jax.sharding import Mesh
from jax.sharding import PartitionSpec as P

HD = 128
QB = 64
KB = 32
NSEL = 16
KV = ("z", "x", "c")
XC = ("x", "c")
SUB = 8
SCALE = HD ** (-0.5)
F32 = jnp.float32
BF16 = jnp.bfloat16
NT = (((1,), (1,)), ((), ()))
TN = (((0,), (0,)), ((), ()))


def to_peers(parts, axis):
    return lax.all_to_all(parts, axis, split_axis=0, concat_axis=0, tiled=True)


def smem():
    return pl.BlockSpec(memory_space=pltpu.SMEM)


def vmem():
    return pl.BlockSpec(memory_space=pltpu.VMEM)


def call(body, outs, ins, scratch=()):
    return pl.pallas_call(
        body,
        out_shape=outs,
        in_specs=[smem() if i == "s" else vmem() for i in ins],
        out_specs=jax.tree.map(lambda _: vmem(), outs),
        scratch_shapes=list(scratch),
        compiler_params=pltpu.CompilerParams(vmem_limit_bytes=40 * 1024 * 1024),
    )


def pick(nq, nz, asked, column, out):
    per = column.shape[0] // nz
    for q in range(nq):
        for z in range(nz):
            block = jnp.maximum(asked[q * nz + z] - 1, 0)
            out[q * nz + z] = column[z * per + block]


def by_feature(nq, rows, features, wanted, out):
    tok, cols = features.shape
    for i in range(cols // HD):
        tile = features[:, i * HD : (i + 1) * HD].T
        for j in range(HD // rows):
            piece = i * (HD // rows) + j
            out[piece % nq, (piece // nq) * rows : (piece // nq + 1) * rows] = tile[
                j * rows : (j + 1) * rows
            ]
    for q in range(nq):
        out[q, cols // nq :] = jnp.broadcast_to(wanted[q : q + 1], (SUB, tok))


def slots_of(chosen, here, b, nq, nz, kblocks):
    slots = []
    for e in range(NSEL):
        c = chosen[b * NSEL + e]
        owner = c // kblocks
        place = (owner % nq) * nz + owner // nq
        slots.append((c, owner != here, place, c % kblocks))
    return slots


def select(slots, got, own, out):
    for e, (_, remote, place, within) in enumerate(slots):
        far = got[jnp.where(remote, place, 0)]
        near = own[within]
        out[e * KB : (e + 1) * KB] = jnp.where(remote, far, near)


def heads_of(ref, b, p):
    rows = slice(b * QB, (b + 1) * QB)
    return jnp.concatenate(
        [ref[rows, (2 * p + i) * HD : (2 * p + i + 1) * HD] for i in range(2)], axis=0
    )


def set_positions(slots, kpos):
    rows = lax.broadcasted_iota(jnp.int32, (KB, HD), 0)
    lanes = lax.broadcasted_iota(jnp.int32, (KB, HD), 1) % QB
    for e, (c, _, _, _) in enumerate(slots):
        kpos[e * KB : (e + 1) * KB] = c * KB + rows - lanes


def prob_of(sel, pair, lse, kpos, start, b, p, pairs):
    scores = lax.dot_general(sel[...], pair, NT, preferred_element_type=F32) * SCALE
    at = b * pairs + p
    return jnp.where(kpos[...] <= start, jnp.exp(scores - lse[at : at + 1, :]), 0.0)


def scatter(slots, parts, total, send, own_sum, peers, kblocks):
    def put(slot):
        _, remote, place, within = slot
        return jnp.where(remote, place, peers + within)

    zero = jnp.zeros((KB, HD), F32)
    for k in range(kblocks):
        total[peers + k] = zero
    for slot in slots[1]:
        total[put(slot)] = zero
    for b, part in enumerate(parts):
        for e, slot in enumerate(slots[b]):
            piece = part[e * KB : (e + 1) * KB]
            at = put(slot)
            total[at] = total[at] + piece if b else piece
    for b in range(len(parts)):
        for _, remote, place, _ in slots[b]:

            @pl.when(remote)
            def _(place=place):
                send[place] = total[place].astype(BF16)

    for k in range(kblocks):
        own_sum[k] = total[peers + k]


def value_terms(nq, nz, chosen, here, queries, dout, lse, got_k, own_k, send, own_sum, sel, kpos, low, rows, total, part):
    peers, kblocks = nq * nz, own_k.shape[0]
    qblocks, pairs = queries.shape[0] // QB, queries.shape[1] // HD // 2
    slots = [slots_of(chosen, here[0], b, nq, nz, kblocks) for b in range(qblocks)]
    for b in range(qblocks):
        select(slots[b], got_k, own_k, sel)
        set_positions(slots[b], kpos)
        start = here[0] * queries.shape[0] + b * QB
        for p in range(pairs):
            pair = heads_of(queries, b, p)
            prob = prob_of(sel, pair, lse, kpos, start, b, p, pairs)
            low[:, p * HD : (p + 1) * HD] = prob.astype(BF16)
            rows[p * HD : (p + 1) * HD] = heads_of(dout, b, p)
        part[b] = jnp.dot(low[...], rows[...], preferred_element_type=F32)
    scatter(slots, [part.at[b] for b in range(qblocks)], total, send, own_sum, peers, kblocks)


def key_terms(nq, nz, chosen, here, queries, dout, lse, got_k, own_k, got_v, own_v, send, own_sum, low, sel, sel_v, kpos, rows, total, part):
    peers, kblocks = nq * nz, own_k.shape[0]
    qblocks, pairs = queries.shape[0] // QB, queries.shape[1] // HD // 2
    slots = [slots_of(chosen, here[0], b, nq, nz, kblocks) for b in range(qblocks)]
    for b in range(qblocks):
        select(slots[b], got_k, own_k, sel.at[b])
        select(slots[b], got_v, own_v, sel_v)
        set_positions(slots[b], kpos)
        start = here[0] * queries.shape[0] + b * QB
        for p in range(pairs):
            pair = heads_of(queries, b, p)
            prob = prob_of(sel.at[b], pair, lse, kpos, start, b, p, pairs)
            dprob = lax.dot_general(sel_v[...], heads_of(dout, b, p), NT, preferred_element_type=F32)
            delta = jnp.sum(prob * dprob, axis=0, keepdims=True)
            low[b, :, p * HD : (p + 1) * HD] = (prob * (dprob - delta)).astype(BF16)
            rows[p * HD : (p + 1) * HD] = pair
        part[b] = jnp.dot(low[b], rows[...], preferred_element_type=F32) * SCALE
    scatter(slots, [part.at[b] for b in range(qblocks)], total, send, own_sum, peers, kblocks)


def query_terms(low, sel, out):
    for b in range(low.shape[0]):
        for p in range(low.shape[2] // HD):
            got = lax.dot_general(
                low[b, :, p * HD : (p + 1) * HD], sel[b], TN, preferred_element_type=F32
            )
            for i in range(2):
                out[b * QB : (b + 1) * QB, (2 * p + i) * HD : (2 * p + i + 1) * HD] = (
                    got[i * QB : (i + 1) * QB] * SCALE
                )


def gather_home(nq, nz, asked, came, dense, total):
    blocks = dense.shape[0]
    kblocks = blocks // nz
    total[...] = jnp.zeros_like(total)
    for q in range(nq):
        for z in range(nz):
            a = asked[q * nz + z]
            at = jnp.where(a > 0, z * kblocks + a - 1, blocks)
            total[at] = total[at] + came[q * nz + z].astype(F32)
    dense[...] = total[0:blocks].astype(BF16)


def weight_terms(rows_out, low, dense, *refs):
    *features, order, out = refs
    nq, nz, tok = low.shape[0], dense.shape[0], dense.shape[1]
    mine = nz // len(features)
    feats = mine * rows_out
    for k, block in enumerate(features):
        total = jnp.dot(block[0, 0:feats], low[0], preferred_element_type=F32)
        for q in range(1, nq):
            total = total + jnp.dot(block[q, 0:feats], low[q], preferred_element_type=F32)
        total = total.astype(BF16)
        for a in range(mine):
            out[order[k] * mine + a, tok:] = total[a * rows_out : (a + 1) * rows_out]
    out[:, 0:tok] = dense[...]


def local(queries, keys, values, logsum, out_grad, normed_input, chosen):
    nz = lax.axis_size("z")
    nq = lax.axis_size(XC)
    tp = lax.axis_size("tp")
    here = lax.axis_index(KV)
    tok, cols = queries.shape
    kblocks = tok // KB
    qblocks = tok // QB
    heads = cols // HD
    span = NSEL * KB
    peers = nq * nz
    shape = jax.ShapeDtypeStruct

    owner = chosen // kblocks
    place = (owner % nq) * nz + owner // nq
    named = (place[:, :, None] == jnp.arange(peers, dtype=jnp.int32)) & (owner != here)[:, :, None]
    wanted = jnp.max(jnp.where(named, (chosen % kblocks)[:, :, None] + 1, 0), axis=(0, 1))
    wanted = jnp.pad(wanted.reshape(nq, nz).astype(BF16), ((0, 0), (0, tok - nz)))

    rows_out = normed_input.shape[1] * tp // peers
    mine = nz // tp
    feats = mine * rows_out
    split = call(
        functools.partial(by_feature, nq, rows_out), shape((nq, feats + SUB, tok), BF16), "vv"
    )(normed_input, wanted)
    split = to_peers(split, XC)
    asked = split[:, feats, :nz].astype(jnp.int32).reshape(peers)
    planes = [split]
    for k in range(1, tp):
        planes.append(lax.ppermute(planes[0], "tp", [(i, (i + k) % tp) for i in range(tp)]))
    order = ((lax.axis_index("tp") - jnp.arange(tp)) % tp).astype(jnp.int32)
    names = chosen.reshape(qblocks * NSEL)
    me = here.reshape(1).astype(jnp.int32)

    def fetch(rows):
        column = lax.all_gather(rows, "z", axis=0, tiled=True).reshape(nz * kblocks, KB, HD)
        sent = call(functools.partial(pick, nq, nz), shape((peers, KB, HD), BF16), "sv")(
            asked, column
        )
        return to_peers(sent.reshape(nq, nz * KB, HD), XC).reshape(peers, KB, HD)

    got_k = fetch(keys)
    got_v = fetch(values)

    own_k = keys.reshape(kblocks, KB, HD)
    own_v = values.reshape(kblocks, KB, HD)
    lse = logsum.reshape(qblocks, QB, heads).transpose(0, 2, 1).reshape(qblocks * heads // 2, 2 * QB)
    terms = (shape((peers, KB, HD), BF16), shape((kblocks, KB, HD), F32))
    work = [
        pltpu.VMEM((span, HD), jnp.int32),
        pltpu.VMEM((heads * QB, HD), BF16),
        pltpu.VMEM((peers + kblocks, KB, HD), F32),
        pltpu.VMEM((qblocks, span, HD), F32),
    ]

    def home(sent):
        came = to_peers(sent.reshape(nq, nz * KB, HD), XC).reshape(peers, KB, HD)
        dense = call(
            functools.partial(gather_home, nq, nz),
            shape((nz * kblocks, KB, HD), BF16),
            "sv",
            [pltpu.VMEM((nz * kblocks + 1, KB, HD), F32)],
        )(asked, came)
        return dense.reshape(nz, tok, HD)

    sent_v, mine_v = call(
        functools.partial(value_terms, nq, nz),
        terms,
        "ssvvvvv",
        [pltpu.VMEM((span, HD), BF16), work[0], pltpu.VMEM((span, heads * QB), BF16), *work[1:]],
    )(names, me, queries, out_grad, lse, got_k, own_k)
    dense_v = home(sent_v)
    sums_v = to_peers(dense_v, "z")
    value_grad = mine_v.reshape(tok, HD) + jnp.sum(sums_v.astype(F32), axis=0)

    sent_k, mine_k, low, sel = call(
        functools.partial(key_terms, nq, nz),
        (*terms, shape((qblocks, span, heads * QB), BF16), shape((qblocks, span, HD), BF16)),
        "ssvvvvvvv",
        [pltpu.VMEM((span, HD), BF16), *work],
    )(names, me, queries, out_grad, lse, got_k, own_k, got_v, own_v)
    dense_k = home(sent_k)
    query_grad = call(query_terms, shape((tok, cols), F32), "vv")(low, sel)

    all_low = lax.all_gather(value_grad.astype(BF16), XC, axis=0)
    both = call(
        functools.partial(weight_terms, rows_out),
        shape((nz, tok + rows_out, HD), BF16),
        "v" * (2 + tp) + "s",
    )(all_low, dense_k, *planes, order)
    both = jnp.sum(to_peers(both, "z").astype(F32), axis=0)
    key_grad = mine_k.reshape(tok, HD) + both[:tok]
    return (query_grad, key_grad, value_grad, both[tok:])


def solution(mesh):
    kv, tp = mesh.shape["kv"], mesh.shape["tp"]
    split = Mesh(mesh.devices.reshape(kv // 8, 4, 2, tp), ("z", "x", "c", "tp"))
    cut = P(KV, "tp")

    return jax.shard_map(
        local,
        mesh=split,
        in_specs=(cut, cut, cut, cut, cut, cut, P(KV, None)),
        out_specs=(cut, cut, cut, cut),
        check_vma=False,
    )
```

time: 262 us -> 239 us (0.912)
  the two profiles are of different devices: /device:TPU:8 before, /device:TPU:24 now
where the time goes in v2:
time: 239 us; the launch traced here: 238 us
  waiting for transfers between devices  84.2 us (35%)
  blocking collectives  80.2 us (34%)
  starting transfers between devices  44 us (18%)
  Pallas kernels  15.9 us (7%)
  local copies, waits for them, and re-layouts  9.5 us (4%)
  other arithmetic  2.97 us (1%)
    all_to_all x7, waiting for transfers between devices, to_peers(): return lax.all_to_all(parts, axis, split_axis=0, concat_axis=0, tiled=True)  84.2 us
    all_gather x2, blocking collectives, fetch(): lax.all_gather(rows, 'z', axis=0, tiled=True).reshape(nz * kblocks, KB, HD)  67.3 us
    all_to_all x7, starting transfers between devices, to_peers(): return lax.all_to_all(parts, axis, split_axis=0, concat_axis=0, tiled=True)  35.5 us
    all_gather x1, blocking collectives, local(): all_low = lax.all_gather(value_grad.astype(BF16), XC, axis=0)  12.8 us
    ppermute x3, starting transfers between devices, local(): lax.ppermute(planes[0], 'tp', [(i, (i + k) % tp) for i in range(tp)])  8.55 us
    unnamed x46, local copies, waits for them, and re-layouts  8.49 us
  transfers between devices with their start and end apart: 10, of which 5 were waited for; matrix products, arithmetic and copies ran while one was open for 0% of the time, Pallas kernels for 5%

profile of v2, /device:TPU:24, one launch (start us, length us, event | category | flops | bytes accessed | tf_op | source)
XLA Modules:
  0.0 237.6 jit_solution(17782771456510168675)
XLA Ops:
  4.0 4.3 %all-to-all-start = ((bf16[8,136,128]{2,1,0:T(8,128)(2,1)}), bf16[8,136,128]{2,1,0:T(8,128)(2,1)S(1)}, u32[]{:S(2)}, u32[]{:S(2)}) async-start(bf16[8,136,128]{2,1,0:T(8,128)(2,1)} %shard_map.102), calls=%async_computation | async-start | bytes 557056 | tf_op jit(solution)/shard_map/all_to_all | solution.py:26
  8.3 38.4 %all_gather.10 = bf16[2048,128]{1,0:T(8,128)(2,1)S(1)} all-gather(bf16[128,128]{1,0:T(8,128)(2,1)S(1)} %copy-done.8), channel_id=1, replica_groups=mesh['z'=16,'x'=4,'c'=2,'tp'=4] {'z'}, dimensions={0}, use_global_device_ids=true | all-gather | bytes 557056 | tf_op jit(solution)/shard_map/all_gather | solution.py:243
  46.9 1.7 shard_map.103
  48.6 4.7 %all-to-all-start.1 = ((bf16[8,512,128]{2,1,0:T(8,128)(2,1)}), bf16[8,512,128]{2,1,0:T(8,128)(2,1)S(1)}, u32[]{:S(2)}, u32[]{:S(2)}) async-start(bf16[8,512,128]{2,1,0:T(8,128)(2,1)} %bitcast.3), calls=%async_computation.1 | async-start | bytes 2097152 | tf_op jit(solution)/shard_map/all_to_all | solution.py:26
  53.3 28.9 %all_gather.11 = bf16[2048,128]{1,0:T(8,128)(2,1)S(1)} all-gather(bf16[128,128]{1,0:T(8,128)(2,1)S(1)} %copy-done.12), channel_id=1, replica_groups=mesh['z'=16,'x'=4,'c'=2,'tp'=4] {'z'}, dimensions={0}, use_global_device_ids=true | all-gather | bytes 557056 | tf_op jit(solution)/shard_map/all_gather | solution.py:243
  82.2 1.7 shard_map.104
  84.0 5.1 %all-to-all-start.2 = ((bf16[8,512,128]{2,1,0:T(8,128)(2,1)}), bf16[8,512,128]{2,1,0:T(8,128)(2,1)S(1)}, u32[]{:S(2)}, u32[]{:S(2)}) async-start(bf16[8,512,128]{2,1,0:T(8,128)(2,1)} %bitcast.7), calls=%async_computation.2 | async-start | bytes 2097152 | tf_op jit(solution)/shard_map/all_to_all | solution.py:26
  89.4 2.1 shard_map.107
  92.5 12.6 %all-to-all-done.2 = bf16[8,512,128]{2,1,0:T(8,128)(2,1)S(1)} async-done(((bf16[8,512,128]{2,1,0:T(8,128)(2,1)}), bf16[8,512,128]{2,1,0:T(8,128)(2,1)S(1)}, u32[]{:S(2)}, u32[]{:S(2)}) %all-to-all-start.2) | async-done | bytes 1048608 | tf_op jit(solution)/shard_map/all_to_all | solution.py:26
  105.1 3.6 %all-to-all-start.3 = ((bf16[8,512,128]{2,1,0:T(8,128)(2,1)}), bf16[8,512,128]{2,1,0:T(8,128)(2,1)S(1)}, u32[]{:S(2)}, u32[]{:S(2)}) async-start(bf16[8,512,128]{2,1,0:T(8,128)(2,1)} %bitcast.39), calls=%async_computation.3 | async-start | bytes 2097152 | tf_op jit(solution)/shard_map/all_to_all | solution.py:26
  111.9 2.7 %shard_map.105 = (bf16[128,32,128]{2,1,0:T(8,128)(2,1)S(1)}, f32[4,32,128]{2,1,0:T(8,128)S(1)}, bf16[2,512,512]{2,1,0:T(8,128)(2,1)S(1)}, bf16[2,512,128]{2,1,0:T(8,128)(2,1)S(1)}) custom-call(s32[32]{0:T(128)S(1)} %copy-done.20, s32[1]{0:T(128)} %bitcast.here, bf16[128,1024]{1,0:T(8,128)(2,1)S(1)} %copy-done.5, bf16[128,1024]{1,0:T(8,128)(2,1)S(1)} %copy-done.7, ...), custom_call_target="tpu_custom_call" | custom-call | tf_op jit(solution)/shard_map/pallas_call | solution.py:283
  117.9 6.6 %all-to-all-done.3 = bf16[8,512,128]{2,1,0:T(8,128)(2,1)S(1)} async-done(((bf16[8,512,128]{2,1,0:T(8,128)(2,1)}), bf16[8,512,128]{2,1,0:T(8,128)(2,1)S(1)}, u32[]{:S(2)}, u32[]{:S(2)}) %all-to-all-start.3) | async-done | bytes 1048608 | tf_op jit(solution)/shard_map/all_to_all | solution.py:26
  124.5 3.7 %all-to-all-start.5 = ((bf16[8,512,128]{2,1,0:T(8,128)(2,1)}), bf16[8,512,128]{2,1,0:T(8,128)(2,1)S(1)}, u32[]{:S(2)}, u32[]{:S(2)}) async-start(bf16[8,512,128]{2,1,0:T(8,128)(2,1)} %bitcast.40), calls=%async_computation.5 | async-start | bytes 2097152 | tf_op jit(solution)/shard_map/all_to_all | solution.py:26
  128.2 2.2 shard_map.108
  130.4 13.6 %all-to-all-done.5 = bf16[8,512,128]{2,1,0:T(8,128)(2,1)S(1)} async-done(((bf16[8,512,128]{2,1,0:T(8,128)(2,1)}), bf16[8,512,128]{2,1,0:T(8,128)(2,1)S(1)}, u32[]{:S(2)}, u32[]{:S(2)}) %all-to-all-start.5) | async-done | bytes 1048608 | tf_op jit(solution)/shard_map/all_to_all | solution.py:26
  144.0 7.5 %all-to-all-start.4 = ((bf16[16,128,128]{2,1,0:T(8,128)(2,1)}), bf16[16,128,128]{2,1,0:T(8,128)(2,1)S(1)}, u32[]{:S(2)}, u32[]{:S(2)}) async-start(bf16[16,128,128]{2,1,0:T(8,128)(2,1)} %bitcast.14), calls=%async_computation.4 | async-start | bytes 1048576 | tf_op jit(solution)/shard_map/all_to_all | solution.py:26
  151.6 2.1 collective-permute-start
  153.7 4.5 %collective-permute-start.1 = (bf16[8,136,128]{2,1,0:T(8,128)(2,1)S(1)}, bf16[8,136,128]{2,1,0:T(8,128)(2,1)S(1)}, u32[]{:S(2)}, u32[]{:S(2)}) collective-permute-start(bf16[8,136,128]{2,1,0:T(8,128)(2,1)S(1)} %all-to-all-done.refs_0_), channel_id=1, source_target_pairs={{0,2},{1,3},{2,0},{3,1},{4,6},{5,7},{6,4},{7,5},{8,10},{9,11},{10,... | collective-permute-start | bytes 835592 | tf_op jit(solution)/shard_map/ppermute | solution.py:237
  158.2 1.9 collective-permute-start.2
  161.6 18.7 %all-to-all-done.4 = bf16[16,128,128]{2,1,0:T(8,128)(2,1)S(1)} async-done(((bf16[16,128,128]{2,1,0:T(8,128)(2,1)}), bf16[16,128,128]{2,1,0:T(8,128)(2,1)S(1)}, u32[]{:S(2)}, u32[]{:S(2)}) %all-to-all-start.4) | async-done | bytes 524320 | tf_op jit(solution)/shard_map/all_to_all | solution.py:26
  180.4 12.8 %all_gather.12.low = bf16[8,128,128]{2,1,0:T(8,128)(2,1)S(1)} all-gather(bf16[1,128,128]{2,1,0:T(8,128)(2,1)S(1)} %fusion), channel_id=1, replica_groups=mesh['z'=16,'x'=4,'c'=2,'tp'=4] {'x','c'}, dimensions={0}, use_global_device_ids=true | all-gather | bytes 294912 | tf_op jit(solution)/shard_map/all_gather | solution.py:292
  193.2 1.8 shard_map.110
  195.1 6.5 %all-to-all-start.6 = ((bf16[16,160,128]{2,1,0:T(8,128)(2,1)}), bf16[16,160,128]{2,1,0:T(8,128)(2,1)S(1)}, u32[]{:S(2)}, u32[]{:S(2)}) async-start(bf16[16,160,128]{2,1,0:T(8,128)(2,1)} %shard_map.110), calls=%async_computation.6 | async-start | bytes 1310720 | tf_op jit(solution)/shard_map/all_to_all | solution.py:26
  203.6 32.7 %all-to-all-done.6 = bf16[16,160,128]{2,1,0:T(8,128)(2,1)S(1)} async-done(((bf16[16,160,128]{2,1,0:T(8,128)(2,1)}), bf16[16,160,128]{2,1,0:T(8,128)(2,1)S(1)}, u32[]{:S(2)}, u32[]{:S(2)}) %all-to-all-start.6) | async-done | bytes 655392 | tf_op jit(solution)/shard_map/all_to_all | solution.py:26
  (73 shorter events, 16.0 us)
Async XLA Ops:
  0.6 7.7 %copy-start.8 = (bf16[128,128]{1,0:T(8,128)(2,1)S(1)}, bf16[128,128]{1,0:T(8,128)(2,1)}, u32[]{:S(2)}) copy-start(bf16[128,128]{1,0:T(8,128)(2,1)} %param.8) | copy-start | bytes 98308
  4.0 42.8 %all-to-all-start = ((bf16[8,136,128]{2,1,0:T(8,128)(2,1)}), bf16[8,136,128]{2,1,0:T(8,128)(2,1)S(1)}, u32[]{:S(2)}, u32[]{:S(2)}) async-start(bf16[8,136,128]{2,1,0:T(8,128)(2,1)} %shard_map.102), calls=%async_computation | async-start | bytes 557056 | tf_op jit(solution)/shard_map/all_to_all | solution.py:26
  46.9 35.4 %copy-start.17 = (s32[128]{0:T(128)}, s32[128]{0:T(128)S(1)}, u32[]{:S(2)}) copy-start(s32[128]{0:T(128)S(1)} %reshape.118.asked) | copy-start | bytes 1540
  48.6 4.7 %copy-start.12 = (bf16[128,128]{1,0:T(8,128)(2,1)S(1)}, bf16[128,128]{1,0:T(8,128)(2,1)}, u32[]{:S(2)}) copy-start(bf16[128,128]{1,0:T(8,128)(2,1)} %param.9) | copy-start | bytes 98308
  48.6 35.4 %all-to-all-start.1 = ((bf16[8,512,128]{2,1,0:T(8,128)(2,1)}), bf16[8,512,128]{2,1,0:T(8,128)(2,1)S(1)}, u32[]{:S(2)}, u32[]{:S(2)}) async-start(bf16[8,512,128]{2,1,0:T(8,128)(2,1)} %bitcast.3), calls=%async_computation.1 | async-start | bytes 2097152 | tf_op jit(solution)/shard_map/all_to_all | solution.py:26
  84.0 5.1 %copy-start.22 = (s32[2,16]{1,0:T(2,128)S(1)}, s32[2,16]{1,0:T(2,128)}, u32[]{:S(2)}) copy-start(s32[2,16]{1,0:T(2,128)} %param.13) | copy-start | bytes 388
  84.0 5.2 %copy-start.21 = (f32[128,8]{0,1:T(8,128)S(1)}, f32[128,8]{0,1:T(8,128)}, u32[]{:S(2)}) copy-start(f32[128,8]{0,1:T(8,128)} %param.10) | copy-start | bytes 12292
  84.0 5.4 %copy-start.4 = (bf16[128,1024]{1,0:T(8,128)(2,1)S(1)}, bf16[128,1024]{1,0:T(8,128)(2,1)}, u32[]{:S(2)}) copy-start(bf16[128,1024]{1,0:T(8,128)(2,1)} %queries.3) | copy-start | bytes 786436
  84.0 5.4 %copy-start.6 = (bf16[128,1024]{1,0:T(8,128)(2,1)S(1)}, bf16[128,1024]{1,0:T(8,128)(2,1)}, u32[]{:S(2)}) copy-start(bf16[128,1024]{1,0:T(8,128)(2,1)} %dout.3) | copy-start | bytes 786436
  84.0 21.1 %all-to-all-start.2 = ((bf16[8,512,128]{2,1,0:T(8,128)(2,1)}), bf16[8,512,128]{2,1,0:T(8,128)(2,1)S(1)}, u32[]{:S(2)}, u32[]{:S(2)}) async-start(bf16[8,512,128]{2,1,0:T(8,128)(2,1)} %bitcast.7), calls=%async_computation.2 | async-start | bytes 2097152 | tf_op jit(solution)/shard_map/all_to_all | solution.py:26
  89.2 15.8 %copy-start.19 = (s32[32]{0:T(128)}, s32[32]{0:T(128)S(1)}, u32[]{:S(2)}) copy-start(s32[32]{0:T(128)S(1)} %reshape.97.chosen) | copy-start | bytes 388
  89.4 15.7 %copy-start.15 = (f32[8,128]{1,0:T(8,128)}, f32[8,128]{1,0:T(8,128)S(1)}, u32[]{:S(2)}) copy-start(f32[8,128]{1,0:T(8,128)S(1)} %reshape.100.lse) | copy-start | bytes 12292
  105.1 19.4 %all-to-all-start.3 = ((bf16[8,512,128]{2,1,0:T(8,128)(2,1)}), bf16[8,512,128]{2,1,0:T(8,128)(2,1)S(1)}, u32[]{:S(2)}, u32[]{:S(2)}) async-start(bf16[8,512,128]{2,1,0:T(8,128)(2,1)} %bitcast.39), calls=%async_computation.3 | async-start | bytes 2097152 | tf_op jit(solution)/shard_map/all_to_all | solution.py:26
  115.6 1.0 copy-start.3
  124.5 3.7 %copy-start.18 = (s32[128]{0:T(128)S(1)}, s32[128]{0:T(128)}, u32[]{:S(2)}) copy-start(s32[128]{0:T(128)} %copy-done.17) | copy-start | bytes 1540
  124.5 19.6 %all-to-all-start.5 = ((bf16[8,512,128]{2,1,0:T(8,128)(2,1)}), bf16[8,512,128]{2,1,0:T(8,128)(2,1)S(1)}, u32[]{:S(2)}, u32[]{:S(2)}) async-start(bf16[8,512,128]{2,1,0:T(8,128)(2,1)} %bitcast.40), calls=%async_computation.5 | async-start | bytes 2097152 | tf_op jit(solution)/shard_map/all_to_all | solution.py:26
  144.0 36.2 %all-to-all-start.4 = ((bf16[16,128,128]{2,1,0:T(8,128)(2,1)}), bf16[16,128,128]{2,1,0:T(8,128)(2,1)S(1)}, u32[]{:S(2)}, u32[]{:S(2)}) async-start(bf16[16,128,128]{2,1,0:T(8,128)(2,1)} %bitcast.14), calls=%async_computation.4 | async-start | bytes 1048576 | tf_op jit(solution)/shard_map/all_to_all | solution.py:26
  151.6 41.6 %collective-permute-start = (bf16[8,136,128]{2,1,0:T(8,128)(2,1)S(1)}, bf16[8,136,128]{2,1,0:T(8,128)(2,1)S(1)}, u32[]{:S(2)}, u32[]{:S(2)}) collective-permute-start(bf16[8,136,128]{2,1,0:T(8,128)(2,1)S(1)} %all-to-all-done.refs_0_), channel_id=1, source_target_pairs={{0,1},{1,2},{2,3},{3,0},{4,5},{5,6},{6,7},{7,4},{8,9},{9,10},{10,1... | collective-permute-start | bytes 835592 | tf_op jit(solution)/shard_map/ppermute | solution.py:237
  153.7 39.5 %collective-permute-start.1 = (bf16[8,136,128]{2,1,0:T(8,128)(2,1)S(1)}, bf16[8,136,128]{2,1,0:T(8,128)(2,1)S(1)}, u32[]{:S(2)}, u32[]{:S(2)}) collective-permute-start(bf16[8,136,128]{2,1,0:T(8,128)(2,1)S(1)} %all-to-all-done.refs_0_), channel_id=1, source_target_pairs={{0,2},{1,3},{2,0},{3,1},{4,6},{5,7},{6,4},{7,5},{8,10},{9,11},{10,... | collective-permute-start | bytes 835592 | tf_op jit(solution)/shard_map/ppermute | solution.py:237
  158.2 35.0 %collective-permute-start.2 = (bf16[8,136,128]{2,1,0:T(8,128)(2,1)S(1)}, bf16[8,136,128]{2,1,0:T(8,128)(2,1)S(1)}, u32[]{:S(2)}, u32[]{:S(2)}) collective-permute-start(bf16[8,136,128]{2,1,0:T(8,128)(2,1)S(1)} %all-to-all-done.refs_0_), channel_id=1, source_target_pairs={{0,3},{1,0},{2,1},{3,2},{4,7},{5,4},{6,5},{7,6},{8,11},{9,8},{10,9... | collective-permute-start | bytes 835592 | tf_op jit(solution)/shard_map/ppermute | solution.py:237
  195.1 6.6 %copy-start.1 = (bf16[2,512,512]{2,1,0:T(8,128)(2,1)S(1)}, bf16[2,512,512]{2,1,0:T(8,128)(2,1)}, u32[]{:S(2)}) copy-start(bf16[2,512,512]{2,1,0:T(8,128)(2,1)} %copy-done) | copy-start | bytes 3145732
  195.1 6.6 %copy-start.10 = (bf16[2,512,128]{2,1,0:T(8,128)(2,1)S(1)}, bf16[2,512,128]{2,1,0:T(8,128)(2,1)}, u32[]{:S(2)}) copy-start(bf16[2,512,128]{2,1,0:T(8,128)(2,1)} %copy-done.9) | copy-start | bytes 786436
  195.1 41.2 %all-to-all-start.6 = ((bf16[16,160,128]{2,1,0:T(8,128)(2,1)}), bf16[16,160,128]{2,1,0:T(8,128)(2,1)S(1)}, u32[]{:S(2)}, u32[]{:S(2)}) async-start(bf16[16,160,128]{2,1,0:T(8,128)(2,1)} %shard_map.110), calls=%async_computation.6 | async-start | bytes 1310720 | tf_op jit(solution)/shard_map/all_to_all | solution.py:26
  201.6 35.3 %copy-start.14 = (f32[4,32,128]{2,1,0:T(8,128)S(1)}, f32[4,32,128]{2,1,0:T(8,128)}, u32[]{:S(2)}) copy-start(f32[4,32,128]{2,1,0:T(8,128)} %copy-done.13) | copy-start | bytes 196612
  (9 other events, 7.5 us)

commit v3 on v2

--- a/solution.py
+++ b/solution.py
@@ -53,8 +53,17 @@
             out[q * nz + z] = column[z * per + block]
 
 
-def by_feature(nq, rows, features, wanted, out):
+def pick_apart(nz, asked, peer, column, *outs):
+    kblocks = column.shape[0] // nz
+    for d, out in enumerate(outs):
+        for z in range(nz):
+            block = jnp.maximum(asked[peer[d] * nz + z] - 1, 0)
+            out[z] = column[z * kblocks + block]
+
+
+def by_feature(nq, rows, chosen, here, features, out):
     tok, cols = features.shape
+    kblocks = tok // KB
     for i in range(cols // HD):
         tile = features[:, i * HD : (i + 1) * HD].T
         for j in range(HD // rows):
@@ -62,25 +71,42 @@
             out[piece % nq, (piece // nq) * rows : (piece // nq + 1) * rows] = tile[
                 j * rows : (j + 1) * rows
             ]
+    at = lax.broadcasted_iota(jnp.int32, (nq, HD), 0) * HD + lax.broadcasted_iota(
+        jnp.int32, (nq, HD), 1
+    )
+    wanted = jnp.zeros((nq, HD), F32)
+    for e in range(chosen.shape[0]):
+        c = chosen[e]
+        owner = c // kblocks
+        place = jnp.where(owner != here[0], (owner % nq) * HD + owner // nq, -1)
+        wanted = jnp.where(at == place, (c % kblocks + 1).astype(F32), wanted)
+    wanted = wanted.astype(BF16)
     for q in range(nq):
-        out[q, cols // nq :] = jnp.broadcast_to(wanted[q : q + 1], (SUB, tok))
-
-
-def slots_of(chosen, here, b, nq, nz, kblocks):
+        out[q, cols // nq :] = jnp.broadcast_to(wanted[q : q + 1], (SUB, HD))
+
+
+def slots_of(chosen, here, b, nq, nz, kblocks, where):
     slots = []
     for e in range(NSEL):
         c = chosen[b * NSEL + e]
         owner = c // kblocks
-        place = (owner % nq) * nz + owner // nq
+        place = where(owner % nq) * nz + owner // nq
         slots.append((c, owner != here, place, c % kblocks))
     return slots
 
 
 def select(slots, got, own, out):
     for e, (_, remote, place, within) in enumerate(slots):
-        far = got[jnp.where(remote, place, 0)]
         near = own[within]
-        out[e * KB : (e + 1) * KB] = jnp.where(remote, far, near)
+        if isinstance(got, tuple):
+            nz = got[0].shape[0]
+            d, z = place // nz, place % nz
+            block = got[0][z]
+            for i in range(1, len(got)):
+                block = jnp.where(d == i, got[i][z], block)
+        else:
+            block = got[jnp.where(remote, place, 0)]
+        out[e * KB : (e + 1) * KB] = jnp.where(remote, block, near)
 
 
 def heads_of(ref, b, p):
@@ -132,7 +158,7 @@
 def value_terms(nq, nz, chosen, here, queries, dout, lse, got_k, own_k, send, own_sum, sel, kpos, low, rows, total, part):
     peers, kblocks = nq * nz, own_k.shape[0]
     qblocks, pairs = queries.shape[0] // QB, queries.shape[1] // HD // 2
-    slots = [slots_of(chosen, here[0], b, nq, nz, kblocks) for b in range(qblocks)]
+    slots = [slots_of(chosen, here[0], b, nq, nz, kblocks, lambda q: q) for b in range(qblocks)]
     for b in range(qblocks):
         select(slots[b], got_k, own_k, sel)
         set_positions(slots[b], kpos)
@@ -146,14 +172,28 @@
     scatter(slots, [part.at[b] for b in range(qblocks)], total, send, own_sum, peers, kblocks)
 
 
-def key_terms(nq, nz, chosen, here, queries, dout, lse, got_k, own_k, got_v, own_v, send, own_sum, low, sel, sel_v, kpos, rows, total, part):
+def key_terms(nx, nc, nz, chosen, here, queries, dout, lse, got_k, own_k, own_v, *refs):
+    nq = nx * nc
+    got_v, refs = refs[:nq], refs[nq:]
+    sends, refs = refs[:nq], refs[nq:]
+    own_sum, low, sel, sel_v, kpos, rows, total, part, send = refs
     peers, kblocks = nq * nz, own_k.shape[0]
     qblocks, pairs = queries.shape[0] // QB, queries.shape[1] // HD // 2
-    slots = [slots_of(chosen, here[0], b, nq, nz, kblocks) for b in range(qblocks)]
+    mine = here[0] % nq
+
+    def behind(q):
+        return (mine // nc - q // nc) % nx * nc + (mine + q) % nc
+
+    def ahead(q):
+        return (q // nc - mine // nc) % nx * nc + (mine + q) % nc
+
+    def slots(b, where):
+        return slots_of(chosen, here[0], b, nq, nz, kblocks, where)
+
     for b in range(qblocks):
-        select(slots[b], got_k, own_k, sel.at[b])
-        select(slots[b], got_v, own_v, sel_v)
-        set_positions(slots[b], kpos)
+        select(slots(b, lambda q: q), got_k, own_k, sel.at[b])
+        select(slots(b, behind), got_v, own_v, sel_v)
+        set_positions(slots(b, ahead), kpos)
         start = here[0] * queries.shape[0] + b * QB
         for p in range(pairs):
             pair = heads_of(queries, b, p)
@@ -163,7 +203,10 @@
             low[b, :, p * HD : (p + 1) * HD] = (prob * (dprob - delta)).astype(BF16)
             rows[p * HD : (p + 1) * HD] = pair
         part[b] = jnp.dot(low[b], rows[...], preferred_element_type=F32) * SCALE
-    scatter(slots, [part.at[b] for b in range(qblocks)], total, send, own_sum, peers, kblocks)
+    back = [slots(b, ahead) for b in range(qblocks)]
+    scatter(back, [part.at[b] for b in range(qblocks)], total, send, own_sum, peers, kblocks)
+    for d, out in enumerate(sends):
+        out[...] = send[d * nz : (d + 1) * nz]
 
 
 def query_terms(low, sel, out):
@@ -178,15 +221,17 @@
                 )
 
 
-def gather_home(nq, nz, asked, came, dense, total):
+def gather_home(nq, nz, asked, peer, *refs):
+    *came, dense, total = refs
     blocks = dense.shape[0]
     kblocks = blocks // nz
     total[...] = jnp.zeros_like(total)
     for q in range(nq):
         for z in range(nz):
-            a = asked[q * nz + z]
+            a = asked[peer[q] * nz + z]
             at = jnp.where(a > 0, z * kblocks + a - 1, blocks)
-            total[at] = total[at] + came[q * nz + z].astype(F32)
+            piece = came[0][q * nz + z] if len(came) == 1 else came[q][z]
+            total[at] = total[at] + piece.astype(F32)
     dense[...] = total[0:blocks].astype(BF16)
 
 
@@ -218,36 +263,52 @@
     peers = nq * nz
     shape = jax.ShapeDtypeStruct
 
-    owner = chosen // kblocks
-    place = (owner % nq) * nz + owner // nq
-    named = (place[:, :, None] == jnp.arange(peers, dtype=jnp.int32)) & (owner != here)[:, :, None]
-    wanted = jnp.max(jnp.where(named, (chosen % kblocks)[:, :, None] + 1, 0), axis=(0, 1))
-    wanted = jnp.pad(wanted.reshape(nq, nz).astype(BF16), ((0, 0), (0, tok - nz)))
+    names = chosen.reshape(qblocks * NSEL)
+    me = here.reshape(1).astype(jnp.int32)
 
     rows_out = normed_input.shape[1] * tp // peers
     mine = nz // tp
     feats = mine * rows_out
     split = call(
-        functools.partial(by_feature, nq, rows_out), shape((nq, feats + SUB, tok), BF16), "vv"
-    )(normed_input, wanted)
+        functools.partial(by_feature, nq, rows_out),
+        shape((nq, feats + SUB, tok), BF16),
+        "ssv",
+    )(names, me, normed_input)
     split = to_peers(split, XC)
     asked = split[:, feats, :nz].astype(jnp.int32).reshape(peers)
     planes = [split]
     for k in range(1, tp):
         planes.append(lax.ppermute(planes[0], "tp", [(i, (i + k) % tp) for i in range(tp)]))
     order = ((lax.axis_index("tp") - jnp.arange(tp)) % tp).astype(jnp.int32)
-    names = chosen.reshape(qblocks * NSEL)
-    me = here.reshape(1).astype(jnp.int32)
-
-    def fetch(rows):
-        column = lax.all_gather(rows, "z", axis=0, tiled=True).reshape(nz * kblocks, KB, HD)
-        sent = call(functools.partial(pick, nq, nz), shape((peers, KB, HD), BF16), "sv")(
-            asked, column
-        )
-        return to_peers(sent.reshape(nq, nz * KB, HD), XC).reshape(peers, KB, HD)
-
-    got_k = fetch(keys)
-    got_v = fetch(values)
+    nx, nc = lax.axis_size("x"), lax.axis_size("c")
+    steps, other = jnp.arange(nq) // nc, jnp.arange(nq) % nc
+    my_x, my_c = lax.axis_index("x"), lax.axis_index("c")
+    ahead = ((my_x + steps) % nx * nc + (my_c + other) % nc).astype(jnp.int32)
+    behind = ((my_x - steps) % nx * nc + (my_c + other) % nc).astype(jnp.int32)
+    direct = jnp.arange(nq, dtype=jnp.int32)
+
+    def around(pieces):
+        came = [pieces[0]]
+        for d in range(1, nq):
+            s, r = d // nc, d % nc
+            pairs = [
+                (x * nc + c, (x + s) % nx * nc + (c + r) % nc) for x in range(nx) for c in range(nc)
+            ]
+            came.append(lax.ppermute(pieces[d], XC, pairs))
+        return came
+
+    def column(rows):
+        return lax.all_gather(rows, "z", axis=0, tiled=True).reshape(nz * kblocks, KB, HD)
+
+    column_k = column(keys)
+    sent = call(functools.partial(pick, nq, nz), shape((peers, KB, HD), BF16), "sv")(
+        asked, column_k
+    )
+    got_k = to_peers(sent.reshape(nq, nz * KB, HD), XC).reshape(peers, KB, HD)
+    column_v = column(values)
+    slab = shape((nz, KB, HD), BF16)
+    sent = call(functools.partial(pick_apart, nz), (slab,) * nq, "ssv")(asked, ahead, column_v)
+    got_v = around(sent)
 
     own_k = keys.reshape(kblocks, KB, HD)
     own_v = values.reshape(kblocks, KB, HD)
@@ -260,15 +321,13 @@
         pltpu.VMEM((qblocks, span, HD), F32),
     ]
 
-    def home(sent):
-        came = to_peers(sent.reshape(nq, nz * KB, HD), XC).reshape(peers, KB, HD)
-        dense = call(
+    def home(came, peer):
+        return call(
             functools.partial(gather_home, nq, nz),
             shape((nz * kblocks, KB, HD), BF16),
-            "sv",
+            "ss" + "v" * len(came),
             [pltpu.VMEM((nz * kblocks + 1, KB, HD), F32)],
-        )(asked, came)
-        return dense.reshape(nz, tok, HD)
+        )(asked, peer, *came).reshape(nz, tok, HD)
 
     sent_v, mine_v = call(
         functools.partial(value_terms, nq, nz),
@@ -276,17 +335,24 @@
         "ssvvvvv",
         [pltpu.VMEM((span, HD), BF16), work[0], pltpu.VMEM((span, heads * QB), BF16), *work[1:]],
     )(names, me, queries, out_grad, lse, got_k, own_k)
-    dense_v = home(sent_v)
+    came_v = to_peers(sent_v.reshape(nq, nz * KB, HD), XC).reshape(peers, KB, HD)
+    dense_v = home([came_v], direct)
     sums_v = to_peers(dense_v, "z")
     value_grad = mine_v.reshape(tok, HD) + jnp.sum(sums_v.astype(F32), axis=0)
 
-    sent_k, mine_k, low, sel = call(
-        functools.partial(key_terms, nq, nz),
-        (*terms, shape((qblocks, span, heads * QB), BF16), shape((qblocks, span, HD), BF16)),
-        "ssvvvvvvv",
-        [pltpu.VMEM((span, HD), BF16), *work],
-    )(names, me, queries, out_grad, lse, got_k, own_k, got_v, own_v)
-    dense_k = home(sent_k)
+    *sent_k, mine_k, low, sel = call(
+        functools.partial(key_terms, nx, nc, nz),
+        (
+            *(slab,) * nq,
+            terms[1],
+            shape((qblocks, span, heads * QB), BF16),
+            shape((qblocks, span, HD), BF16),
+        ),
+        "ss" + "v" * (6 + nq),
+        [pltpu.VMEM((span, HD), BF16), *work, pltpu.VMEM((peers, KB, HD), BF16)],
+    )(names, me, queries, out_grad, lse, got_k, own_k, own_v, *got_v)
+    came_k = around(sent_k)
+    dense_k = home(came_k, behind)
     query_grad = call(query_terms, shape((tok, cols), F32), "vv")(low, sel)
 
     all_low = lax.all_gather(value_grad.astype(BF16), XC, axis=0)

time: 239 us -> 287 us (1.20)
  the two profiles are of different devices: /device:TPU:24 before, /device:TPU:2 now
where the time goes in v3:
time: 287 us; the launch traced here: 286 us
  blocking collectives  118 us (41%)
  starting transfers between devices  84.8 us (30%)
  waiting for transfers between devices  51.9 us (18%)
  Pallas kernels  18.3 us (6%)
  local copies, waits for them, and re-layouts  9.39 us (3%)
    all_gather x2, blocking collectives, column(): lax.all_gather(rows, 'z', axis=0, tiled=True).reshape(nz * kblocks, KB, HD)  84.9 us
    all_to_all x4, waiting for transfers between devices, to_peers(): return lax.all_to_all(parts, axis, split_axis=0, concat_axis=0, tiled=True)  47 us
    ppermute x14, starting transfers between devices, around(): came.append(lax.ppermute(pieces[d], XC, pairs))  41.6 us
    all_to_all x4, starting transfers between devices, to_peers(): return lax.all_to_all(parts, axis, split_axis=0, concat_axis=0, tiled=True)  31.7 us
    all_to_all x1, blocking collectives, to_peers(): return lax.all_to_all(parts, axis, split_axis=0, concat_axis=0, tiled=True)  18.5 us
    all_gather x1, blocking collectives, local(): all_low = lax.all_gather(value_grad.astype(BF16), XC, axis=0)  14.1 us
    ppermute x3, starting transfers between devices, local(): lax.ppermute(planes[0], 'tp', [(i, (i + k) % tp) for i in range(tp)])  11.5 us
    unnamed x32, local copies, waits for them, and re-layouts  7.79 us
  transfers between devices with their start and end apart: 21, of which 4 were waited for; matrix products, arithmetic and copies ran while one was open for 1% of the time, Pallas kernels for 3%

profile of v3, /device:TPU:2, one launch (start us, length us, event | category | flops | bytes accessed | tf_op | source)
XLA Modules:
  0.0 285.6 jit_solution(6298160931230371024)
XLA Ops:
  4.0 9.2 %all-to-all-start = ((bf16[8,136,128]{2,1,0:T(8,128)(2,1)}), bf16[8,136,128]{2,1,0:T(8,128)(2,1)S(1)}, u32[]{:S(2)}, u32[]{:S(2)}) async-start(bf16[8,136,128]{2,1,0:T(8,128)(2,1)} %shard_map.102), calls=%async_computation | async-start | bytes 557056 | tf_op jit(solution)/shard_map/all_to_all | solution.py:26
  13.2 33.9 %all_gather.10 = bf16[2048,128]{1,0:T(8,128)(2,1)S(1)} all-gather(bf16[128,128]{1,0:T(8,128)(2,1)S(1)} %copy-done.2), channel_id=1, replica_groups=mesh['z'=16,'x'=4,'c'=2,'tp'=4] {'z'}, dimensions={0}, use_global_device_ids=true | all-gather | bytes 557056 | tf_op jit(solution)/shard_map/all_gather | solution.py:301
  48.9 4.9 %all-to-all-start.1 = ((bf16[8,512,128]{2,1,0:T(8,128)(2,1)}), bf16[8,512,128]{2,1,0:T(8,128)(2,1)S(1)}, u32[]{:S(2)}, u32[]{:S(2)}) async-start(bf16[8,512,128]{2,1,0:T(8,128)(2,1)} %bitcast.3), calls=%async_computation.1 | async-start | bytes 2097152 | tf_op jit(solution)/shard_map/all_to_all | solution.py:26
  54.0 14.3 %all-to-all-done.1 = bf16[8,512,128]{2,1,0:T(8,128)(2,1)S(1)} async-done(((bf16[8,512,128]{2,1,0:T(8,128)(2,1)}), bf16[8,512,128]{2,1,0:T(8,128)(2,1)S(1)}, u32[]{:S(2)}, u32[]{:S(2)}) %all-to-all-start.1) | async-done | bytes 1048608 | tf_op jit(solution)/shard_map/all_to_all | solution.py:26
  70.5 18.5 %all_to_all.25 = bf16[8,512,128]{2,1,0:T(8,128)(2,1)S(1)} all-to-all(bf16[8,512,128]{2,1,0:T(8,128)(2,1)S(1)} %bitcast.33), channel_id=1, replica_groups=mesh['z'=16,'x'=4,'c'=2,'tp'=4] {'x','c'}, dimensions={0} | all-to-all | bytes 2097152 | tf_op jit(solution)/shard_map/all_to_all | solution.py:26
  91.3 7.1 %all-to-all-start.3 = ((bf16[16,128,128]{2,1,0:T(8,128)(2,1)}), bf16[16,128,128]{2,1,0:T(8,128)(2,1)}, u32[]{:S(2)}, u32[]{:S(2)}) async-start(bf16[16,128,128]{2,1,0:T(8,128)(2,1)} %bitcast.12), calls=%async_computation.3 | async-start | bytes 1048576 | tf_op jit(solution)/shard_map/all_to_all | solution.py:26
  98.4 51.1 %all_gather.11 = bf16[2048,128]{1,0:T(8,128)(2,1)S(1)} all-gather(bf16[128,128]{1,0:T(8,128)(2,1)S(1)} %copy-done.4), channel_id=1, replica_groups=mesh['z'=16,'x'=4,'c'=2,'tp'=4] {'z'}, dimensions={0}, use_global_device_ids=true | all-gather | bytes 557056 | tf_op jit(solution)/shard_map/all_gather | solution.py:301
  154.2 3.6 %collective-permute-start.2 = (bf16[16,32,128]{2,1,0:T(8,128)(2,1)S(1)}, bf16[16,32,128]{2,1,0:T(8,128)(2,1)S(1)}, u32[]{:S(2)}, u32[]{:S(2)}) collective-permute-start(bf16[16,32,128]{2,1,0:T(8,128)(2,1)S(1)} %get-tuple-element.28), channel_id=1, source_target_pairs={{0,12},{4,8},{8,20},{12,16},{16,28},{20,24},{24,4},{28,0},{1,13},{... | collective-permute-start | bytes 393224 | tf_op jit(solution)/shard_map/ppermute | solution.py:297
  157.8 4.1 %collective-permute-start.3 = (bf16[16,32,128]{2,1,0:T(8,128)(2,1)S(1)}, bf16[16,32,128]{2,1,0:T(8,128)(2,1)S(1)}, u32[]{:S(2)}, u32[]{:S(2)}) collective-permute-start(bf16[16,32,128]{2,1,0:T(8,128)(2,1)S(1)} %get-tuple-element.29), channel_id=1, source_target_pairs={{0,16},{4,20},{8,24},{12,28},{16,0},{20,4},{24,8},{28,12},{1,17},{... | collective-permute-start | bytes 393224 | tf_op jit(solution)/shard_map/ppermute | solution.py:297
  161.9 2.9 %collective-permute-start.4 = (bf16[16,32,128]{2,1,0:T(8,128)(2,1)S(1)}, bf16[16,32,128]{2,1,0:T(8,128)(2,1)S(1)}, u32[]{:S(2)}, u32[]{:S(2)}) collective-permute-start(bf16[16,32,128]{2,1,0:T(8,128)(2,1)S(1)} %get-tuple-element.30), channel_id=1, source_target_pairs={{0,20},{4,16},{8,28},{12,24},{16,4},{20,0},{24,12},{28,8},{1,21},{... | collective-permute-start | bytes 393224 | tf_op jit(solution)/shard_map/ppermute | solution.py:297
  164.8 2.9 %collective-permute-start.5 = (bf16[16,32,128]{2,1,0:T(8,128)(2,1)S(1)}, bf16[16,32,128]{2,1,0:T(8,128)(2,1)S(1)}, u32[]{:S(2)}, u32[]{:S(2)}) collective-permute-start(bf16[16,32,128]{2,1,0:T(8,128)(2,1)S(1)} %get-tuple-element.31), channel_id=1, source_target_pairs={{0,24},{4,28},{8,0},{12,4},{16,8},{20,12},{24,16},{28,20},{1,25},{... | collective-permute-start | bytes 393224 | tf_op jit(solution)/shard_map/ppermute | solution.py:297
  167.8 4.0 %collective-permute-start.6 = (bf16[16,32,128]{2,1,0:T(8,128)(2,1)S(1)}, bf16[16,32,128]{2,1,0:T(8,128)(2,1)S(1)}, u32[]{:S(2)}, u32[]{:S(2)}) collective-permute-start(bf16[16,32,128]{2,1,0:T(8,128)(2,1)S(1)} %get-tuple-element.32), channel_id=1, source_target_pairs={{0,28},{4,24},{8,4},{12,0},{16,12},{20,8},{24,20},{28,16},{1,29},{... | collective-permute-start | bytes 393224 | tf_op jit(solution)/shard_map/ppermute | solution.py:297
  173.9 2.8 collective-permute-done.6.refs_7_
  176.7 5.1 %shard_map.105 = (bf16[16,32,128]{2,1,0:T(8,128)(2,1)S(1)}, bf16[16,32,128]{2,1,0:T(8,128)(2,1)}, bf16[16,32,128]{2,1,0:T(8,128)(2,1)}, bf16[16,32,128]{2,1,0:T(...) custom-call(s32[32]{0:T(128)S(1)} %reshape.79.chosen, ...), custom_call_target="tpu_custom_call" | custom-call | tf_op jit(solution)/shard_map/pallas_call | solution.py:343
  183.1 4.0 %collective-permute-start.10 = (bf16[16,32,128]{2,1,0:T(8,128)(2,1)S(1)}, bf16[16,32,128]{2,1,0:T(8,128)(2,1)S(1)}, u32[]{:S(2)}, u32[]{:S(2)}) collective-permute-start(bf16[16,32,128]{2,1,0:T(8,128)(2,1)S(1)} %get-tuple-element.42), channel_id=1, source_target_pairs={{0,16},{4,20},{8,24},{12,28},{16,0},{20,4},{24,8},{28,12},{1,17},{... | collective-permute-start | bytes 393224 | tf_op jit(solution)/shard_map/ppermute | solution.py:297
  187.1 2.8 collective-permute-start.11
  189.9 2.7 collective-permute-start.12
  192.6 4.4 %collective-permute-start.13 = (bf16[16,32,128]{2,1,0:T(8,128)(2,1)}, bf16[16,32,128]{2,1,0:T(8,128)(2,1)S(1)}, u32[]{:S(2)}, u32[]{:S(2)}) collective-permute-start(bf16[16,32,128]{2,1,0:T(8,128)(2,1)} %get-tuple-element.45), channel_id=1, source_target_pairs={{0,28},{4,24},{8,4},{12,0},{16,12},{20,8},{24,20},{28,16},{1,29},{... | collective-permute-start | bytes 393224 | tf_op jit(solution)/shard_map/ppermute | solution.py:297
  203.4 3.5 %collective-permute-start.14 = (bf16[8,136,128]{2,1,0:T(8,128)(2,1)S(1)}, bf16[8,136,128]{2,1,0:T(8,128)(2,1)S(1)}, u32[]{:S(2)}, u32[]{:S(2)}) collective-permute-start(bf16[8,136,128]{2,1,0:T(8,128)(2,1)S(1)} %all-to-all-done.refs_0_), channel_id=1, source_target_pairs={{0,1},{1,2},{2,3},{3,0},{4,5},{5,6},{6,7},{7,4},{8,9},{9,10},{10,1... | collective-permute-start | bytes 835592 | tf_op jit(solution)/shard_map/ppermute | solution.py:281
  206.9 4.8 %collective-permute-start.15 = (bf16[8,136,128]{2,1,0:T(8,128)(2,1)S(1)}, bf16[8,136,128]{2,1,0:T(8,128)(2,1)S(1)}, u32[]{:S(2)}, u32[]{:S(2)}) collective-permute-start(bf16[8,136,128]{2,1,0:T(8,128)(2,1)S(1)} %all-to-all-done.refs_0_), channel_id=1, source_target_pairs={{0,2},{1,3},{2,0},{3,1},{4,6},{5,7},{6,4},{7,5},{8,10},{9,11},{10,... | collective-permute-start | bytes 835592 | tf_op jit(solution)/shard_map/ppermute | solution.py:281
  212.4 3.2 %collective-permute-start.16 = (bf16[8,136,128]{2,1,0:T(8,128)(2,1)S(1)}, bf16[8,136,128]{2,1,0:T(8,128)(2,1)S(1)}, u32[]{:S(2)}, u32[]{:S(2)}) collective-permute-start(bf16[8,136,128]{2,1,0:T(8,128)(2,1)S(1)} %all-to-all-done.refs_0_), channel_id=1, source_target_pairs={{0,3},{1,0},{2,1},{3,2},{4,7},{5,4},{6,5},{7,6},{8,11},{9,8},{10,9... | collective-permute-start | bytes 835592 | tf_op jit(solution)/shard_map/ppermute | solution.py:281
  223.2 14.1 %all_gather.12.low = bf16[8,128,128]{2,1,0:T(8,128)(2,1)S(1)} all-gather(bf16[1,128,128]{2,1,0:T(8,128)(2,1)S(1)} %fusion), channel_id=1, replica_groups=mesh['z'=16,'x'=4,'c'=2,'tp'=4] {'x','c'}, dimensions={0}, use_global_device_ids=true | all-gather | bytes 294912 | tf_op jit(solution)/shard_map/all_gather | solution.py:358
  239.2 10.4 %all-to-all-start.4 = ((bf16[16,160,128]{2,1,0:T(8,128)(2,1)}), bf16[16,160,128]{2,1,0:T(8,128)(2,1)S(1)}, u32[]{:S(2)}, u32[]{:S(2)}) async-start(bf16[16,160,128]{2,1,0:T(8,128)(2,1)} %shard_map.110), calls=%async_computation.4 | async-start | bytes 1310720 | tf_op jit(solution)/shard_map/all_to_all | solution.py:26
  251.5 32.7 %all-to-all-done.4 = bf16[16,160,128]{2,1,0:T(8,128)(2,1)S(1)} async-done(((bf16[16,160,128]{2,1,0:T(8,128)(2,1)}), bf16[16,160,128]{2,1,0:T(8,128)(2,1)S(1)}, u32[]{:S(2)}, u32[]{:S(2)}) %all-to-all-start.4) | async-done | bytes 655392 | tf_op jit(solution)/shard_map/all_to_all | solution.py:26
  (79 shorter events, 37.5 us)
Async XLA Ops:
  4.0 43.1 %all-to-all-start = ((bf16[8,136,128]{2,1,0:T(8,128)(2,1)}), bf16[8,136,128]{2,1,0:T(8,128)(2,1)S(1)}, u32[]{:S(2)}, u32[]{:S(2)}) async-start(bf16[8,136,128]{2,1,0:T(8,128)(2,1)} %shard_map.102), calls=%async_computation | async-start | bytes 557056 | tf_op jit(solution)/shard_map/all_to_all | solution.py:26
  48.9 19.4 %copy-start = (bf16[128,1024]{1,0:T(8,128)(2,1)S(1)}, bf16[128,1024]{1,0:T(8,128)(2,1)}, u32[]{:S(2)}) copy-start(bf16[128,1024]{1,0:T(8,128)(2,1)} %queries.3) | copy-start | bytes 786436
  48.9 19.4 %copy-start.1 = (bf16[128,1024]{1,0:T(8,128)(2,1)S(1)}, bf16[128,1024]{1,0:T(8,128)(2,1)}, u32[]{:S(2)}) copy-start(bf16[128,1024]{1,0:T(8,128)(2,1)} %dout.3) | copy-start | bytes 786436
  48.9 19.4 %all-to-all-start.1 = ((bf16[8,512,128]{2,1,0:T(8,128)(2,1)}), bf16[8,512,128]{2,1,0:T(8,128)(2,1)S(1)}, u32[]{:S(2)}, u32[]{:S(2)}) async-start(bf16[8,512,128]{2,1,0:T(8,128)(2,1)} %bitcast.3), calls=%async_computation.1 | async-start | bytes 2097152 | tf_op jit(solution)/shard_map/all_to_all | solution.py:26
  91.3 130.8 %all-to-all-start.3 = ((bf16[16,128,128]{2,1,0:T(8,128)(2,1)}), bf16[16,128,128]{2,1,0:T(8,128)(2,1)}, u32[]{:S(2)}, u32[]{:S(2)}) async-start(bf16[16,128,128]{2,1,0:T(8,128)(2,1)} %bitcast.12), calls=%async_computation.3 | async-start | bytes 1048576 | tf_op jit(solution)/shard_map/all_to_all | solution.py:26
  150.3 14.5 %collective-permute-start = (bf16[16,32,128]{2,1,0:T(8,128)(2,1)S(1)}, bf16[16,32,128]{2,1,0:T(8,128)(2,1)S(1)}, u32[]{:S(2)}, u32[]{:S(2)}) collective-permute-start(bf16[16,32,128]{2,1,0:T(8,128)(2,1)S(1)} %get-tuple-element.26), channel_id=1, source_target_pairs={{0,4},{4,0},{8,12},{12,8},{16,20},{20,16},{24,28},{28,24},{1,5},{5... | collective-permute-start | bytes 393224 | tf_op jit(solution)/shard_map/ppermute | solution.py:297
  152.2 15.5 %collective-permute-start.1 = (bf16[16,32,128]{2,1,0:T(8,128)(2,1)S(1)}, bf16[16,32,128]{2,1,0:T(8,128)(2,1)S(1)}, u32[]{:S(2)}, u32[]{:S(2)}) collective-permute-start(bf16[16,32,128]{2,1,0:T(8,128)(2,1)S(1)} %get-tuple-element.27), channel_id=1, source_target_pairs={{0,8},{4,12},{8,16},{12,20},{16,24},{20,28},{24,0},{28,4},{1,9},{5... | collective-permute-start | bytes 393224 | tf_op jit(solution)/shard_map/ppermute | solution.py:297
  154.2 17.6 %collective-permute-start.2 = (bf16[16,32,128]{2,1,0:T(8,128)(2,1)S(1)}, bf16[16,32,128]{2,1,0:T(8,128)(2,1)S(1)}, u32[]{:S(2)}, u32[]{:S(2)}) collective-permute-start(bf16[16,32,128]{2,1,0:T(8,128)(2,1)S(1)} %get-tuple-element.28), channel_id=1, source_target_pairs={{0,12},{4,8},{8,20},{12,16},{16,28},{20,24},{24,4},{28,0},{1,13},{... | collective-permute-start | bytes 393224 | tf_op jit(solution)/shard_map/ppermute | solution.py:297
  157.8 14.0 %collective-permute-start.3 = (bf16[16,32,128]{2,1,0:T(8,128)(2,1)S(1)}, bf16[16,32,128]{2,1,0:T(8,128)(2,1)S(1)}, u32[]{:S(2)}, u32[]{:S(2)}) collective-permute-start(bf16[16,32,128]{2,1,0:T(8,128)(2,1)S(1)} %get-tuple-element.29), channel_id=1, source_target_pairs={{0,16},{4,20},{8,24},{12,28},{16,0},{20,4},{24,8},{28,12},{1,17},{... | collective-permute-start | bytes 393224 | tf_op jit(solution)/shard_map/ppermute | solution.py:297
  161.9 9.9 %collective-permute-start.4 = (bf16[16,32,128]{2,1,0:T(8,128)(2,1)S(1)}, bf16[16,32,128]{2,1,0:T(8,128)(2,1)S(1)}, u32[]{:S(2)}, u32[]{:S(2)}) collective-permute-start(bf16[16,32,128]{2,1,0:T(8,128)(2,1)S(1)} %get-tuple-element.30), channel_id=1, source_target_pairs={{0,20},{4,16},{8,28},{12,24},{16,4},{20,0},{24,12},{28,8},{1,21},{... | collective-permute-start | bytes 393224 | tf_op jit(solution)/shard_map/ppermute | solution.py:297
  164.8 9.1 %collective-permute-start.5 = (bf16[16,32,128]{2,1,0:T(8,128)(2,1)S(1)}, bf16[16,32,128]{2,1,0:T(8,128)(2,1)S(1)}, u32[]{:S(2)}, u32[]{:S(2)}) collective-permute-start(bf16[16,32,128]{2,1,0:T(8,128)(2,1)S(1)} %get-tuple-element.31), channel_id=1, source_target_pairs={{0,24},{4,28},{8,0},{12,4},{16,8},{20,12},{24,16},{28,20},{1,25},{... | collective-permute-start | bytes 393224 | tf_op jit(solution)/shard_map/ppermute | solution.py:297
  167.8 8.9 %collective-permute-start.6 = (bf16[16,32,128]{2,1,0:T(8,128)(2,1)S(1)}, bf16[16,32,128]{2,1,0:T(8,128)(2,1)S(1)}, u32[]{:S(2)}, u32[]{:S(2)}) collective-permute-start(bf16[16,32,128]{2,1,0:T(8,128)(2,1)S(1)} %get-tuple-element.32), channel_id=1, source_target_pairs={{0,28},{4,24},{8,4},{12,0},{16,12},{20,8},{24,20},{28,16},{1,29},{... | collective-permute-start | bytes 393224 | tf_op jit(solution)/shard_map/ppermute | solution.py:297
  183.1 16.0 %collective-permute-start.10 = (bf16[16,32,128]{2,1,0:T(8,128)(2,1)S(1)}, bf16[16,32,128]{2,1,0:T(8,128)(2,1)S(1)}, u32[]{:S(2)}, u32[]{:S(2)}) collective-permute-start(bf16[16,32,128]{2,1,0:T(8,128)(2,1)S(1)} %get-tuple-element.42), channel_id=1, source_target_pairs={{0,16},{4,20},{8,24},{12,28},{16,0},{20,4},{24,8},{28,12},{1,17},{... | collective-permute-start | bytes 393224 | tf_op jit(solution)/shard_map/ppermute | solution.py:297
  187.1 14.0 %collective-permute-start.11 = (bf16[16,32,128]{2,1,0:T(8,128)(2,1)S(1)}, bf16[16,32,128]{2,1,0:T(8,128)(2,1)S(1)}, u32[]{:S(2)}, u32[]{:S(2)}) collective-permute-start(bf16[16,32,128]{2,1,0:T(8,128)(2,1)S(1)} %get-tuple-element.43), channel_id=1, source_target_pairs={{0,20},{4,16},{8,28},{12,24},{16,4},{20,0},{24,12},{28,8},{1,21},{... | collective-permute-start | bytes 393224 | tf_op jit(solution)/shard_map/ppermute | solution.py:297
  189.9 13.5 %collective-permute-start.12 = (bf16[16,32,128]{2,1,0:T(8,128)(2,1)}, bf16[16,32,128]{2,1,0:T(8,128)(2,1)S(1)}, u32[]{:S(2)}, u32[]{:S(2)}) collective-permute-start(bf16[16,32,128]{2,1,0:T(8,128)(2,1)} %get-tuple-element.44), channel_id=1, source_target_pairs={{0,24},{4,28},{8,0},{12,4},{16,8},{20,12},{24,16},{28,20},{1,25},{... | collective-permute-start | bytes 393224 | tf_op jit(solution)/shard_map/ppermute | solution.py:297
  192.6 14.3 %collective-permute-start.13 = (bf16[16,32,128]{2,1,0:T(8,128)(2,1)}, bf16[16,32,128]{2,1,0:T(8,128)(2,1)S(1)}, u32[]{:S(2)}, u32[]{:S(2)}) collective-permute-start(bf16[16,32,128]{2,1,0:T(8,128)(2,1)} %get-tuple-element.45), channel_id=1, source_target_pairs={{0,28},{4,24},{8,4},{12,0},{16,12},{20,8},{24,20},{28,16},{1,29},{... | collective-permute-start | bytes 393224 | tf_op jit(solution)/shard_map/ppermute | solution.py:297
  197.0 14.8 %collective-permute-start.7 = (bf16[16,32,128]{2,1,0:T(8,128)(2,1)}, bf16[16,32,128]{2,1,0:T(8,128)(2,1)S(1)}, u32[]{:S(2)}, u32[]{:S(2)}) collective-permute-start(bf16[16,32,128]{2,1,0:T(8,128)(2,1)} %get-tuple-element.39), channel_id=1, source_target_pairs={{0,4},{4,0},{8,12},{12,8},{16,20},{20,16},{24,28},{28,24},{1,5},{5... | collective-permute-start | bytes 393224 | tf_op jit(solution)/shard_map/ppermute | solution.py:297
  199.1 16.5 %collective-permute-start.8 = (bf16[16,32,128]{2,1,0:T(8,128)(2,1)}, bf16[16,32,128]{2,1,0:T(8,128)(2,1)S(1)}, u32[]{:S(2)}, u32[]{:S(2)}) collective-permute-start(bf16[16,32,128]{2,1,0:T(8,128)(2,1)} %get-tuple-element.40), channel_id=1, source_target_pairs={{0,8},{4,12},{8,16},{12,20},{16,24},{20,28},{24,0},{28,4},{1,9},{5... | collective-permute-start | bytes 393224 | tf_op jit(solution)/shard_map/ppermute | solution.py:297
  201.1 15.3 %collective-permute-start.9 = (bf16[16,32,128]{2,1,0:T(8,128)(2,1)}, bf16[16,32,128]{2,1,0:T(8,128)(2,1)S(1)}, u32[]{:S(2)}, u32[]{:S(2)}) collective-permute-start(bf16[16,32,128]{2,1,0:T(8,128)(2,1)} %get-tuple-element.41), channel_id=1, source_target_pairs={{0,12},{4,8},{8,20},{12,16},{16,28},{20,24},{24,4},{28,0},{1,13},{... | collective-permute-start | bytes 393224 | tf_op jit(solution)/shard_map/ppermute | solution.py:297
  203.4 33.9 %collective-permute-start.14 = (bf16[8,136,128]{2,1,0:T(8,128)(2,1)S(1)}, bf16[8,136,128]{2,1,0:T(8,128)(2,1)S(1)}, u32[]{:S(2)}, u32[]{:S(2)}) collective-permute-start(bf16[8,136,128]{2,1,0:T(8,128)(2,1)S(1)} %all-to-all-done.refs_0_), channel_id=1, source_target_pairs={{0,1},{1,2},{2,3},{3,0},{4,5},{5,6},{6,7},{7,4},{8,9},{9,10},{10,1... | collective-permute-start | bytes 835592 | tf_op jit(solution)/shard_map/ppermute | solution.py:281
  206.9 30.4 %collective-permute-start.15 = (bf16[8,136,128]{2,1,0:T(8,128)(2,1)S(1)}, bf16[8,136,128]{2,1,0:T(8,128)(2,1)S(1)}, u32[]{:S(2)}, u32[]{:S(2)}) collective-permute-start(bf16[8,136,128]{2,1,0:T(8,128)(2,1)S(1)} %all-to-all-done.refs_0_), channel_id=1, source_target_pairs={{0,2},{1,3},{2,0},{3,1},{4,6},{5,7},{6,4},{7,5},{8,10},{9,11},{10,... | collective-permute-start | bytes 835592 | tf_op jit(solution)/shard_map/ppermute | solution.py:281
  212.4 24.9 %collective-permute-start.16 = (bf16[8,136,128]{2,1,0:T(8,128)(2,1)S(1)}, bf16[8,136,128]{2,1,0:T(8,128)(2,1)S(1)}, u32[]{:S(2)}, u32[]{:S(2)}) collective-permute-start(bf16[8,136,128]{2,1,0:T(8,128)(2,1)S(1)} %all-to-all-done.refs_0_), channel_id=1, source_target_pairs={{0,3},{1,0},{2,1},{3,2},{4,7},{5,4},{6,5},{7,6},{8,11},{9,8},{10,9... | collective-permute-start | bytes 835592 | tf_op jit(solution)/shard_map/ppermute | solution.py:281
  239.2 45.0 %all-to-all-start.4 = ((bf16[16,160,128]{2,1,0:T(8,128)(2,1)}), bf16[16,160,128]{2,1,0:T(8,128)(2,1)S(1)}, u32[]{:S(2)}, u32[]{:S(2)}) async-start(bf16[16,160,128]{2,1,0:T(8,128)(2,1)} %shard_map.110), calls=%async_computation.4 | async-start | bytes 1310720 | tf_op jit(solution)/shard_map/all_to_all | solution.py:26
  249.6 35.4 %copy-start.14 = (f32[4,32,128]{2,1,0:T(8,128)S(1)}, f32[4,32,128]{2,1,0:T(8,128)}, u32[]{:S(2)}) copy-start(f32[4,32,128]{2,1,0:T(8,128)} %copy-done.13) | copy-start | bytes 196612
  (13 other events, 34.8 us)

commit v4 on v3

--- a/solution.py
+++ b/solution.py
@@ -34,34 +34,66 @@
     return pl.BlockSpec(memory_space=pltpu.VMEM)
 
 
-def call(body, outs, ins, scratch=()):
+def hbm():
+    return pl.BlockSpec(memory_space=pltpu.HBM)
+
+
+SPECS = {"s": smem, "v": vmem, "h": hbm}
+
+
+def dma(n):
+    return pltpu.SemaphoreType.DMA((n,))
+
+
+def moves(pairs, sems):
+    copies = [pltpu.make_async_copy(a, b, sems.at[i]) for i, (a, b) in enumerate(pairs)]
+    for copy in copies:
+        copy.start()
+    return copies
+
+
+def call(body, outs, ins, scratch=(), mib=60, to="v"):
+    many = isinstance(outs, tuple)
+    kinds = [SPECS[t]() for t in (to if many else to[0])]
     return pl.pallas_call(
         body,
         out_shape=outs,
-        in_specs=[smem() if i == "s" else vmem() for i in ins],
-        out_specs=jax.tree.map(lambda _: vmem(), outs),
+        in_specs=[SPECS[i]() for i in ins],
+        out_specs=tuple(kinds) if many else kinds[0],
         scratch_shapes=list(scratch),
-        compiler_params=pltpu.CompilerParams(vmem_limit_bytes=40 * 1024 * 1024),
+        compiler_params=pltpu.CompilerParams(vmem_limit_bytes=mib * 1024 * 1024),
     )
 
 
-def pick(nq, nz, asked, column, out):
-    per = column.shape[0] // nz
+def pick(nq, nz, asked, column, target, out, sems):
+    kblocks = column.shape[0] // nz
     for q in range(nq):
         for z in range(nz):
-            block = jnp.maximum(asked[q * nz + z] - 1, 0)
-            out[q * nz + z] = column[z * per + block]
-
-
-def pick_apart(nz, asked, peer, column, *outs):
+            block = jnp.maximum(asked[q * 2 * nz + z] - 1, 0)
+            out[q * nz + z] = column[z * kblocks + block]
+        part = slice(q * nz, (q + 1) * nz)
+        pltpu.make_async_copy(out.at[part], target.at[part], sems.at[q]).start()
+    for q in range(nq):
+        part = slice(q * nz, (q + 1) * nz)
+        pltpu.make_async_copy(out.at[part], target.at[part], sems.at[q]).wait()
+
+
+def pick_apart(nz, asked, ahead, column, other, *refs):
+    *targets, outs, sems = refs
     kblocks = column.shape[0] // nz
-    for d, out in enumerate(outs):
-        for z in range(nz):
-            block = jnp.maximum(asked[peer[d] * nz + z] - 1, 0)
-            out[z] = column[z * kblocks + block]
-
-
-def by_feature(nq, rows, chosen, here, features, out):
+    for s, target in enumerate(targets):
+        out = outs.at[s]
+        first = ahead[s] * 2 * nz
+        for i in range(2 * nz):
+            source = other if i >= nz else column
+            block = jnp.maximum(asked[first + i] - 1, 0)
+            out[i] = source[i % nz * kblocks + block]
+        pltpu.make_async_copy(out, target, sems.at[s]).start()
+    for s, target in enumerate(targets):
+        pltpu.make_async_copy(outs.at[s], target, sems.at[s]).wait()
+
+
+def by_feature(nq, nz, rows, chosen, here, features, out):
     tok, cols = features.shape
     kblocks = tok // KB
     for i in range(cols // HD):
@@ -79,7 +111,9 @@
         c = chosen[e]
         owner = c // kblocks
         place = jnp.where(owner != here[0], (owner % nq) * HD + owner // nq, -1)
-        wanted = jnp.where(at == place, (c % kblocks + 1).astype(F32), wanted)
+        pair = jnp.where(owner != here[0], (owner % nq ^ 1) * HD + nz + owner // nq, -1)
+        block = (c % kblocks + 1).astype(F32)
+        wanted = jnp.where((at == place) | (at == pair), block, wanted)
     wanted = wanted.astype(BF16)
     for q in range(nq):
         out[q, cols // nq :] = jnp.broadcast_to(wanted[q : q + 1], (SUB, HD))
@@ -99,11 +133,11 @@
     for e, (_, remote, place, within) in enumerate(slots):
         near = own[within]
         if isinstance(got, tuple):
-            nz = got[0].shape[0]
-            d, z = place // nz, place % nz
-            block = got[0][z]
+            size = got[0].shape[0]
+            step, at = place // size, place % size
+            block = got[0][at]
             for i in range(1, len(got)):
-                block = jnp.where(d == i, got[i][z], block)
+                block = jnp.where(step == i, got[i][at], block)
         else:
             block = got[jnp.where(remote, place, 0)]
         out[e * KB : (e + 1) * KB] = jnp.where(remote, block, near)
@@ -155,7 +189,7 @@
         own_sum[k] = total[peers + k]
 
 
-def value_terms(nq, nz, chosen, here, queries, dout, lse, got_k, own_k, send, own_sum, sel, kpos, low, rows, total, part):
+def value_terms(nq, nz, chosen, here, queries, dout, lse, got_k, own_k, target, own_sum, sel, kpos, low, rows, total, part, send, sems):
     peers, kblocks = nq * nz, own_k.shape[0]
     qblocks, pairs = queries.shape[0] // QB, queries.shape[1] // HD // 2
     slots = [slots_of(chosen, here[0], b, nq, nz, kblocks, lambda q: q) for b in range(qblocks)]
@@ -170,13 +204,18 @@
             rows[p * HD : (p + 1) * HD] = heads_of(dout, b, p)
         part[b] = jnp.dot(low[...], rows[...], preferred_element_type=F32)
     scatter(slots, [part.at[b] for b in range(qblocks)], total, send, own_sum, peers, kblocks)
+    for copy in moves([(send, target)], sems):
+        copy.wait()
 
 
 def key_terms(nx, nc, nz, chosen, here, queries, dout, lse, got_k, own_k, own_v, *refs):
     nq = nx * nc
-    got_v, refs = refs[:nq], refs[nq:]
-    sends, refs = refs[:nq], refs[nq:]
-    own_sum, low, sel, sel_v, kpos, rows, total, part, send = refs
+    far_v, refs = refs[:nx], refs[nx:]
+    targets, refs = refs[:nx], refs[nx:]
+    own_sum, low, sel, sel_v, kpos, rows, total, part, send, held, sems = refs
+    got_v = tuple(held.at[s] for s in range(nx))
+    for copy in moves(list(zip(far_v, got_v)), sems):
+        copy.wait()
     peers, kblocks = nq * nz, own_k.shape[0]
     qblocks, pairs = queries.shape[0] // QB, queries.shape[1] // HD // 2
     mine = here[0] % nq
@@ -205,8 +244,10 @@
         part[b] = jnp.dot(low[b], rows[...], preferred_element_type=F32) * SCALE
     back = [slots(b, ahead) for b in range(qblocks)]
     scatter(back, [part.at[b] for b in range(qblocks)], total, send, own_sum, peers, kblocks)
-    for d, out in enumerate(sends):
-        out[...] = send[d * nz : (d + 1) * nz]
+    size = nc * nz
+    ends = [(send.at[s * size : (s + 1) * size], to) for s, to in enumerate(targets)]
+    for copy in moves(ends, sems):
+        copy.wait()
 
 
 def query_terms(low, sel, out):
@@ -221,21 +262,40 @@
                 )
 
 
-def gather_home(nq, nz, asked, peer, *refs):
-    *came, dense, total = refs
+def gather_home(nq, nz, asked, came, dense, total):
     blocks = dense.shape[0]
     kblocks = blocks // nz
     total[...] = jnp.zeros_like(total)
     for q in range(nq):
         for z in range(nz):
-            a = asked[peer[q] * nz + z]
+            a = asked[q * 2 * nz + z]
             at = jnp.where(a > 0, z * kblocks + a - 1, blocks)
-            piece = came[0][q * nz + z] if len(came) == 1 else came[q][z]
-            total[at] = total[at] + piece.astype(F32)
+            total[at] = total[at] + came[q * nz + z].astype(F32)
     dense[...] = total[0:blocks].astype(BF16)
 
 
-def weight_terms(rows_out, low, dense, *refs):
+def gather_both(nz, asked, behind, *refs):
+    *sent, dense, target, total, came, other, sems = refs
+    copies = moves([(a, came.at[s]) for s, a in enumerate(sent)], sems)
+    blocks = dense.shape[0]
+    kblocks = blocks // nz
+    total[...] = jnp.zeros_like(total)
+    for s, copy in enumerate(copies):
+        copy.wait()
+        part = came.at[s]
+        first = behind[s] * 2 * nz
+        for i in range(2 * nz):
+            a = asked[first + i]
+            at = jnp.where(a > 0, i * kblocks + a - 1, 2 * blocks)
+            total[at] = total[at] + part[i].astype(F32)
+    other[...] = total[blocks : 2 * blocks].astype(BF16)
+    copies = moves([(other, target)], sems)
+    dense[...] = total[0:blocks]
+    for copy in copies:
+        copy.wait()
+
+
+def weight_terms(rows_out, low, dense, other, *refs):
     *features, order, out = refs
     nq, nz, tok = low.shape[0], dense.shape[0], dense.shape[1]
     mine = nz // len(features)
@@ -247,7 +307,7 @@
         total = total.astype(BF16)
         for a in range(mine):
             out[order[k] * mine + a, tok:] = total[a * rows_out : (a + 1) * rows_out]
-    out[:, 0:tok] = dense[...]
+    out[:, 0:tok] = (dense[...] + other[...].astype(F32)).astype(BF16)
 
 
 def local(queries, keys, values, logsum, out_grad, normed_input, chosen):
@@ -270,50 +330,58 @@
     mine = nz // tp
     feats = mine * rows_out
     split = call(
-        functools.partial(by_feature, nq, rows_out),
+        functools.partial(by_feature, nq, nz, rows_out),
         shape((nq, feats + SUB, tok), BF16),
         "ssv",
     )(names, me, normed_input)
     split = to_peers(split, XC)
-    asked = split[:, feats, :nz].astype(jnp.int32).reshape(peers)
+    asked = split[:, feats, : 2 * nz].astype(jnp.int32).reshape(2 * peers)
     planes = [split]
     for k in range(1, tp):
         planes.append(lax.ppermute(planes[0], "tp", [(i, (i + k) % tp) for i in range(tp)]))
     order = ((lax.axis_index("tp") - jnp.arange(tp)) % tp).astype(jnp.int32)
     nx, nc = lax.axis_size("x"), lax.axis_size("c")
-    steps, other = jnp.arange(nq) // nc, jnp.arange(nq) % nc
+    steps = jnp.arange(nx)
     my_x, my_c = lax.axis_index("x"), lax.axis_index("c")
-    ahead = ((my_x + steps) % nx * nc + (my_c + other) % nc).astype(jnp.int32)
-    behind = ((my_x - steps) % nx * nc + (my_c + other) % nc).astype(jnp.int32)
-    direct = jnp.arange(nq, dtype=jnp.int32)
+    ahead = ((my_x + steps) % nx * nc + my_c).astype(jnp.int32)
+    behind = ((my_x - steps) % nx * nc + my_c).astype(jnp.int32)
 
     def around(pieces):
-        came = [pieces[0]]
-        for d in range(1, nq):
-            s, r = d // nc, d % nc
-            pairs = [
-                (x * nc + c, (x + s) % nx * nc + (c + r) % nc) for x in range(nx) for c in range(nc)
-            ]
-            came.append(lax.ppermute(pieces[d], XC, pairs))
-        return came
+        turns = [[(x, (x + s) % nx) for x in range(nx)] for s in range(nx)]
+        return [pieces[0]] + [lax.ppermute(pieces[s], "x", turns[s]) for s in range(1, nx)]
+
+    def swapped(rows):
+        return lax.ppermute(rows, "c", [(0, 1), (1, 0)])
 
     def column(rows):
         return lax.all_gather(rows, "z", axis=0, tiled=True).reshape(nz * kblocks, KB, HD)
 
     column_k = column(keys)
-    sent = call(functools.partial(pick, nq, nz), shape((peers, KB, HD), BF16), "sv")(
-        asked, column_k
-    )
+    sent = call(
+        functools.partial(pick, nq, nz),
+        shape((peers, KB, HD), BF16),
+        "sv",
+        [pltpu.VMEM((peers, KB, HD), BF16), dma(nq)],
+        to="h",
+    )(asked, column_k)
     got_k = to_peers(sent.reshape(nq, nz * KB, HD), XC).reshape(peers, KB, HD)
     column_v = column(values)
-    slab = shape((nz, KB, HD), BF16)
-    sent = call(functools.partial(pick_apart, nz), (slab,) * nq, "ssv")(asked, ahead, column_v)
+    other_v = swapped(column_v)
+    slab = shape((nc * nz, KB, HD), BF16)
+    sent = call(
+        functools.partial(pick_apart, nz),
+        (slab,) * nx,
+        "ssvv",
+        [pltpu.VMEM((nx, nc * nz, KB, HD), BF16), dma(nx)],
+        to="h" * nx,
+    )(asked, ahead, column_v, other_v)
     got_v = around(sent)
 
     own_k = keys.reshape(kblocks, KB, HD)
     own_v = values.reshape(kblocks, KB, HD)
     lse = logsum.reshape(qblocks, QB, heads).transpose(0, 2, 1).reshape(qblocks * heads // 2, 2 * QB)
     terms = (shape((peers, KB, HD), BF16), shape((kblocks, KB, HD), F32))
+    slots = pltpu.VMEM((peers, KB, HD), BF16)
     work = [
         pltpu.VMEM((span, HD), jnp.int32),
         pltpu.VMEM((heads * QB, HD), BF16),
@@ -321,46 +389,65 @@
         pltpu.VMEM((qblocks, span, HD), F32),
     ]
 
-    def home(came, peer):
-        return call(
-            functools.partial(gather_home, nq, nz),
-            shape((nz * kblocks, KB, HD), BF16),
-            "ss" + "v" * len(came),
-            [pltpu.VMEM((nz * kblocks + 1, KB, HD), F32)],
-        )(asked, peer, *came).reshape(nz, tok, HD)
-
     sent_v, mine_v = call(
         functools.partial(value_terms, nq, nz),
         terms,
         "ssvvvvv",
-        [pltpu.VMEM((span, HD), BF16), work[0], pltpu.VMEM((span, heads * QB), BF16), *work[1:]],
+        [pltpu.VMEM((span, HD), BF16), work[0], pltpu.VMEM((span, heads * QB), BF16), *work[1:], slots, dma(1)],
+        to="hv",
     )(names, me, queries, out_grad, lse, got_k, own_k)
     came_v = to_peers(sent_v.reshape(nq, nz * KB, HD), XC).reshape(peers, KB, HD)
-    dense_v = home([came_v], direct)
+    dense_v = call(
+        functools.partial(gather_home, nq, nz),
+        shape((nz * kblocks, KB, HD), BF16),
+        "sv",
+        [pltpu.VMEM((nz * kblocks + 1, KB, HD), F32)],
+        6,
+    )(asked, came_v).reshape(nz, tok, HD)
     sums_v = to_peers(dense_v, "z")
     value_grad = mine_v.reshape(tok, HD) + jnp.sum(sums_v.astype(F32), axis=0)
 
     *sent_k, mine_k, low, sel = call(
         functools.partial(key_terms, nx, nc, nz),
         (
-            *(slab,) * nq,
+            *(slab,) * nx,
             terms[1],
             shape((qblocks, span, heads * QB), BF16),
             shape((qblocks, span, HD), BF16),
         ),
-        "ss" + "v" * (6 + nq),
-        [pltpu.VMEM((span, HD), BF16), *work, pltpu.VMEM((peers, KB, HD), BF16)],
+        "ss" + "v" * 6 + "h" * nx,
+        [
+            *(pltpu.VMEM((span, HD), BF16), *work, slots),
+            *(pltpu.VMEM((nx, nc * nz, KB, HD), BF16), dma(nx)),
+        ],
+        to="h" * nx + "vvv",
     )(names, me, queries, out_grad, lse, got_k, own_k, own_v, *got_v)
     came_k = around(sent_k)
-    dense_k = home(came_k, behind)
+    blocks = (nz * kblocks, KB, HD)
+    dense_k, other_k = call(
+        functools.partial(gather_both, nz),
+        (shape(blocks, F32), shape(blocks, BF16)),
+        "ss" + "h" * nx,
+        [
+            pltpu.VMEM((2 * nz * kblocks + 1, KB, HD), F32),
+            pltpu.VMEM((nx, nc * nz, KB, HD), BF16),
+            pltpu.VMEM(blocks, BF16),
+            dma(nx),
+        ],
+        to="vh",
+    )(asked, behind, *came_k)
+    other_k = swapped(other_k)
     query_grad = call(query_terms, shape((tok, cols), F32), "vv")(low, sel)
 
     all_low = lax.all_gather(value_grad.astype(BF16), XC, axis=0)
     both = call(
         functools.partial(weight_terms, rows_out),
         shape((nz, tok + rows_out, HD), BF16),
-        "v" * (2 + tp) + "s",
-    )(all_low, dense_k, *planes, order)
+        "v" * (3 + tp) + "s",
+        mib=6,
+    )(
+        all_low, dense_k.reshape(nz, tok, HD), other_k.reshape(nz, tok, HD), *planes, order
+    )
     both = jnp.sum(to_peers(both, "z").astype(F32), axis=0)
     key_grad = mine_k.reshape(tok, HD) + both[:tok]
     return (query_grad, key_grad, value_grad, both[tok:])

time: 287 us -> 294 us (1.024)
  the two profiles are of different devices: /device:TPU:2 before, /device:TPU:32 now
where the time goes in v4:
time: 294 us; the launch traced here: 293 us
  blocking collectives  120 us (41%)
  waiting for transfers between devices  67.5 us (23%)
  starting transfers between devices  65 us (22%)
  Pallas kernels  30.2 us (10%)
  local copies, waits for them, and re-layouts  6.61 us (2%)
    all_gather x2, blocking collectives, column(): lax.all_gather(rows, 'z', axis=0, tiled=True).reshape(nz * kblocks, KB, HD)  87.8 us
    all_to_all x4, waiting for transfers between devices, to_peers(): return lax.all_to_all(parts, axis, split_axis=0, concat_axis=0, tiled=True)  46.6 us
    all_to_all x4, starting transfers between devices, to_peers(): return lax.all_to_all(parts, axis, split_axis=0, concat_axis=0, tiled=True)  30.4 us
    ppermute x6, waiting for transfers between devices, around(): lax.ppermute(pieces[s], 'x', turns[s])  19.6 us
    all_to_all x1, blocking collectives, to_peers(): return lax.all_to_all(parts, axis, split_axis=0, concat_axis=0, tiled=True)  19.4 us
    ppermute x6, starting transfers between devices, around(): lax.ppermute(pieces[s], 'x', turns[s])  19.1 us
    all_gather x1, blocking collectives, local(): all_low = lax.all_gather(value_grad.astype(BF16), XC, axis=0)  12.8 us
    ppermute x3, starting transfers between devices, local(): lax.ppermute(planes[0], 'tp', [(i, (i + k) % tp) for i in range(tp)])  11.6 us
  transfers between devices with their start and end apart: 15, of which 8 were waited for; matrix products, arithmetic and copies ran while one was open for 1% of the time, Pallas kernels for 6%

profile of v4, /device:TPU:32, one launch (start us, length us, event | category | flops | bytes accessed | tf_op | source)
XLA Modules:
  0.0 292.9 jit_solution(11913147988051016297)
XLA Ops:
  4.1 4.3 %all-to-all-start = ((bf16[8,136,128]{2,1,0:T(8,128)(2,1)}), bf16[8,136,128]{2,1,0:T(8,128)(2,1)S(1)}, u32[]{:S(2)}, u32[]{:S(2)}) async-start(bf16[8,136,128]{2,1,0:T(8,128)(2,1)} %shard_map.102), calls=%async_computation | async-start | bytes 557056 | tf_op jit(solution)/shard_map/all_to_all | solution.py:26
  8.4 38.5 %all_gather.10 = bf16[2048,128]{1,0:T(8,128)(2,1)} all-gather(bf16[128,128]{1,0:T(8,128)(2,1)S(1)} %copy-done.5), channel_id=1, replica_groups=mesh['z'=16,'x'=4,'c'=2,'tp'=4] {'z'}, dimensions={0}, use_global_device_ids=true | all-gather | bytes 557056 | tf_op jit(solution)/shard_map/all_gather | solution.py:357
  49.8 4.9 %all-to-all-start.1 = ((bf16[8,512,128]{2,1,0:T(8,128)(2,1)}), bf16[8,512,128]{2,1,0:T(8,128)(2,1)S(1)}, u32[]{:S(2)}, u32[]{:S(2)}) async-start(bf16[8,512,128]{2,1,0:T(8,128)(2,1)} %bitcast.33), calls=%async_computation.1 | async-start | bytes 2097152 | tf_op jit(solution)/shard_map/all_to_all | solution.py:26
  55.4 15.2 %all-to-all-done.1 = bf16[8,512,128]{2,1,0:T(8,128)(2,1)S(1)} async-done(((bf16[8,512,128]{2,1,0:T(8,128)(2,1)}), bf16[8,512,128]{2,1,0:T(8,128)(2,1)S(1)}, u32[]{:S(2)}, u32[]{:S(2)}) %all-to-all-start.1) | async-done | bytes 1048608 | tf_op jit(solution)/shard_map/all_to_all | solution.py:26
  71.6 4.5 %shard_map.107 = (bf16[128,32,128]{2,1,0:T(8,128)(2,1)}, f32[4,32,128]{2,1,0:T(8,128)}) custom-call(s32[32]{0:T(128)} %reshape.82.chosen, s32[1]{0:T(128)} %bitcast.here, bf16[128,1024]{1,0:T(8,128)(2,1)} %queries.3, bf16[128,1024]{1,0:T(8,128)(2,1)} %dout.3, f32[8,128]{1,0:T(8,128)} %reshape.85.lse, bf16[128,32,128]{2,1,0:T(8,128)(2,1)} %bitcast.31, ...), custom_call_target="tpu_custom_call" | custom-call | tf_op jit(solution)/shard_map/pallas_call | solution.py:392
  76.1 19.4 %all_to_all.25 = bf16[8,512,128]{2,1,0:T(8,128)(2,1)S(1)} all-to-all(bf16[8,512,128]{2,1,0:T(8,128)(2,1)} %bitcast.37), channel_id=1, replica_groups=mesh['z'=16,'x'=4,'c'=2,'tp'=4] {'x','c'}, dimensions={0} | all-to-all | bytes 2097152 | tf_op jit(solution)/shard_map/all_to_all | solution.py:26
  97.9 8.9 %all-to-all-start.3 = ((bf16[16,128,128]{2,1,0:T(8,128)(2,1)}), bf16[16,128,128]{2,1,0:T(8,128)(2,1)S(1)}, u32[]{:S(2)}, u32[]{:S(2)}) async-start(bf16[16,128,128]{2,1,0:T(8,128)(2,1)} %bitcast.12), calls=%async_computation.3 | async-start | bytes 1048576 | tf_op jit(solution)/shard_map/all_to_all | solution.py:26
  106.7 49.3 %all_gather.11 = bf16[2048,128]{1,0:T(8,128)(2,1)S(1)} all-gather(bf16[128,128]{1,0:T(8,128)(2,1)S(1)} %copy-done.13), channel_id=1, replica_groups=mesh['z'=16,'x'=4,'c'=2,'tp'=4] {'z'}, dimensions={0}, use_global_device_ids=true | all-gather | bytes 557056 | tf_op jit(solution)/shard_map/all_gather | solution.py:357
  163.0 2.5 collective-permute-start.1
  165.5 3.9 %collective-permute-start.2 = (bf16[32,32,128]{2,1,0:T(8,128)(2,1)}, bf16[32,32,128]{2,1,0:T(8,128)(2,1)S(1)}, u32[]{:S(2)}, u32[]{:S(2)}) collective-permute-start(bf16[32,32,128]{2,1,0:T(8,128)(2,1)} %get-tuple-element.21), channel_id=1, source_target_pairs={{0,16},{8,24},{16,0},{24,8},{1,17},{9,25},{17,1},{25,9},{2,18},{10... | collective-permute-start | bytes 786440 | tf_op jit(solution)/shard_map/ppermute | solution.py:351
  169.4 2.7 collective-permute-start.3
  172.2 8.1 %collective-permute-done.1.refs_1_ = bf16[32,32,128]{2,1,0:T(8,128)(2,1)S(1)} collective-permute-done((bf16[32,32,128]{2,1,0:T(8,128)(2,1)}, bf16[32,32,128]{2,1,0:T(8,128)(2,1)S(1)}, u32[]{:S(2)}, u32[]{:S(2)}) %collective-permute-start.1) | collective-permute-done | bytes 262176 | tf_op jit(solution)/shard_map/ppermute | solution.py:351
  180.2 2.5 collective-permute-done.3.refs_3_
  183.5 8.0 %shard_map.105 = (bf16[32,32,128]{2,1,0:T(8,128)(2,1)}, bf16[32,32,128]{2,1,0:T(8,128)(2,1)}, bf16[32,32,128]{2,1,0:T(8,128)(2,1)}, bf16[32,32,128]{2,1,0:T(8,12...) custom-call(s32[32]{0:T(128)} %reshape.82.chosen, s32[1]{0:T(128)} %bitcast.here, ...), custom_call_target="tpu_custom_call" | custom-call | tf_op jit(solution)/shard_map/pallas_call | solution.py:410
  193.8 5.7 %collective-permute-start.5 = (bf16[32,32,128]{2,1,0:T(8,128)(2,1)}, bf16[32,32,128]{2,1,0:T(8,128)(2,1)S(1)}, u32[]{:S(2)}, u32[]{:S(2)}) collective-permute-start(bf16[32,32,128]{2,1,0:T(8,128)(2,1)} %get-tuple-element.30), channel_id=1, source_target_pairs={{0,16},{8,24},{16,0},{24,8},{1,17},{9,25},{17,1},{25,9},{2,18},{10... | collective-permute-start | bytes 786440 | tf_op jit(solution)/shard_map/ppermute | solution.py:351
  202.8 6.8 %collective-permute-done.5.refs_2_ = bf16[32,32,128]{2,1,0:T(8,128)(2,1)S(1)} collective-permute-done((bf16[32,32,128]{2,1,0:T(8,128)(2,1)}, bf16[32,32,128]{2,1,0:T(8,128)(2,1)S(1)}, u32[]{:S(2)}, u32[]{:S(2)}) %collective-permute-start.5) | collective-permute-done | bytes 262176 | tf_op jit(solution)/shard_map/ppermute | solution.py:351
  211.7 4.3 %shard_map.109 = (f32[64,32,128]{2,1,0:T(8,128)}, bf16[64,32,128]{2,1,0:T(8,128)(2,1)}) custom-call(s32[256]{0:T(256)} %reshape.100.asked, s32[4]{0:T(128)} %fusion.5.behind, bf16[32,32,128]{2,1,0:T(8,128)(2,1)} %get-tuple-element.28.refs_0_, bf16[32,32,128]{2,1,0:T(8,128)(2,1)} %copy-done.7, bf16[32,32,128]{2,1,0:T(8,128)(2,1)} %copy-done.9, ...), custom_call_target="tpu_custom_call" | custom-call | tf_op jit(solution)/shard_map/pallas_call | solution.py:427
  218.1 3.5 %collective-permute-start.8 = (bf16[8,136,128]{2,1,0:T(8,128)(2,1)S(1)}, bf16[8,136,128]{2,1,0:T(8,128)(2,1)S(1)}, u32[]{:S(2)}, u32[]{:S(2)}) collective-permute-start(bf16[8,136,128]{2,1,0:T(8,128)(2,1)S(1)} %all-to-all-done.refs_0_), channel_id=1, source_target_pairs={{0,1},{1,2},{2,3},{3,0},{4,5},{5,6},{6,7},{7,4},{8,9},{9,10},{10,1... | collective-permute-start | bytes 835592 | tf_op jit(solution)/shard_map/ppermute | solution.py:341
  221.6 4.8 %collective-permute-start.9 = (bf16[8,136,128]{2,1,0:T(8,128)(2,1)S(1)}, bf16[8,136,128]{2,1,0:T(8,128)(2,1)S(1)}, u32[]{:S(2)}, u32[]{:S(2)}) collective-permute-start(bf16[8,136,128]{2,1,0:T(8,128)(2,1)S(1)} %all-to-all-done.refs_0_), channel_id=1, source_target_pairs={{0,2},{1,3},{2,0},{3,1},{4,6},{5,7},{6,4},{7,5},{8,10},{9,11},{10,... | collective-permute-start | bytes 835592 | tf_op jit(solution)/shard_map/ppermute | solution.py:341
  226.4 3.3 %collective-permute-start.10 = (bf16[8,136,128]{2,1,0:T(8,128)(2,1)S(1)}, bf16[8,136,128]{2,1,0:T(8,128)(2,1)S(1)}, u32[]{:S(2)}, u32[]{:S(2)}) collective-permute-start(bf16[8,136,128]{2,1,0:T(8,128)(2,1)S(1)} %all-to-all-done.refs_0_), channel_id=1, source_target_pairs={{0,3},{1,0},{2,1},{3,2},{4,7},{5,4},{6,5},{7,6},{8,11},{9,8},{10,9... | collective-permute-start | bytes 835592 | tf_op jit(solution)/shard_map/ppermute | solution.py:341
  229.8 12.8 %all_gather.12.low = bf16[8,128,128]{2,1,0:T(8,128)(2,1)S(1)} all-gather(bf16[1,128,128]{2,1,0:T(8,128)(2,1)S(1)} %fusion), channel_id=1, replica_groups=mesh['z'=16,'x'=4,'c'=2,'tp'=4] {'x','c'}, dimensions={0}, use_global_device_ids=true | all-gather | bytes 294912 | tf_op jit(solution)/shard_map/all_gather | solution.py:442
  244.6 12.3 %all-to-all-start.4 = ((bf16[16,160,128]{2,1,0:T(8,128)(2,1)}), bf16[16,160,128]{2,1,0:T(8,128)(2,1)S(1)}, u32[]{:S(2)}, u32[]{:S(2)}) async-start(bf16[16,160,128]{2,1,0:T(8,128)(2,1)} %shard_map.110), calls=%async_computation.4 | async-start | bytes 1310720 | tf_op jit(solution)/shard_map/all_to_all | solution.py:26
  256.9 2.6 shard_map.106
  260.2 31.4 %all-to-all-done.4 = bf16[16,160,128]{2,1,0:T(8,128)(2,1)S(1)} async-done(((bf16[16,160,128]{2,1,0:T(8,128)(2,1)}), bf16[16,160,128]{2,1,0:T(8,128)(2,1)S(1)}, u32[]{:S(2)}, u32[]{:S(2)}) %all-to-all-start.4) | async-done | bytes 655392 | tf_op jit(solution)/shard_map/all_to_all | solution.py:26
  (66 shorter events, 31.7 us)
Async XLA Ops:
  0.6 7.8 %copy-start.5 = (bf16[128,128]{1,0:T(8,128)(2,1)S(1)}, bf16[128,128]{1,0:T(8,128)(2,1)}, u32[]{:S(2)}) copy-start(bf16[128,128]{1,0:T(8,128)(2,1)} %param.8) | copy-start | bytes 98308
  4.1 42.8 %all-to-all-start = ((bf16[8,136,128]{2,1,0:T(8,128)(2,1)}), bf16[8,136,128]{2,1,0:T(8,128)(2,1)S(1)}, u32[]{:S(2)}, u32[]{:S(2)}) async-start(bf16[8,136,128]{2,1,0:T(8,128)(2,1)} %shard_map.102), calls=%async_computation | async-start | bytes 557056 | tf_op jit(solution)/shard_map/all_to_all | solution.py:26
  49.8 4.9 %copy-start.15 = (f32[128,8]{0,1:T(8,128)S(1)}, f32[128,8]{0,1:T(8,128)}, u32[]{:S(2)}) copy-start(f32[128,8]{0,1:T(8,128)} %param.10) | copy-start | bytes 12292
  49.8 20.8 %all-to-all-start.1 = ((bf16[8,512,128]{2,1,0:T(8,128)(2,1)}), bf16[8,512,128]{2,1,0:T(8,128)(2,1)S(1)}, u32[]{:S(2)}, u32[]{:S(2)}) async-start(bf16[8,512,128]{2,1,0:T(8,128)(2,1)} %bitcast.33), calls=%async_computation.1 | async-start | bytes 2097152 | tf_op jit(solution)/shard_map/all_to_all | solution.py:26
  76.1 19.5 %copy-start.1 = (s32[256]{0:T(256)S(1)}, s32[256]{0:T(256)}, u32[]{:S(2)}) copy-start(s32[256]{0:T(256)} %reshape.100.asked) | copy-start | bytes 3076
  95.6 11.1 %copy-start.13 = (bf16[128,128]{1,0:T(8,128)(2,1)S(1)}, bf16[128,128]{1,0:T(8,128)(2,1)}, u32[]{:S(2)}) copy-start(bf16[128,128]{1,0:T(8,128)(2,1)} %param.9) | copy-start | bytes 98308
  97.9 131.8 %all-to-all-start.3 = ((bf16[16,128,128]{2,1,0:T(8,128)(2,1)}), bf16[16,128,128]{2,1,0:T(8,128)(2,1)S(1)}, u32[]{:S(2)}, u32[]{:S(2)}) async-start(bf16[16,128,128]{2,1,0:T(8,128)(2,1)} %bitcast.12), calls=%async_computation.3 | async-start | bytes 1048576 | tf_op jit(solution)/shard_map/all_to_all | solution.py:26
  156.0 3.8 %copy-start.3 = (bf16[2048,128]{1,0:T(8,128)(2,1)}, bf16[2048,128]{1,0:T(8,128)(2,1)S(1)}, u32[]{:S(2)}) copy-start(bf16[2048,128]{1,0:T(8,128)(2,1)S(1)} %all_gather.11) | copy-start | bytes 1572868
  156.0 3.8 %collective-permute-start = (bf16[64,32,128]{2,1,0:T(8,128)(2,1)S(1)}, bf16[64,32,128]{2,1,0:T(8,128)(2,1)S(1)}, u32[]{:S(2)}, u32[]{:S(2)}) collective-permute-start(bf16[64,32,128]{2,1,0:T(8,128)(2,1)S(1)} %bitcast.34), channel_id=1, source_target_pairs={{0,4},{4,0},{1,5},{5,1},{2,6},{6,2},{3,7},{7,3},{8,12},{12,8},{9,1... | collective-permute-start | bytes 1572872 | tf_op jit(solution)/shard_map/ppermute | solution.py:354
  163.0 17.3 %collective-permute-start.1 = (bf16[32,32,128]{2,1,0:T(8,128)(2,1)}, bf16[32,32,128]{2,1,0:T(8,128)(2,1)S(1)}, u32[]{:S(2)}, u32[]{:S(2)}) collective-permute-start(bf16[32,32,128]{2,1,0:T(8,128)(2,1)} %get-tuple-element.20), channel_id=1, source_target_pairs={{0,8},{8,16},{16,24},{24,0},{1,9},{9,17},{17,25},{25,1},{2,10},{10... | collective-permute-start | bytes 786440 | tf_op jit(solution)/shard_map/ppermute | solution.py:351
  165.5 14.7 %collective-permute-start.2 = (bf16[32,32,128]{2,1,0:T(8,128)(2,1)}, bf16[32,32,128]{2,1,0:T(8,128)(2,1)S(1)}, u32[]{:S(2)}, u32[]{:S(2)}) collective-permute-start(bf16[32,32,128]{2,1,0:T(8,128)(2,1)} %get-tuple-element.21), channel_id=1, source_target_pairs={{0,16},{8,24},{16,0},{24,8},{1,17},{9,25},{17,1},{25,9},{2,18},{10... | collective-permute-start | bytes 786440 | tf_op jit(solution)/shard_map/ppermute | solution.py:351
  169.4 13.4 %collective-permute-start.3 = (bf16[32,32,128]{2,1,0:T(8,128)(2,1)}, bf16[32,32,128]{2,1,0:T(8,128)(2,1)S(1)}, u32[]{:S(2)}, u32[]{:S(2)}) collective-permute-start(bf16[32,32,128]{2,1,0:T(8,128)(2,1)} %get-tuple-element.22), channel_id=1, source_target_pairs={{0,24},{8,0},{16,8},{24,16},{1,25},{9,1},{17,9},{25,17},{2,26},{10... | collective-permute-start | bytes 786440 | tf_op jit(solution)/shard_map/ppermute | solution.py:351
  191.5 38.3 %copy-start.12 = (f32[4,32,128]{2,1,0:T(8,128)S(1)}, f32[4,32,128]{2,1,0:T(8,128)}, u32[]{:S(2)}) copy-start(f32[4,32,128]{2,1,0:T(8,128)} %get-tuple-element.26) | copy-start | bytes 196612
  191.5 11.4 %collective-permute-start.4 = (bf16[32,32,128]{2,1,0:T(8,128)(2,1)}, bf16[32,32,128]{2,1,0:T(8,128)(2,1)S(1)}, u32[]{:S(2)}, u32[]{:S(2)}) collective-permute-start(bf16[32,32,128]{2,1,0:T(8,128)(2,1)} %get-tuple-element.29), channel_id=1, source_target_pairs={{0,8},{8,16},{16,24},{24,0},{1,9},{9,17},{17,25},{25,1},{2,10},{10... | collective-permute-start | bytes 786440 | tf_op jit(solution)/shard_map/ppermute | solution.py:351
  193.8 15.8 %collective-permute-start.5 = (bf16[32,32,128]{2,1,0:T(8,128)(2,1)}, bf16[32,32,128]{2,1,0:T(8,128)(2,1)S(1)}, u32[]{:S(2)}, u32[]{:S(2)}) collective-permute-start(bf16[32,32,128]{2,1,0:T(8,128)(2,1)} %get-tuple-element.30), channel_id=1, source_target_pairs={{0,16},{8,24},{16,0},{24,8},{1,17},{9,25},{17,1},{25,9},{2,18},{10... | collective-permute-start | bytes 786440 | tf_op jit(solution)/shard_map/ppermute | solution.py:351
  199.5 11.4 %collective-permute-start.6 = (bf16[32,32,128]{2,1,0:T(8,128)(2,1)}, bf16[32,32,128]{2,1,0:T(8,128)(2,1)S(1)}, u32[]{:S(2)}, u32[]{:S(2)}) collective-permute-start(bf16[32,32,128]{2,1,0:T(8,128)(2,1)} %get-tuple-element.31), channel_id=1, source_target_pairs={{0,24},{8,0},{16,8},{24,16},{1,25},{9,1},{17,9},{25,17},{2,26},{10... | collective-permute-start | bytes 786440 | tf_op jit(solution)/shard_map/ppermute | solution.py:351
  202.8 8.1 %copy-start.7 = (bf16[32,32,128]{2,1,0:T(8,128)(2,1)}, bf16[32,32,128]{2,1,0:T(8,128)(2,1)S(1)}, u32[]{:S(2)}) copy-start(bf16[32,32,128]{2,1,0:T(8,128)(2,1)S(1)} %collective-permute-done.4.refs_1_) | copy-start | bytes 786436
  216.0 26.6 %copy-start = (f32[64,32,128]{2,1,0:T(8,128)S(1)}, f32[64,32,128]{2,1,0:T(8,128)}, u32[]{:S(2)}) copy-start(f32[64,32,128]{2,1,0:T(8,128)} %get-tuple-element.32) | copy-start | bytes 3145732
  216.0 26.6 %collective-permute-start.7 = (bf16[64,32,128]{2,1,0:T(8,128)(2,1)}, bf16[64,32,128]{2,1,0:T(8,128)(2,1)S(1)}, u32[]{:S(2)}, u32[]{:S(2)}) collective-permute-start(bf16[64,32,128]{2,1,0:T(8,128)(2,1)} %get-tuple-element.33), channel_id=1, source_target_pairs={{0,4},{4,0},{1,5},{5,1},{2,6},{6,2},{3,7},{7,3},{8,12},{12,8},{9,1... | collective-permute-start | bytes 1572872 | tf_op jit(solution)/shard_map/ppermute | solution.py:354
  218.1 24.5 %collective-permute-start.8 = (bf16[8,136,128]{2,1,0:T(8,128)(2,1)S(1)}, bf16[8,136,128]{2,1,0:T(8,128)(2,1)S(1)}, u32[]{:S(2)}, u32[]{:S(2)}) collective-permute-start(bf16[8,136,128]{2,1,0:T(8,128)(2,1)S(1)} %all-to-all-done.refs_0_), channel_id=1, source_target_pairs={{0,1},{1,2},{2,3},{3,0},{4,5},{5,6},{6,7},{7,4},{8,9},{9,10},{10,1... | collective-permute-start | bytes 835592 | tf_op jit(solution)/shard_map/ppermute | solution.py:341
  221.6 21.1 %collective-permute-start.9 = (bf16[8,136,128]{2,1,0:T(8,128)(2,1)S(1)}, bf16[8,136,128]{2,1,0:T(8,128)(2,1)S(1)}, u32[]{:S(2)}, u32[]{:S(2)}) collective-permute-start(bf16[8,136,128]{2,1,0:T(8,128)(2,1)S(1)} %all-to-all-done.refs_0_), channel_id=1, source_target_pairs={{0,2},{1,3},{2,0},{3,1},{4,6},{5,7},{6,4},{7,5},{8,10},{9,11},{10,... | collective-permute-start | bytes 835592 | tf_op jit(solution)/shard_map/ppermute | solution.py:341
  226.4 16.2 %collective-permute-start.10 = (bf16[8,136,128]{2,1,0:T(8,128)(2,1)S(1)}, bf16[8,136,128]{2,1,0:T(8,128)(2,1)S(1)}, u32[]{:S(2)}, u32[]{:S(2)}) collective-permute-start(bf16[8,136,128]{2,1,0:T(8,128)(2,1)S(1)} %all-to-all-done.refs_0_), channel_id=1, source_target_pairs={{0,3},{1,0},{2,1},{3,2},{4,7},{5,4},{6,5},{7,6},{8,11},{9,8},{10,9... | collective-permute-start | bytes 835592 | tf_op jit(solution)/shard_map/ppermute | solution.py:341
  244.6 46.9 %all-to-all-start.4 = ((bf16[16,160,128]{2,1,0:T(8,128)(2,1)}), bf16[16,160,128]{2,1,0:T(8,128)(2,1)S(1)}, u32[]{:S(2)}, u32[]{:S(2)}) async-start(bf16[16,160,128]{2,1,0:T(8,128)(2,1)} %shard_map.110), calls=%async_computation.4 | async-start | bytes 1310720 | tf_op jit(solution)/shard_map/all_to_all | solution.py:26
  256.9 35.3 %copy-start.14 = (f32[4,32,128]{2,1,0:T(8,128)S(1)}, f32[4,32,128]{2,1,0:T(8,128)}, u32[]{:S(2)}) copy-start(f32[4,32,128]{2,1,0:T(8,128)} %get-tuple-element.25) | copy-start | bytes 196612
  (7 other events, 9.7 us)

commit v5 on v4

--- a/solution.py
+++ b/solution.py
@@ -69,7 +69,7 @@
     kblocks = column.shape[0] // nz
     for q in range(nq):
         for z in range(nz):
-            block = jnp.maximum(asked[q * 2 * nz + z] - 1, 0)
+            block = jnp.maximum(asked[q, z] - 1, 0)
             out[q * nz + z] = column[z * kblocks + block]
         part = slice(q * nz, (q + 1) * nz)
         pltpu.make_async_copy(out.at[part], target.at[part], sems.at[q]).start()
@@ -78,15 +78,21 @@
         pltpu.make_async_copy(out.at[part], target.at[part], sems.at[q]).wait()
 
 
-def pick_apart(nz, asked, ahead, column, other, *refs):
+def across(here, s, nx, nc):
+    mine = here % (nx * nc)
+    return (mine // nc + s + nx) % nx * nc + mine % nc
+
+
+def pick_apart(nc, nz, asked, here, column, other, *refs):
     *targets, outs, sems = refs
+    nx = len(targets)
     kblocks = column.shape[0] // nz
     for s, target in enumerate(targets):
         out = outs.at[s]
-        first = ahead[s] * 2 * nz
+        peer = across(here[0], s, nx, nc)
         for i in range(2 * nz):
             source = other if i >= nz else column
-            block = jnp.maximum(asked[first + i] - 1, 0)
+            block = jnp.maximum(asked[peer, i] - 1, 0)
             out[i] = source[i % nz * kblocks + block]
         pltpu.make_async_copy(out, target, sems.at[s]).start()
     for s, target in enumerate(targets):
@@ -107,8 +113,8 @@
         jnp.int32, (nq, HD), 1
     )
     wanted = jnp.zeros((nq, HD), F32)
-    for e in range(chosen.shape[0]):
-        c = chosen[e]
+    for e in range(chosen.shape[0] * NSEL):
+        c = chosen[e // NSEL, e % NSEL]
         owner = c // kblocks
         place = jnp.where(owner != here[0], (owner % nq) * HD + owner // nq, -1)
         pair = jnp.where(owner != here[0], (owner % nq ^ 1) * HD + nz + owner // nq, -1)
@@ -122,7 +128,7 @@
 def slots_of(chosen, here, b, nq, nz, kblocks, where):
     slots = []
     for e in range(NSEL):
-        c = chosen[b * NSEL + e]
+        c = chosen[b, e]
         owner = c // kblocks
         place = where(owner % nq) * nz + owner // nq
         slots.append((c, owner != here, place, c % kblocks))
@@ -157,10 +163,13 @@
         kpos[e * KB : (e + 1) * KB] = c * KB + rows - lanes
 
 
-def prob_of(sel, pair, lse, kpos, start, b, p, pairs):
+def prob_of(sel, pair, lse, kpos, start, b, p):
     scores = lax.dot_general(sel[...], pair, NT, preferred_element_type=F32) * SCALE
-    at = b * pairs + p
-    return jnp.where(kpos[...] <= start, jnp.exp(scores - lse[at : at + 1, :]), 0.0)
+    turned = pltpu.roll(lse[...], QB, 1)
+    left, right = (turned, lse[...]) if b else (lse[...], turned)
+    first = lax.broadcasted_iota(jnp.int32, (1, HD), 1) < QB
+    row = jnp.where(first, left[2 * p : 2 * p + 1], right[2 * p + 1 : 2 * p + 2])
+    return jnp.where(kpos[...] <= start, jnp.exp(scores - row), 0.0)
 
 
 def scatter(slots, parts, total, send, own_sum, peers, kblocks):
@@ -199,7 +208,7 @@
         start = here[0] * queries.shape[0] + b * QB
         for p in range(pairs):
             pair = heads_of(queries, b, p)
-            prob = prob_of(sel, pair, lse, kpos, start, b, p, pairs)
+            prob = prob_of(sel, pair, lse, kpos, start, b, p)
             low[:, p * HD : (p + 1) * HD] = prob.astype(BF16)
             rows[p * HD : (p + 1) * HD] = heads_of(dout, b, p)
         part[b] = jnp.dot(low[...], rows[...], preferred_element_type=F32)
@@ -208,13 +217,13 @@
         copy.wait()
 
 
-def key_terms(nx, nc, nz, chosen, here, queries, dout, lse, got_k, own_k, own_v, *refs):
+def key_terms(nx, nc, nz, chosen, here, lse, own_k, own_v, *refs):
     nq = nx * nc
-    far_v, refs = refs[:nx], refs[nx:]
+    ins, refs = refs[: 3 + nx], refs[3 + nx :]
     targets, refs = refs[:nx], refs[nx:]
-    own_sum, low, sel, sel_v, kpos, rows, total, part, send, held, sems = refs
+    own_sum, low, sel, sel_v, kpos, rows, total, part, send, held, queries, dout, got_k, sems = refs
     got_v = tuple(held.at[s] for s in range(nx))
-    for copy in moves(list(zip(far_v, got_v)), sems):
+    for copy in moves(list(zip(ins, (queries, dout, got_k, *got_v))), sems):
         copy.wait()
     peers, kblocks = nq * nz, own_k.shape[0]
     qblocks, pairs = queries.shape[0] // QB, queries.shape[1] // HD // 2
@@ -236,7 +245,7 @@
         start = here[0] * queries.shape[0] + b * QB
         for p in range(pairs):
             pair = heads_of(queries, b, p)
-            prob = prob_of(sel.at[b], pair, lse, kpos, start, b, p, pairs)
+            prob = prob_of(sel.at[b], pair, lse, kpos, start, b, p)
             dprob = lax.dot_general(sel_v[...], heads_of(dout, b, p), NT, preferred_element_type=F32)
             delta = jnp.sum(prob * dprob, axis=0, keepdims=True)
             low[b, :, p * HD : (p + 1) * HD] = (prob * (dprob - delta)).astype(BF16)
@@ -268,13 +277,13 @@
     total[...] = jnp.zeros_like(total)
     for q in range(nq):
         for z in range(nz):
-            a = asked[q * 2 * nz + z]
+            a = asked[q, z]
             at = jnp.where(a > 0, z * kblocks + a - 1, blocks)
             total[at] = total[at] + came[q * nz + z].astype(F32)
     dense[...] = total[0:blocks].astype(BF16)
 
 
-def gather_both(nz, asked, behind, *refs):
+def gather_both(nc, nz, asked, here, *refs):
     *sent, dense, target, total, came, other, sems = refs
     copies = moves([(a, came.at[s]) for s, a in enumerate(sent)], sems)
     blocks = dense.shape[0]
@@ -283,9 +292,9 @@
     for s, copy in enumerate(copies):
         copy.wait()
         part = came.at[s]
-        first = behind[s] * 2 * nz
+        peer = across(here[0], -s, len(sent), nc)
         for i in range(2 * nz):
-            a = asked[first + i]
+            a = asked[peer, i]
             at = jnp.where(a > 0, i * kblocks + a - 1, 2 * blocks)
             total[at] = total[at] + part[i].astype(F32)
     other[...] = total[blocks : 2 * blocks].astype(BF16)
@@ -298,9 +307,9 @@
 def weight_terms(rows_out, low, dense, other, *refs):
     *features, order, out = refs
     nq, nz, tok = low.shape[0], dense.shape[0], dense.shape[1]
-    mine = nz // len(features)
+    mine = nz // (2 * len(features))
     feats = mine * rows_out
-    for k, block in enumerate(features):
+    for k, block in enumerate(f.at[i] for f in features for i in range(2)):
         total = jnp.dot(block[0, 0:feats], low[0], preferred_element_type=F32)
         for q in range(1, nq):
             total = total + jnp.dot(block[q, 0:feats], low[q], preferred_element_type=F32)
@@ -323,7 +332,7 @@
     peers = nq * nz
     shape = jax.ShapeDtypeStruct
 
-    names = chosen.reshape(qblocks * NSEL)
+    names = chosen
     me = here.reshape(1).astype(jnp.int32)
 
     rows_out = normed_input.shape[1] * tp // peers
@@ -335,16 +344,20 @@
         "ssv",
     )(names, me, normed_input)
     split = to_peers(split, XC)
-    asked = split[:, feats, : 2 * nz].astype(jnp.int32).reshape(2 * peers)
-    planes = [split]
-    for k in range(1, tp):
-        planes.append(lax.ppermute(planes[0], "tp", [(i, (i + k) % tp) for i in range(tp)]))
-    order = ((lax.axis_index("tp") - jnp.arange(tp)) % tp).astype(jnp.int32)
+    asked = split[:, feats, : 2 * nz].astype(jnp.int32)
+    pairs = [(i, i ^ 1) for i in range(tp)]
+    cross = [(i, (i + 1 if i % 2 else i - 1) % tp) for i in range(tp)]
+    my_t = lax.axis_index("tp")
+    near = lax.ppermute(split, "tp", pairs)
+    held = jnp.stack([split, near])
+    names_of = jnp.stack([my_t, my_t ^ 1])
+    planes, order = [held], [names_of]
+    if tp > 2:
+        planes.append(lax.ppermute(held, "tp", cross))
+        over = jnp.where(my_t % 2 == 1, my_t + 1, my_t - 1 + tp) % tp
+        order.append(jnp.stack([over, over ^ 1]))
+    order = jnp.concatenate(order).astype(jnp.int32)
     nx, nc = lax.axis_size("x"), lax.axis_size("c")
-    steps = jnp.arange(nx)
-    my_x, my_c = lax.axis_index("x"), lax.axis_index("c")
-    ahead = ((my_x + steps) % nx * nc + my_c).astype(jnp.int32)
-    behind = ((my_x - steps) % nx * nc + my_c).astype(jnp.int32)
 
     def around(pieces):
         turns = [[(x, (x + s) % nx) for x in range(nx)] for s in range(nx)]
@@ -369,19 +382,20 @@
     other_v = swapped(column_v)
     slab = shape((nc * nz, KB, HD), BF16)
     sent = call(
-        functools.partial(pick_apart, nz),
+        functools.partial(pick_apart, nc, nz),
         (slab,) * nx,
         "ssvv",
         [pltpu.VMEM((nx, nc * nz, KB, HD), BF16), dma(nx)],
         to="h" * nx,
-    )(asked, ahead, column_v, other_v)
+    )(asked, me, column_v, other_v)
     got_v = around(sent)
 
     own_k = keys.reshape(kblocks, KB, HD)
     own_v = values.reshape(kblocks, KB, HD)
-    lse = logsum.reshape(qblocks, QB, heads).transpose(0, 2, 1).reshape(qblocks * heads // 2, 2 * QB)
+    lse = logsum.T
     terms = (shape((peers, KB, HD), BF16), shape((kblocks, KB, HD), F32))
     slots = pltpu.VMEM((peers, KB, HD), BF16)
+    rows = pltpu.VMEM((tok, cols), BF16)
     work = [
         pltpu.VMEM((span, HD), jnp.int32),
         pltpu.VMEM((heads * QB, HD), BF16),
@@ -394,6 +408,7 @@
         terms,
         "ssvvvvv",
         [pltpu.VMEM((span, HD), BF16), work[0], pltpu.VMEM((span, heads * QB), BF16), *work[1:], slots, dma(1)],
+        mib=8,
         to="hv",
     )(names, me, queries, out_grad, lse, got_k, own_k)
     came_v = to_peers(sent_v.reshape(nq, nz * KB, HD), XC).reshape(peers, KB, HD)
@@ -415,17 +430,17 @@
             shape((qblocks, span, heads * QB), BF16),
             shape((qblocks, span, HD), BF16),
         ),
-        "ss" + "v" * 6 + "h" * nx,
+        "ssvvv" + "h" * (3 + nx),
         [
             *(pltpu.VMEM((span, HD), BF16), *work, slots),
-            *(pltpu.VMEM((nx, nc * nz, KB, HD), BF16), dma(nx)),
+            *(pltpu.VMEM((nx, nc * nz, KB, HD), BF16), rows, rows, slots, dma(3 + nx)),
         ],
         to="h" * nx + "vvv",
-    )(names, me, queries, out_grad, lse, got_k, own_k, own_v, *got_v)
+    )(names, me, lse, own_k, own_v, queries, out_grad, got_k, *got_v)
     came_k = around(sent_k)
     blocks = (nz * kblocks, KB, HD)
     dense_k, other_k = call(
-        functools.partial(gather_both, nz),
+        functools.partial(gather_both, nc, nz),
         (shape(blocks, F32), shape(blocks, BF16)),
         "ss" + "h" * nx,
         [
@@ -435,7 +450,7 @@
             dma(nx),
         ],
         to="vh",
-    )(asked, behind, *came_k)
+    )(asked, me, *came_k)
     other_k = swapped(other_k)
     query_grad = call(query_terms, shape((tok, cols), F32), "vv")(low, sel)
 
@@ -443,7 +458,7 @@
     both = call(
         functools.partial(weight_terms, rows_out),
         shape((nz, tok + rows_out, HD), BF16),
-        "v" * (3 + tp) + "s",
+        "v" * (3 + len(planes)) + "s",
         mib=6,
     )(
         all_low, dense_k.reshape(nz, tok, HD), other_k.reshape(nz, tok, HD), *planes, order

time: 294 us -> 277 us (0.942)
  the two profiles are of different devices: /device:TPU:32 before, /device:TPU:24 now
where the time goes in v5:
time: 277 us; the launch traced here: 276 us
  blocking collectives  144 us (52%)
  starting transfers between devices  49.3 us (18%)
  waiting for transfers between devices  48.6 us (18%)
  Pallas kernels  27.8 us (10%)
  local copies, waits for them, and re-layouts  3.5 us (1%)
    all_gather x2, blocking collectives, column(): lax.all_gather(rows, 'z', axis=0, tiled=True).reshape(nz * kblocks, KB, HD)  91.7 us
    all_to_all x2, blocking collectives, to_peers(): return lax.all_to_all(parts, axis, split_axis=0, concat_axis=0, tiled=True)  39.4 us
    all_to_all x3, waiting for transfers between devices, to_peers(): return lax.all_to_all(parts, axis, split_axis=0, concat_axis=0, tiled=True)  31.5 us
    all_to_all x3, starting transfers between devices, to_peers(): return lax.all_to_all(parts, axis, split_axis=0, concat_axis=0, tiled=True)  21.7 us
    ppermute x6, starting transfers between devices, around(): lax.ppermute(pieces[s], 'x', turns[s])  18.9 us
    ppermute x6, waiting for transfers between devices, around(): lax.ppermute(pieces[s], 'x', turns[s])  15.3 us
    all_gather x1, blocking collectives, local(): all_low = lax.all_gather(value_grad.astype(BF16), XC, axis=0)  12.8 us
    pallas_call x1, Pallas kernels, local(): call(functools.partial(key_terms, nx, nc, nz), (*(slab,) * nx, terms[1],...  7.88 us
  transfers between devices with their start and end apart: 13, of which 6 were waited for; matrix products, arithmetic and copies ran while one was open for 0% of the time, Pallas kernels for 6%

profile of v5, /device:TPU:24, one launch (start us, length us, event | category | flops | bytes accessed | tf_op | source)
XLA Modules:
  0.0 276.3 jit_solution(3198060453184773723)
XLA Ops:
  2.8 4.3 %all-to-all-start = ((bf16[8,136,128]{2,1,0:T(8,128)(2,1)}), bf16[8,136,128]{2,1,0:T(8,128)(2,1)S(1)}, u32[]{:S(2)}, u32[]{:S(2)}) async-start(bf16[8,136,128]{2,1,0:T(8,128)(2,1)} %shard_map.102), calls=%async_computation | async-start | bytes 557056 | tf_op jit(solution)/shard_map/all_to_all | solution.py:26
  7.1 40.5 %all_gather.10 = bf16[2048,128]{1,0:T(8,128)(2,1)} all-gather(bf16[128,128]{1,0:T(8,128)(2,1)S(1)} %copy-done.4), channel_id=1, replica_groups=mesh['z'=16,'x'=4,'c'=2,'tp'=4] {'z'}, dimensions={0}, use_global_device_ids=true | all-gather | bytes 557056 | tf_op jit(solution)/shard_map/all_gather | solution.py:370
  50.4 21.0 %all_to_all.25 = bf16[8,512,128]{2,1,0:T(8,128)(2,1)S(1)} all-to-all(bf16[8,512,128]{2,1,0:T(8,128)(2,1)} %bitcast.46), channel_id=1, replica_groups=mesh['z'=16,'x'=4,'c'=2,'tp'=4] {'x','c'}, dimensions={0} | all-to-all | bytes 2097152 | tf_op jit(solution)/shard_map/all_to_all | solution.py:26
  71.4 2.2 shard_map.107
  73.7 18.4 %all_to_all.26 = bf16[8,512,128]{2,1,0:T(8,128)(2,1)S(1)} all-to-all(bf16[8,512,128]{2,1,0:T(8,128)(2,1)S(1)} %bitcast.34), channel_id=1, replica_groups=mesh['z'=16,'x'=4,'c'=2,'tp'=4] {'x','c'}, dimensions={0} | all-to-all | bytes 2097152 | tf_op jit(solution)/shard_map/all_to_all | solution.py:26
  92.1 2.3 shard_map.108
  94.4 6.9 %all-to-all-start.3 = ((bf16[16,128,128]{2,1,0:T(8,128)(2,1)}), bf16[16,128,128]{2,1,0:T(8,128)(2,1)S(1)}, u32[]{:S(2)}, u32[]{:S(2)}) async-start(bf16[16,128,128]{2,1,0:T(8,128)(2,1)} %bitcast.13), calls=%async_computation.3 | async-start | bytes 1048576 | tf_op jit(solution)/shard_map/all_to_all | solution.py:26
  101.3 51.2 %all_gather.11 = bf16[2048,128]{1,0:T(8,128)(2,1)S(1)} all-gather(bf16[128,128]{1,0:T(8,128)(2,1)S(1)} %copy-done.18), channel_id=1, replica_groups=mesh['z'=16,'x'=4,'c'=2,'tp'=4] {'z'}, dimensions={0}, use_global_device_ids=true | all-gather | bytes 557056 | tf_op jit(solution)/shard_map/all_gather | solution.py:370
  157.0 2.3 shard_map.104
  159.4 2.6 collective-permute-start.1
  161.9 3.9 %collective-permute-start.2 = (bf16[32,32,128]{2,1,0:T(8,128)(2,1)}, bf16[32,32,128]{2,1,0:T(8,128)(2,1)S(1)}, u32[]{:S(2)}, u32[]{:S(2)}) collective-permute-start(bf16[32,32,128]{2,1,0:T(8,128)(2,1)} %get-tuple-element.21), channel_id=1, source_target_pairs={{0,16},{8,24},{16,0},{24,8},{1,17},{9,25},{17,1},{25,9},{2,18},{10... | collective-permute-start | bytes 786440 | tf_op jit(solution)/shard_map/ppermute | solution.py:364
  165.8 2.6 collective-permute-start.3
  168.5 2.7 collective-permute-start.8
  171.1 5.5 %collective-permute-done.1.refs_4_ = bf16[32,32,128]{2,1,0:T(8,128)(2,1)S(1)} collective-permute-done((bf16[32,32,128]{2,1,0:T(8,128)(2,1)}, bf16[32,32,128]{2,1,0:T(8,128)(2,1)S(1)}, u32[]{:S(2)}, u32[]{:S(2)}) %collective-permute-start.1) | collective-permute-done | bytes 262176 | tf_op jit(solution)/shard_map/ppermute | solution.py:364
  176.7 2.5 collective-permute-done.3.refs_6_
  179.9 7.9 %shard_map.105 = (bf16[32,32,128]{2,1,0:T(8,128)(2,1)}, bf16[32,32,128]{2,1,0:T(8,128)(2,1)}, bf16[32,32,128]{2,1,0:T(8,128)(2,1)}, bf16[32,32,128]{2,1,0:T(8,12...) custom-call(s32[2,16]{1,0:T(2,128)} %chosen.5, s32[1]{0:T(128)} %bitcast.here, ...), custom_call_target="tpu_custom_call" | custom-call | tf_op jit(solution)/shard_map/pallas_call | solution.py:425
  187.8 2.2 collective-permute-start.4
  190.0 5.7 %collective-permute-start.5 = (bf16[32,32,128]{2,1,0:T(8,128)(2,1)}, bf16[32,32,128]{2,1,0:T(8,128)(2,1)S(1)}, u32[]{:S(2)}, u32[]{:S(2)}) collective-permute-start(bf16[32,32,128]{2,1,0:T(8,128)(2,1)} %get-tuple-element.30), channel_id=1, source_target_pairs={{0,16},{8,24},{16,0},{24,8},{1,17},{9,25},{17,1},{25,9},{2,18},{10... | collective-permute-start | bytes 786440 | tf_op jit(solution)/shard_map/ppermute | solution.py:364
  199.9 5.9 %collective-permute-done.5.refs_2_ = bf16[32,32,128]{2,1,0:T(8,128)(2,1)S(1)} collective-permute-done((bf16[32,32,128]{2,1,0:T(8,128)(2,1)}, bf16[32,32,128]{2,1,0:T(8,128)(2,1)S(1)}, u32[]{:S(2)}, u32[]{:S(2)}) %collective-permute-start.5) | collective-permute-done | bytes 262176 | tf_op jit(solution)/shard_map/ppermute | solution.py:364
  207.8 4.3 %shard_map.109 = (f32[64,32,128]{2,1,0:T(8,128)}, bf16[64,32,128]{2,1,0:T(8,128)(2,1)}) custom-call(s32[8,32]{1,0:T(8,128)} %bitcast.42, s32[1]{0:T(128)} %bitcast.here, bf16[32,32,128]{2,1,0:T(8,128)(2,1)} %get-tuple-element.28.refs_0_, bf16[32,32,128]{2,1,0:T(8,128)(2,1)} %copy-done.12, bf16[32,32,128]{2,1,0:T(8,128)(2,1)} %copy-done.13, ...), custom_call_target="tpu_custom_call" | custom-call | tf_op jit(solution)/shard_map/pallas_call | solution.py:442
  215.0 12.8 %all_gather.12.low = bf16[8,128,128]{2,1,0:T(8,128)(2,1)S(1)} all-gather(bf16[1,128,128]{2,1,0:T(8,128)(2,1)S(1)} %fusion), channel_id=1, replica_groups=mesh['z'=16,'x'=4,'c'=2,'tp'=4] {'x','c'}, dimensions={0}, use_global_device_ids=true | all-gather | bytes 294912 | tf_op jit(solution)/shard_map/all_gather | solution.py:457
  229.8 10.5 %all-to-all-start.4 = ((bf16[16,160,128]{2,1,0:T(8,128)(2,1)}), bf16[16,160,128]{2,1,0:T(8,128)(2,1)S(1)}, u32[]{:S(2)}, u32[]{:S(2)}) async-start(bf16[16,160,128]{2,1,0:T(8,128)(2,1)} %shard_map.110), calls=%async_computation.4 | async-start | bytes 1310720 | tf_op jit(solution)/shard_map/all_to_all | solution.py:26
  240.3 2.6 shard_map.106
  243.6 31.4 %all-to-all-done.4 = bf16[16,160,128]{2,1,0:T(8,128)(2,1)S(1)} async-done(((bf16[16,160,128]{2,1,0:T(8,128)(2,1)}), bf16[16,160,128]{2,1,0:T(8,128)(2,1)S(1)}, u32[]{:S(2)}, u32[]{:S(2)}) %all-to-all-start.4) | async-done | bytes 655392 | tf_op jit(solution)/shard_map/all_to_all | solution.py:26
  (65 shorter events, 23.2 us)
Async XLA Ops:
  0.6 6.5 %copy-start.4 = (bf16[128,128]{1,0:T(8,128)(2,1)S(1)}, bf16[128,128]{1,0:T(8,128)(2,1)}, u32[]{:S(2)}) copy-start(bf16[128,128]{1,0:T(8,128)(2,1)} %param.8) | copy-start | bytes 98308
  2.8 44.9 %all-to-all-start = ((bf16[8,136,128]{2,1,0:T(8,128)(2,1)}), bf16[8,136,128]{2,1,0:T(8,128)(2,1)S(1)}, u32[]{:S(2)}, u32[]{:S(2)}) async-start(bf16[8,136,128]{2,1,0:T(8,128)(2,1)} %shard_map.102), calls=%async_computation | async-start | bytes 557056 | tf_op jit(solution)/shard_map/all_to_all | solution.py:26
  50.4 21.0 %copy-start.2 = (bf16[128,1024]{1,0:T(8,128)(2,1)S(1)}, bf16[128,1024]{1,0:T(8,128)(2,1)}, u32[]{:S(2)}) copy-start(bf16[128,1024]{1,0:T(8,128)(2,1)} %queries.1) | copy-start | bytes 786436
  50.4 21.0 %copy-start.3 = (bf16[128,1024]{1,0:T(8,128)(2,1)S(1)}, bf16[128,1024]{1,0:T(8,128)(2,1)}, u32[]{:S(2)}) copy-start(bf16[128,1024]{1,0:T(8,128)(2,1)} %dout.1) | copy-start | bytes 786436
  50.4 21.0 %copy-start.6 = (f32[128,8]{0,1:T(8,128)S(1)}, f32[128,8]{0,1:T(8,128)}, u32[]{:S(2)}) copy-start(f32[128,8]{0,1:T(8,128)} %param.10) | copy-start | bytes 12292
  50.4 21.0 %copy-start.7 = (s32[2,16]{1,0:T(2,128)S(1)}, s32[2,16]{1,0:T(2,128)}, u32[]{:S(2)}) copy-start(s32[2,16]{1,0:T(2,128)} %chosen.5) | copy-start | bytes 388
  71.4 20.7 %copy-start = (bf16[8,512,128]{2,1,0:T(8,128)(2,1)}, bf16[8,512,128]{2,1,0:T(8,128)(2,1)S(1)}, u32[]{:S(2)}) copy-start(bf16[8,512,128]{2,1,0:T(8,128)(2,1)S(1)} %all_to_all.25) | copy-start | bytes 3145732
  73.7 18.4 %copy-start.5 = (s32[8,1,32]{2,1,0:T(1,128)S(1)}, s32[8,1,32]{2,1,0:T(1,128)}, u32[]{:S(2)}) copy-start(s32[8,1,32]{2,1,0:T(1,128)} %slice_convert_fusion) | copy-start | bytes 3076
  92.1 9.2 %copy-start.18 = (bf16[128,128]{1,0:T(8,128)(2,1)S(1)}, bf16[128,128]{1,0:T(8,128)(2,1)}, u32[]{:S(2)}) copy-start(bf16[128,128]{1,0:T(8,128)(2,1)} %param.9) | copy-start | bytes 98308
  94.4 119.9 %all-to-all-start.3 = ((bf16[16,128,128]{2,1,0:T(8,128)(2,1)}), bf16[16,128,128]{2,1,0:T(8,128)(2,1)S(1)}, u32[]{:S(2)}, u32[]{:S(2)}) async-start(bf16[16,128,128]{2,1,0:T(8,128)(2,1)} %bitcast.13), calls=%async_computation.3 | async-start | bytes 1048576 | tf_op jit(solution)/shard_map/all_to_all | solution.py:26
  152.5 3.8 %collective-permute-start = (bf16[64,32,128]{2,1,0:T(8,128)(2,1)S(1)}, bf16[64,32,128]{2,1,0:T(8,128)(2,1)S(1)}, u32[]{:S(2)}, u32[]{:S(2)}) collective-permute-start(bf16[64,32,128]{2,1,0:T(8,128)(2,1)S(1)} %bitcast.48), channel_id=1, source_target_pairs={{0,4},{4,0},{1,5},{5,1},{2,6},{6,2},{3,7},{7,3},{8,12},{12,8},{9,1... | collective-permute-start | bytes 1572872 | tf_op jit(solution)/shard_map/ppermute | solution.py:367
  159.4 17.3 %collective-permute-start.1 = (bf16[32,32,128]{2,1,0:T(8,128)(2,1)}, bf16[32,32,128]{2,1,0:T(8,128)(2,1)S(1)}, u32[]{:S(2)}, u32[]{:S(2)}) collective-permute-start(bf16[32,32,128]{2,1,0:T(8,128)(2,1)} %get-tuple-element.20), channel_id=1, source_target_pairs={{0,8},{8,16},{16,24},{24,0},{1,9},{9,17},{17,25},{25,1},{2,10},{10... | collective-permute-start | bytes 786440 | tf_op jit(solution)/shard_map/ppermute | solution.py:364
  161.9 14.7 %collective-permute-start.2 = (bf16[32,32,128]{2,1,0:T(8,128)(2,1)}, bf16[32,32,128]{2,1,0:T(8,128)(2,1)S(1)}, u32[]{:S(2)}, u32[]{:S(2)}) collective-permute-start(bf16[32,32,128]{2,1,0:T(8,128)(2,1)} %get-tuple-element.21), channel_id=1, source_target_pairs={{0,16},{8,24},{16,0},{24,8},{1,17},{9,25},{17,1},{25,9},{2,18},{10... | collective-permute-start | bytes 786440 | tf_op jit(solution)/shard_map/ppermute | solution.py:364
  165.8 13.3 %collective-permute-start.3 = (bf16[32,32,128]{2,1,0:T(8,128)(2,1)}, bf16[32,32,128]{2,1,0:T(8,128)(2,1)S(1)}, u32[]{:S(2)}, u32[]{:S(2)}) collective-permute-start(bf16[32,32,128]{2,1,0:T(8,128)(2,1)} %get-tuple-element.22), channel_id=1, source_target_pairs={{0,24},{8,0},{16,8},{24,16},{1,25},{9,1},{17,9},{25,17},{2,26},{10... | collective-permute-start | bytes 786440 | tf_op jit(solution)/shard_map/ppermute | solution.py:364
  168.5 29.2 %collective-permute-start.8 = (bf16[8,136,128]{2,1,0:T(8,128)(2,1)S(1)}, bf16[8,136,128]{2,1,0:T(8,128)(2,1)S(1)}, u32[]{:S(2)}, u32[]{:S(2)}) collective-permute-start(bf16[8,136,128]{2,1,0:T(8,128)(2,1)S(1)} %all-to-all-done), channel_id=1, source_target_pairs={{0,1},{1,0},{2,3},{3,2},{4,5},{5,4},{6,7},{7,6},{8,9},{9,8},{10,11... | collective-permute-start | bytes 835592 | tf_op jit(solution)/shard_map/ppermute | solution.py:351
  187.8 12.1 %collective-permute-start.4 = (bf16[32,32,128]{2,1,0:T(8,128)(2,1)}, bf16[32,32,128]{2,1,0:T(8,128)(2,1)S(1)}, u32[]{:S(2)}, u32[]{:S(2)}) collective-permute-start(bf16[32,32,128]{2,1,0:T(8,128)(2,1)} %get-tuple-element.29), channel_id=1, source_target_pairs={{0,8},{8,16},{16,24},{24,0},{1,9},{9,17},{17,25},{25,1},{2,10},{10... | collective-permute-start | bytes 786440 | tf_op jit(solution)/shard_map/ppermute | solution.py:364
  190.0 15.8 %collective-permute-start.5 = (bf16[32,32,128]{2,1,0:T(8,128)(2,1)}, bf16[32,32,128]{2,1,0:T(8,128)(2,1)S(1)}, u32[]{:S(2)}, u32[]{:S(2)}) collective-permute-start(bf16[32,32,128]{2,1,0:T(8,128)(2,1)} %get-tuple-element.30), channel_id=1, source_target_pairs={{0,16},{8,24},{16,0},{24,8},{1,17},{9,25},{17,1},{25,9},{2,18},{10... | collective-permute-start | bytes 786440 | tf_op jit(solution)/shard_map/ppermute | solution.py:364
  195.7 11.4 %collective-permute-start.6 = (bf16[32,32,128]{2,1,0:T(8,128)(2,1)}, bf16[32,32,128]{2,1,0:T(8,128)(2,1)S(1)}, u32[]{:S(2)}, u32[]{:S(2)}) collective-permute-start(bf16[32,32,128]{2,1,0:T(8,128)(2,1)} %get-tuple-element.31), channel_id=1, source_target_pairs={{0,24},{8,0},{16,8},{24,16},{1,25},{9,1},{17,9},{25,17},{2,26},{10... | collective-permute-start | bytes 786440 | tf_op jit(solution)/shard_map/ppermute | solution.py:364
  197.7 30.1 %collective-permute-start.9 = (bf16[2,8,136,128]{3,2,1,0:T(8,128)(2,1)S(1)}, bf16[2,8,136,128]{3,2,1,0:T(8,128)(2,1)S(1)}, u32[]{:S(2)}, u32[]{:S(2)}) collective-permute-start(bf16[2,8,136,128]{3,2,1,0:T(8,128)(2,1)S(1)} %pad_maximum_fusion.refs_0_), channel_id=1, source_target_pairs={{0,3},{1,2},{2,1},{3,0},{4,7},{5,6},{6,5},{7,4},{8,11},{9,10},{10,... | collective-permute-start | bytes 1671176 | tf_op jit(solution)/shard_map/ppermute | solution.py:356
  199.9 7.2 %copy-start.12 = (bf16[32,32,128]{2,1,0:T(8,128)(2,1)}, bf16[32,32,128]{2,1,0:T(8,128)(2,1)S(1)}, u32[]{:S(2)}) copy-start(bf16[32,32,128]{2,1,0:T(8,128)(2,1)S(1)} %collective-permute-done.4.refs_1_) | copy-start | bytes 786436
  212.1 15.7 %copy-start.1 = (f32[64,32,128]{2,1,0:T(8,128)S(1)}, f32[64,32,128]{2,1,0:T(8,128)}, u32[]{:S(2)}) copy-start(f32[64,32,128]{2,1,0:T(8,128)} %get-tuple-element.32) | copy-start | bytes 3145732
  212.1 15.7 %collective-permute-start.7 = (bf16[64,32,128]{2,1,0:T(8,128)(2,1)}, bf16[64,32,128]{2,1,0:T(8,128)(2,1)S(1)}, u32[]{:S(2)}, u32[]{:S(2)}) collective-permute-start(bf16[64,32,128]{2,1,0:T(8,128)(2,1)} %get-tuple-element.33), channel_id=1, source_target_pairs={{0,4},{4,0},{1,5},{5,1},{2,6},{6,2},{3,7},{7,3},{8,12},{12,8},{9,1... | collective-permute-start | bytes 1572872 | tf_op jit(solution)/shard_map/ppermute | solution.py:367
  229.8 45.2 %all-to-all-start.4 = ((bf16[16,160,128]{2,1,0:T(8,128)(2,1)}), bf16[16,160,128]{2,1,0:T(8,128)(2,1)S(1)}, u32[]{:S(2)}, u32[]{:S(2)}) async-start(bf16[16,160,128]{2,1,0:T(8,128)(2,1)} %shard_map.110), calls=%async_computation.4 | async-start | bytes 1310720 | tf_op jit(solution)/shard_map/all_to_all | solution.py:26
  240.3 35.4 %copy-start.19 = (f32[4,32,128]{2,1,0:T(8,128)S(1)}, f32[4,32,128]{2,1,0:T(8,128)}, u32[]{:S(2)}) copy-start(f32[4,32,128]{2,1,0:T(8,128)} %get-tuple-element.25) | copy-start | bytes 196612
  (9 other events, 15.6 us)

commit v6 on v5

--- a/solution.py
+++ b/solution.py
@@ -223,7 +223,8 @@
     targets, refs = refs[:nx], refs[nx:]
     own_sum, low, sel, sel_v, kpos, rows, total, part, send, held, queries, dout, got_k, sems = refs
     got_v = tuple(held.at[s] for s in range(nx))
-    for copy in moves(list(zip(ins, (queries, dout, got_k, *got_v))), sems):
+    copies = moves(list(zip(ins, (queries, got_k, dout, *got_v))), sems)
+    for copy in copies[:2]:
         copy.wait()
     peers, kblocks = nq * nz, own_k.shape[0]
     qblocks, pairs = queries.shape[0] // QB, queries.shape[1] // HD // 2
@@ -240,6 +241,9 @@
 
     for b in range(qblocks):
         select(slots(b, lambda q: q), got_k, own_k, sel.at[b])
+        if not b:
+            for copy in copies[2:]:
+                copy.wait()
         select(slots(b, behind), got_v, own_v, sel_v)
         set_positions(slots(b, ahead), kpos)
         start = here[0] * queries.shape[0] + b * QB
@@ -436,7 +440,7 @@
             *(pltpu.VMEM((nx, nc * nz, KB, HD), BF16), rows, rows, slots, dma(3 + nx)),
         ],
         to="h" * nx + "vvv",
-    )(names, me, lse, own_k, own_v, queries, out_grad, got_k, *got_v)
+    )(names, me, lse, own_k, own_v, queries, got_k, out_grad, *got_v)
     came_k = around(sent_k)
     blocks = (nz * kblocks, KB, HD)
     dense_k, other_k = call(

time: 277 us -> 277 us (level)
  the two profiles are of different devices: /device:TPU:24 before, /device:TPU:8 now
where the time goes in v6:
time: 277 us; the launch traced here: 276 us
  blocking collectives  144 us (52%)
  starting transfers between devices  50.4 us (18%)
  waiting for transfers between devices  47.6 us (17%)
  Pallas kernels  27.8 us (10%)
  local copies, waits for them, and re-layouts  3.5 us (1%)
    all_gather x2, blocking collectives, column(): lax.all_gather(rows, 'z', axis=0, tiled=True).reshape(nz * kblocks, KB, HD)  91.7 us
    all_to_all x2, blocking collectives, to_peers(): return lax.all_to_all(parts, axis, split_axis=0, concat_axis=0, tiled=True)  39.4 us
    all_to_all x3, waiting for transfers between devices, to_peers(): return lax.all_to_all(parts, axis, split_axis=0, concat_axis=0, tiled=True)  31.5 us
    all_to_all x3, starting transfers between devices, to_peers(): return lax.all_to_all(parts, axis, split_axis=0, concat_axis=0, tiled=True)  21.7 us
    ppermute x6, starting transfers between devices, around(): lax.ppermute(pieces[s], 'x', turns[s])  18.9 us
    ppermute x6, waiting for transfers between devices, around(): lax.ppermute(pieces[s], 'x', turns[s])  14.3 us
    all_gather x1, blocking collectives, local(): all_low = lax.all_gather(value_grad.astype(BF16), XC, axis=0)  12.8 us
    pallas_call x1, Pallas kernels, local(): call(functools.partial(key_terms, nx, nc, nz), (*(slab,) * nx, terms[1],...  7.86 us
  transfers between devices with their start and end apart: 13, of which 6 were waited for; matrix products, arithmetic and copies ran while one was open for 0% of the time, Pallas kernels for 6%

profile of v6, /device:TPU:8, one launch (start us, length us, event | category | flops | bytes accessed | tf_op | source)
XLA Modules:
  0.0 276.3 jit_solution(17964460974375395810)
XLA Ops:
  2.8 4.3 %all-to-all-start = ((bf16[8,136,128]{2,1,0:T(8,128)(2,1)}), bf16[8,136,128]{2,1,0:T(8,128)(2,1)S(1)}, u32[]{:S(2)}, u32[]{:S(2)}) async-start(bf16[8,136,128]{2,1,0:T(8,128)(2,1)} %shard_map.102), calls=%async_computation | async-start | bytes 557056 | tf_op jit(solution)/shard_map/all_to_all | solution.py:26
  7.1 40.5 %all_gather.10 = bf16[2048,128]{1,0:T(8,128)(2,1)} all-gather(bf16[128,128]{1,0:T(8,128)(2,1)S(1)} %copy-done.4), channel_id=1, replica_groups=mesh['z'=16,'x'=4,'c'=2,'tp'=4] {'z'}, dimensions={0}, use_global_device_ids=true | all-gather | bytes 557056 | tf_op jit(solution)/shard_map/all_gather | solution.py:374
  50.4 21.0 %all_to_all.25 = bf16[8,512,128]{2,1,0:T(8,128)(2,1)S(1)} all-to-all(bf16[8,512,128]{2,1,0:T(8,128)(2,1)} %bitcast.46), channel_id=1, replica_groups=mesh['z'=16,'x'=4,'c'=2,'tp'=4] {'x','c'}, dimensions={0} | all-to-all | bytes 2097152 | tf_op jit(solution)/shard_map/all_to_all | solution.py:26
  73.7 18.4 %all_to_all.26 = bf16[8,512,128]{2,1,0:T(8,128)(2,1)S(1)} all-to-all(bf16[8,512,128]{2,1,0:T(8,128)(2,1)S(1)} %bitcast.34), channel_id=1, replica_groups=mesh['z'=16,'x'=4,'c'=2,'tp'=4] {'x','c'}, dimensions={0} | all-to-all | bytes 2097152 | tf_op jit(solution)/shard_map/all_to_all | solution.py:26
  92.1 2.3 shard_map.108
  94.4 6.9 %all-to-all-start.3 = ((bf16[16,128,128]{2,1,0:T(8,128)(2,1)}), bf16[16,128,128]{2,1,0:T(8,128)(2,1)S(1)}, u32[]{:S(2)}, u32[]{:S(2)}) async-start(bf16[16,128,128]{2,1,0:T(8,128)(2,1)} %bitcast.13), calls=%async_computation.3 | async-start | bytes 1048576 | tf_op jit(solution)/shard_map/all_to_all | solution.py:26
  101.3 51.2 %all_gather.11 = bf16[2048,128]{1,0:T(8,128)(2,1)S(1)} all-gather(bf16[128,128]{1,0:T(8,128)(2,1)S(1)} %copy-done.18), channel_id=1, replica_groups=mesh['z'=16,'x'=4,'c'=2,'tp'=4] {'z'}, dimensions={0}, use_global_device_ids=true | all-gather | bytes 557056 | tf_op jit(solution)/shard_map/all_gather | solution.py:374
  157.0 2.3 shard_map.104
  159.4 2.6 collective-permute-start.1
  161.9 3.9 %collective-permute-start.2 = (bf16[32,32,128]{2,1,0:T(8,128)(2,1)}, bf16[32,32,128]{2,1,0:T(8,128)(2,1)S(1)}, u32[]{:S(2)}, u32[]{:S(2)}) collective-permute-start(bf16[32,32,128]{2,1,0:T(8,128)(2,1)} %get-tuple-element.21), channel_id=1, source_target_pairs={{0,16},{8,24},{16,0},{24,8},{1,17},{9,25},{17,1},{25,9},{2,18},{10... | collective-permute-start | bytes 786440 | tf_op jit(solution)/shard_map/ppermute | solution.py:368
  165.9 2.6 collective-permute-start.3
  168.5 2.4 collective-permute-start.8
  170.8 5.8 %collective-permute-done.1.refs_4_ = bf16[32,32,128]{2,1,0:T(8,128)(2,1)S(1)} collective-permute-done((bf16[32,32,128]{2,1,0:T(8,128)(2,1)}, bf16[32,32,128]{2,1,0:T(8,128)(2,1)S(1)}, u32[]{:S(2)}, u32[]{:S(2)}) %collective-permute-start.1) | collective-permute-done | bytes 262176 | tf_op jit(solution)/shard_map/ppermute | solution.py:368
  176.7 2.5 collective-permute-done.3.refs_6_
  179.9 7.9 %shard_map.105 = (bf16[32,32,128]{2,1,0:T(8,128)(2,1)}, bf16[32,32,128]{2,1,0:T(8,128)(2,1)}, bf16[32,32,128]{2,1,0:T(8,128)(2,1)}, bf16[32,32,128]{2,1,0:T(8,12...) custom-call(s32[2,16]{1,0:T(2,128)} %chosen.5, s32[1]{0:T(128)} %bitcast.here, ...), custom_call_target="tpu_custom_call" | custom-call | tf_op jit(solution)/shard_map/pallas_call | solution.py:429
  187.8 2.2 collective-permute-start.4
  190.0 5.7 %collective-permute-start.5 = (bf16[32,32,128]{2,1,0:T(8,128)(2,1)}, bf16[32,32,128]{2,1,0:T(8,128)(2,1)S(1)}, u32[]{:S(2)}, u32[]{:S(2)}) collective-permute-start(bf16[32,32,128]{2,1,0:T(8,128)(2,1)} %get-tuple-element.30), channel_id=1, source_target_pairs={{0,16},{8,24},{16,0},{24,8},{1,17},{9,25},{17,1},{25,9},{2,18},{10... | collective-permute-start | bytes 786440 | tf_op jit(solution)/shard_map/ppermute | solution.py:368
  197.7 3.5 %collective-permute-start.9 = (bf16[2,8,136,128]{3,2,1,0:T(8,128)(2,1)S(1)}, bf16[2,8,136,128]{3,2,1,0:T(8,128)(2,1)S(1)}, u32[]{:S(2)}, u32[]{:S(2)}) collective-permute-start(bf16[2,8,136,128]{3,2,1,0:T(8,128)(2,1)S(1)} %pad_maximum_fusion.refs_0_), channel_id=1, source_target_pairs={{0,3},{1,2},{2,1},{3,0},{4,7},{5,6},{6,5},{7,4},{8,11},{9,10},{10,... | collective-permute-start | bytes 1671176 | tf_op jit(solution)/shard_map/ppermute | solution.py:360
  201.2 4.6 %collective-permute-done.5.refs_2_ = bf16[32,32,128]{2,1,0:T(8,128)(2,1)S(1)} collective-permute-done((bf16[32,32,128]{2,1,0:T(8,128)(2,1)}, bf16[32,32,128]{2,1,0:T(8,128)(2,1)S(1)}, u32[]{:S(2)}, u32[]{:S(2)}) %collective-permute-start.5) | collective-permute-done | bytes 262176 | tf_op jit(solution)/shard_map/ppermute | solution.py:368
  207.8 4.3 %shard_map.109 = (f32[64,32,128]{2,1,0:T(8,128)}, bf16[64,32,128]{2,1,0:T(8,128)(2,1)}) custom-call(s32[8,32]{1,0:T(8,128)} %bitcast.42, s32[1]{0:T(128)} %bitcast.here, bf16[32,32,128]{2,1,0:T(8,128)(2,1)} %get-tuple-element.28.refs_0_, bf16[32,32,128]{2,1,0:T(8,128)(2,1)} %copy-done.12, bf16[32,32,128]{2,1,0:T(8,128)(2,1)} %copy-done.13, ...), custom_call_target="tpu_custom_call" | custom-call | tf_op jit(solution)/shard_map/pallas_call | solution.py:446
  215.0 12.8 %all_gather.12.low = bf16[8,128,128]{2,1,0:T(8,128)(2,1)S(1)} all-gather(bf16[1,128,128]{2,1,0:T(8,128)(2,1)S(1)} %fusion), channel_id=1, replica_groups=mesh['z'=16,'x'=4,'c'=2,'tp'=4] {'x','c'}, dimensions={0}, use_global_device_ids=true | all-gather | bytes 294912 | tf_op jit(solution)/shard_map/all_gather | solution.py:461
  229.8 10.5 %all-to-all-start.4 = ((bf16[16,160,128]{2,1,0:T(8,128)(2,1)}), bf16[16,160,128]{2,1,0:T(8,128)(2,1)S(1)}, u32[]{:S(2)}, u32[]{:S(2)}) async-start(bf16[16,160,128]{2,1,0:T(8,128)(2,1)} %shard_map.110), calls=%async_computation.4 | async-start | bytes 1310720 | tf_op jit(solution)/shard_map/all_to_all | solution.py:26
  240.3 2.6 shard_map.106
  243.5 31.4 %all-to-all-done.4 = bf16[16,160,128]{2,1,0:T(8,128)(2,1)S(1)} async-done(((bf16[16,160,128]{2,1,0:T(8,128)(2,1)}), bf16[16,160,128]{2,1,0:T(8,128)(2,1)S(1)}, u32[]{:S(2)}, u32[]{:S(2)}) %all-to-all-start.4) | async-done | bytes 655392 | tf_op jit(solution)/shard_map/all_to_all | solution.py:26
  (65 shorter events, 23.2 us)
Async XLA Ops:
  0.6 6.5 %copy-start.4 = (bf16[128,128]{1,0:T(8,128)(2,1)S(1)}, bf16[128,128]{1,0:T(8,128)(2,1)}, u32[]{:S(2)}) copy-start(bf16[128,128]{1,0:T(8,128)(2,1)} %param.8) | copy-start | bytes 98308
  2.8 44.9 %all-to-all-start = ((bf16[8,136,128]{2,1,0:T(8,128)(2,1)}), bf16[8,136,128]{2,1,0:T(8,128)(2,1)S(1)}, u32[]{:S(2)}, u32[]{:S(2)}) async-start(bf16[8,136,128]{2,1,0:T(8,128)(2,1)} %shard_map.102), calls=%async_computation | async-start | bytes 557056 | tf_op jit(solution)/shard_map/all_to_all | solution.py:26
  50.4 21.0 %copy-start.2 = (bf16[128,1024]{1,0:T(8,128)(2,1)S(1)}, bf16[128,1024]{1,0:T(8,128)(2,1)}, u32[]{:S(2)}) copy-start(bf16[128,1024]{1,0:T(8,128)(2,1)} %queries.1) | copy-start | bytes 786436
  50.4 21.0 %copy-start.3 = (bf16[128,1024]{1,0:T(8,128)(2,1)S(1)}, bf16[128,1024]{1,0:T(8,128)(2,1)}, u32[]{:S(2)}) copy-start(bf16[128,1024]{1,0:T(8,128)(2,1)} %dout.1) | copy-start | bytes 786436
  50.4 21.0 %copy-start.6 = (f32[128,8]{0,1:T(8,128)S(1)}, f32[128,8]{0,1:T(8,128)}, u32[]{:S(2)}) copy-start(f32[128,8]{0,1:T(8,128)} %param.10) | copy-start | bytes 12292
  50.4 21.0 %copy-start.7 = (s32[2,16]{1,0:T(2,128)S(1)}, s32[2,16]{1,0:T(2,128)}, u32[]{:S(2)}) copy-start(s32[2,16]{1,0:T(2,128)} %chosen.5) | copy-start | bytes 388
  71.4 20.6 %copy-start = (bf16[8,512,128]{2,1,0:T(8,128)(2,1)}, bf16[8,512,128]{2,1,0:T(8,128)(2,1)S(1)}, u32[]{:S(2)}) copy-start(bf16[8,512,128]{2,1,0:T(8,128)(2,1)S(1)} %all_to_all.25) | copy-start | bytes 3145732
  73.7 18.4 %copy-start.5 = (s32[8,1,32]{2,1,0:T(1,128)S(1)}, s32[8,1,32]{2,1,0:T(1,128)}, u32[]{:S(2)}) copy-start(s32[8,1,32]{2,1,0:T(1,128)} %slice_convert_fusion) | copy-start | bytes 3076
  92.1 9.2 %copy-start.18 = (bf16[128,128]{1,0:T(8,128)(2,1)S(1)}, bf16[128,128]{1,0:T(8,128)(2,1)}, u32[]{:S(2)}) copy-start(bf16[128,128]{1,0:T(8,128)(2,1)} %param.9) | copy-start | bytes 98308
  94.4 119.9 %all-to-all-start.3 = ((bf16[16,128,128]{2,1,0:T(8,128)(2,1)}), bf16[16,128,128]{2,1,0:T(8,128)(2,1)S(1)}, u32[]{:S(2)}, u32[]{:S(2)}) async-start(bf16[16,128,128]{2,1,0:T(8,128)(2,1)} %bitcast.13), calls=%async_computation.3 | async-start | bytes 1048576 | tf_op jit(solution)/shard_map/all_to_all | solution.py:26
  152.5 3.8 %collective-permute-start = (bf16[64,32,128]{2,1,0:T(8,128)(2,1)S(1)}, bf16[64,32,128]{2,1,0:T(8,128)(2,1)S(1)}, u32[]{:S(2)}, u32[]{:S(2)}) collective-permute-start(bf16[64,32,128]{2,1,0:T(8,128)(2,1)S(1)} %bitcast.48), channel_id=1, source_target_pairs={{0,4},{4,0},{1,5},{5,1},{2,6},{6,2},{3,7},{7,3},{8,12},{12,8},{9,1... | collective-permute-start | bytes 1572872 | tf_op jit(solution)/shard_map/ppermute | solution.py:371
  159.4 17.3 %collective-permute-start.1 = (bf16[32,32,128]{2,1,0:T(8,128)(2,1)}, bf16[32,32,128]{2,1,0:T(8,128)(2,1)S(1)}, u32[]{:S(2)}, u32[]{:S(2)}) collective-permute-start(bf16[32,32,128]{2,1,0:T(8,128)(2,1)} %get-tuple-element.20), channel_id=1, source_target_pairs={{0,8},{8,16},{16,24},{24,0},{1,9},{9,17},{17,25},{25,1},{2,10},{10... | collective-permute-start | bytes 786440 | tf_op jit(solution)/shard_map/ppermute | solution.py:368
  161.9 14.7 %collective-permute-start.2 = (bf16[32,32,128]{2,1,0:T(8,128)(2,1)}, bf16[32,32,128]{2,1,0:T(8,128)(2,1)S(1)}, u32[]{:S(2)}, u32[]{:S(2)}) collective-permute-start(bf16[32,32,128]{2,1,0:T(8,128)(2,1)} %get-tuple-element.21), channel_id=1, source_target_pairs={{0,16},{8,24},{16,0},{24,8},{1,17},{9,25},{17,1},{25,9},{2,18},{10... | collective-permute-start | bytes 786440 | tf_op jit(solution)/shard_map/ppermute | solution.py:368
  165.9 13.3 %collective-permute-start.3 = (bf16[32,32,128]{2,1,0:T(8,128)(2,1)}, bf16[32,32,128]{2,1,0:T(8,128)(2,1)S(1)}, u32[]{:S(2)}, u32[]{:S(2)}) collective-permute-start(bf16[32,32,128]{2,1,0:T(8,128)(2,1)} %get-tuple-element.22), channel_id=1, source_target_pairs={{0,24},{8,0},{16,8},{24,16},{1,25},{9,1},{17,9},{25,17},{2,26},{10... | collective-permute-start | bytes 786440 | tf_op jit(solution)/shard_map/ppermute | solution.py:368
  168.5 29.2 %collective-permute-start.8 = (bf16[8,136,128]{2,1,0:T(8,128)(2,1)S(1)}, bf16[8,136,128]{2,1,0:T(8,128)(2,1)S(1)}, u32[]{:S(2)}, u32[]{:S(2)}) collective-permute-start(bf16[8,136,128]{2,1,0:T(8,128)(2,1)S(1)} %all-to-all-done), channel_id=1, source_target_pairs={{0,1},{1,0},{2,3},{3,2},{4,5},{5,4},{6,7},{7,6},{8,9},{9,8},{10,11... | collective-permute-start | bytes 835592 | tf_op jit(solution)/shard_map/ppermute | solution.py:355
  187.8 13.4 %collective-permute-start.4 = (bf16[32,32,128]{2,1,0:T(8,128)(2,1)}, bf16[32,32,128]{2,1,0:T(8,128)(2,1)S(1)}, u32[]{:S(2)}, u32[]{:S(2)}) collective-permute-start(bf16[32,32,128]{2,1,0:T(8,128)(2,1)} %get-tuple-element.29), channel_id=1, source_target_pairs={{0,8},{8,16},{16,24},{24,0},{1,9},{9,17},{17,25},{25,1},{2,10},{10... | collective-permute-start | bytes 786440 | tf_op jit(solution)/shard_map/ppermute | solution.py:368
  190.0 15.8 %collective-permute-start.5 = (bf16[32,32,128]{2,1,0:T(8,128)(2,1)}, bf16[32,32,128]{2,1,0:T(8,128)(2,1)S(1)}, u32[]{:S(2)}, u32[]{:S(2)}) collective-permute-start(bf16[32,32,128]{2,1,0:T(8,128)(2,1)} %get-tuple-element.30), channel_id=1, source_target_pairs={{0,16},{8,24},{16,0},{24,8},{1,17},{9,25},{17,1},{25,9},{2,18},{10... | collective-permute-start | bytes 786440 | tf_op jit(solution)/shard_map/ppermute | solution.py:368
  195.7 11.4 %collective-permute-start.6 = (bf16[32,32,128]{2,1,0:T(8,128)(2,1)}, bf16[32,32,128]{2,1,0:T(8,128)(2,1)S(1)}, u32[]{:S(2)}, u32[]{:S(2)}) collective-permute-start(bf16[32,32,128]{2,1,0:T(8,128)(2,1)} %get-tuple-element.31), channel_id=1, source_target_pairs={{0,24},{8,0},{16,8},{24,16},{1,25},{9,1},{17,9},{25,17},{2,26},{10... | collective-permute-start | bytes 786440 | tf_op jit(solution)/shard_map/ppermute | solution.py:368
  197.7 30.1 %collective-permute-start.9 = (bf16[2,8,136,128]{3,2,1,0:T(8,128)(2,1)S(1)}, bf16[2,8,136,128]{3,2,1,0:T(8,128)(2,1)S(1)}, u32[]{:S(2)}, u32[]{:S(2)}) collective-permute-start(bf16[2,8,136,128]{3,2,1,0:T(8,128)(2,1)S(1)} %pad_maximum_fusion.refs_0_), channel_id=1, source_target_pairs={{0,3},{1,2},{2,1},{3,0},{4,7},{5,6},{6,5},{7,4},{8,11},{9,10},{10,... | collective-permute-start | bytes 1671176 | tf_op jit(solution)/shard_map/ppermute | solution.py:360
  201.2 5.9 %copy-start.12 = (bf16[32,32,128]{2,1,0:T(8,128)(2,1)}, bf16[32,32,128]{2,1,0:T(8,128)(2,1)S(1)}, u32[]{:S(2)}) copy-start(bf16[32,32,128]{2,1,0:T(8,128)(2,1)S(1)} %collective-permute-done.4.refs_1_) | copy-start | bytes 786436
  212.1 15.7 %copy-start.1 = (f32[64,32,128]{2,1,0:T(8,128)S(1)}, f32[64,32,128]{2,1,0:T(8,128)}, u32[]{:S(2)}) copy-start(f32[64,32,128]{2,1,0:T(8,128)} %get-tuple-element.32) | copy-start | bytes 3145732
  212.1 15.7 %collective-permute-start.7 = (bf16[64,32,128]{2,1,0:T(8,128)(2,1)}, bf16[64,32,128]{2,1,0:T(8,128)(2,1)S(1)}, u32[]{:S(2)}, u32[]{:S(2)}) collective-permute-start(bf16[64,32,128]{2,1,0:T(8,128)(2,1)} %get-tuple-element.33), channel_id=1, source_target_pairs={{0,4},{4,0},{1,5},{5,1},{2,6},{6,2},{3,7},{7,3},{8,12},{12,8},{9,1... | collective-permute-start | bytes 1572872 | tf_op jit(solution)/shard_map/ppermute | solution.py:371
  229.8 45.2 %all-to-all-start.4 = ((bf16[16,160,128]{2,1,0:T(8,128)(2,1)}), bf16[16,160,128]{2,1,0:T(8,128)(2,1)S(1)}, u32[]{:S(2)}, u32[]{:S(2)}) async-start(bf16[16,160,128]{2,1,0:T(8,128)(2,1)} %shard_map.110), calls=%async_computation.4 | async-start | bytes 1310720 | tf_op jit(solution)/shard_map/all_to_all | solution.py:26
  240.3 35.4 %copy-start.19 = (f32[4,32,128]{2,1,0:T(8,128)S(1)}, f32[4,32,128]{2,1,0:T(8,128)}, u32[]{:S(2)}) copy-start(f32[4,32,128]{2,1,0:T(8,128)} %get-tuple-element.25) | copy-start | bytes 196612
  (9 other events, 15.6 us)
